TPU v7x, 256 devices: a whole 4x4x8 slice. The times are simulated.
256 devices in a mesh: dp: 4 (over x), kv: 32 (over z, y), tp: 2 (over core).
Axes of the slice: x: 4, y: 4, z: 8, core: 2. Of those that a mesh axis runs over, the one named last changes fastest.
Arguments:
- hidden_in: bfloat16 [384, 2048], P('dp', ('kv', 'tp')), may hold values from -21 to 21
- state: float32 [384, 16, 128, 128], P(('dp', 'kv'), 'tp'), may hold values from -6 to 6
- forget_floor: float32 [16, 128], P('tp'), may hold values from 0 to 0.9
- ffn_gain_one: float32 [2048], replicated, may hold values from 0.1 to 1.9
- w_gate_one: bfloat16 [2048, 5632], P(None, ('kv', 'tp')), may hold values from -0.125 to 0.125
- w_up_one: bfloat16 [2048, 5632], P(None, ('kv', 'tp')), may hold values from -0.125 to 0.125
- w_down_one: bfloat16 [5632, 2048], P(('kv', 'tp')), may hold values from -0.21875 to 0.21875
- mix_gain: float32 [2048], replicated, may hold values from 0.1 to 1.9
- w_query: bfloat16 [2048, 16, 128], P(None, 'tp', 'kv'), may hold values from -0.125 to 0.125
- w_forget: bfloat16 [2048, 16, 128], P(None, 'tp', 'kv'), may hold values from -0.125 to 0.125
- w_input: bfloat16 [2048, 16, 128], P(None, 'tp', 'kv'), may hold values from -0.125 to 0.125
- w_outgate: bfloat16 [2048, 16, 128], P(None, 'tp', 'kv'), may hold values from -0.125 to 0.125
- head_gain: float32 [16, 128], P('tp'), may hold values from 0.1 to 1.9
- w_mix_out: bfloat16 [2048, 2048], P(None, ('kv', 'tp')), may hold values from -0.125 to 0.125
- ffn_gain_two: float32 [2048], replicated, may hold values from 0.1 to 1.9
- w_gate_two: bfloat16 [2048, 5632], P(None, ('kv', 'tp')), may hold values from -0.125 to 0.125
- w_up_two: bfloat16 [2048, 5632], P(None, ('kv', 'tp')), may hold values from -0.125 to 0.125
- w_down_two: bfloat16 [5632, 2048], P(('kv', 'tp')), may hold values from -0.21875 to 0.21875
Outputs:
- output_rows: bfloat16 [384, 2048], P('dp', ('kv', 'tp'))
- new_state: float32 [384, 16, 128, 128], P(('dp', 'kv'), 'tp')
All inputs are finite; a program needn't handle non-finite values.
Results may differ from a plain program's by a relative error of at most 0.009.
Values may be sent and summed in bfloat16 or wider, within the bound.
No kernel may reach another device: no remote copies, remote signals or barrier semaphores. Data moves between devices by JAX's collectives and lax.ppermute only.
A program may use at most 64 MiB of HBM per device.

v0:
```python
import jax
import jax.numpy as jnp
from jax import lax
from jax.sharding import PartitionSpec as P

EPS = 1e-06


def copy_for_each(x, axis):
    copies = jnp.broadcast_to(x, (lax.axis_size(axis), *x.shape))
    return lax.all_to_all(copies, axis, split_axis=0, concat_axis=0, tiled=True)


def in_order(tiles, dim):
    tiles = jnp.moveaxis(tiles, 0, dim)
    lengths = tiles.shape
    return tiles.reshape(*lengths[:dim], lengths[dim] * lengths[dim + 1], *lengths[dim + 2 :])


def gathered_copies(x, axis, dim):
    tiles = copy_for_each(x, axis)
    return in_order(tiles, dim)


def in_blocks(x, dim, devices):
    before, after = (x.shape[:dim], x.shape[dim + 1 :])
    return jnp.moveaxis(x.reshape(*before, devices, -1, *after), dim, 0)


def sent_and_summed(x, axis, dim):
    tiles = in_blocks(x, dim, lax.axis_size(axis))
    arrived = lax.all_to_all(tiles, axis, split_axis=0, concat_axis=0, tiled=True)
    return arrived.astype(jnp.float32).sum(axis=0)


def sent_together(arrays, axis, split_dim, concat_dim, along):
    widths = [a.shape[along] for a in arrays]
    both = jnp.concatenate(arrays, axis=along)
    whole = lax.all_to_all(both, axis, split_axis=split_dim, concat_axis=concat_dim, tiled=True)
    return tuple(jnp.split(whole, [sum(widths[:k]) for k in range(1, len(widths))], axis=along))


def local_norm(full_rows, gain_vec):
    values = full_rows.astype(jnp.float32)
    row_scale = lax.rsqrt(jnp.mean(values * values, axis=1, keepdims=True) + EPS)
    return (values * row_scale * gain_vec[None, :]).astype(jnp.bfloat16)


def spread_norm(shard_in, gain_vec):
    full_rows = gathered_copies(shard_in, ("kv", "tp"), 1)
    return local_norm(full_rows, gain_vec)


def mlp_term(normed, w_gate, w_upper, w_lower):
    gate_act = jnp.dot(normed, w_gate, preferred_element_type=jnp.float32)
    upper = jnp.dot(normed, w_upper, preferred_element_type=jnp.float32)
    hidden_mid = (jax.nn.silu(gate_act) * upper).astype(jnp.bfloat16)
    return jnp.dot(hidden_mid, w_lower, preferred_element_type=jnp.float32)


def project(normed, weight):
    flat = jnp.einsum("rd,dhk->rhk", normed, weight, preferred_element_type=jnp.float32)
    return flat.astype(jnp.bfloat16)


def shards(
    hidden_in,
    state,
    forget_floor,
    ffn_gain_one,
    w_gate_one,
    w_up_one,
    w_down_one,
    mix_gain,
    w_query,
    w_forget,
    w_input,
    w_outgate,
    head_gain,
    w_mix_out,
    ffn_gain_two,
    w_gate_two,
    w_up_two,
    w_down_two,
):
    columns = hidden_in.shape[1]
    normed_one = spread_norm(hidden_in, ffn_gain_one)
    ffn_term = mlp_term(normed_one, w_gate_one, w_up_one, w_down_one)
    summed_one = sent_and_summed(ffn_term.astype(jnp.bfloat16), ("kv", "tp"), 1)
    after_own = (hidden_in.astype(jnp.float32) + 0.5 * summed_one).astype(jnp.bfloat16)
    after_rows = gathered_copies(after_own, ("kv", "tp"), 1)
    normed_mix = local_norm(after_rows, mix_gain)
    projected = (
        project(normed_mix, w_query),
        project(normed_mix, w_forget),
        project(normed_mix, w_input),
        project(normed_mix, w_outgate),
    )
    query, forget_pre, inputs, out_gate = sent_together(
        (projected[0], projected[1], projected[2], projected[3]), "kv", 0, 2, 1
    )
    forget_raw = forget_pre.astype(jnp.float32)
    forget = forget_floor[None] + (1.0 - forget_floor[None]) * jax.nn.sigmoid(forget_raw)
    keep_in = (1.0 - forget_floor[None]) * jax.nn.sigmoid(-forget_raw)
    new_state = (
        forget[..., None] * state + keep_in[..., None] * inputs.astype(jnp.float32)[:, :, None, :]
    )
    readout = jnp.einsum(
        "shk,shkv->shv", query.astype(jnp.float32), new_state, precision=lax.Precision.HIGHEST
    )
    head_scale = lax.rsqrt(jnp.mean(readout * readout, axis=2, keepdims=True) + EPS)
    gated = readout * head_scale * head_gain[None] * jax.nn.silu(out_gate.astype(jnp.float32))
    seq_count = gated.shape[0]
    merged = gated.reshape(seq_count, -1).astype(jnp.bfloat16)
    gathered = gathered_copies(merged[None], ("kv", "tp"), 0)
    kv_count = lax.axis_size("kv")
    tp_count = lax.axis_size("tp")
    blocks = gathered.reshape(kv_count, tp_count, seq_count, merged.shape[1])
    weight_blocks = w_mix_out.reshape(tp_count, merged.shape[1], columns)
    mixed = jnp.einsum("ktsc,tcd->ksd", blocks, weight_blocks, preferred_element_type=jnp.float32)
    mixed = mixed.reshape(kv_count * seq_count, columns)
    after_mix = (after_own.astype(jnp.float32) + mixed).astype(jnp.bfloat16)
    normed_two = spread_norm(after_mix, ffn_gain_two)
    summed_two = sent_and_summed(
        mlp_term(normed_two, w_gate_two, w_up_two, w_down_two).astype(jnp.bfloat16), ("kv", "tp"), 1
    )
    output_rows = (after_mix.astype(jnp.float32) + 0.5 * summed_two).astype(jnp.bfloat16)
    return (output_rows, new_state)


def solution(mesh):
    return jax.shard_map(
        shards,
        mesh=mesh,
        in_specs=(
            P("dp", ("kv", "tp")),
            P(("dp", "kv"), "tp", None, None),
            P("tp", None),
            P(),
            P(None, ("kv", "tp")),
            P(None, ("kv", "tp")),
            P(("kv", "tp"), None),
            P(),
            P(None, "tp", "kv"),
            P(None, "tp", "kv"),
            P(None, "tp", "kv"),
            P(None, "tp", "kv"),
            P("tp", None),
            P(None, ("kv", "tp")),
            P(),
            P(None, ("kv", "tp")),
            P(None, ("kv", "tp")),
            P(("kv", "tp"), None),
        ),
        out_specs=(P("dp", ("kv", "tp")), P(("dp", "kv"), "tp", None, None)),
        check_vma=False,
    )
```

profile of v0, /device:TPU:1, one launch (start us, length us, event | category | flops | bytes accessed | tf_op | source)
XLA Modules:
  0.0 173.0 jit_solution(12563263159288492009)
XLA Ops:
  0.6 0.0 copy-start
  0.6 0.0 copy-start.14
  0.7 0.0 copy-start.3
  0.7 0.8 broadcast_in_dim.8
  1.5 0.0 copy-start.5
  1.5 30.8 %all_to_all.48 = bf16[64,96,32]{1,2,0:T(8,128)(2,1)S(1)} all-to-all(bf16[64,96,32]{1,2,0:T(8,128)(2,1)S(1)} %broadcast_in_dim.8), channel_id=1, replica_groups=mesh['dp'=4,'kv'=32,'tp'=2] {'kv','tp'}, dimensions={0} | all-to-all | bytes 786432 | tf_op jit(solution)/shard_map/all_to_all | solution.py:11
  32.3 0.3 multiply_reduce_fusion.2
  32.6 0.3 fusion.7
  32.9 0.2 fusion.45
  33.2 0.0 copy-done
  33.2 0.5 convolution_convert_fusion.1
  33.8 0.0 copy-start.12
  33.8 0.3 copy.94
  34.0 23.2 %all_to_all.49 = bf16[64,96,32]{1,2,0:T(8,128)(2,1)S(1)} all-to-all(bf16[64,96,32]{1,2,0:T(8,128)(2,1)S(1)} %bitcast.75), channel_id=1, replica_groups=mesh['dp'=4,'kv'=32,'tp'=2] {'kv','tp'}, dimensions={0} | all-to-all | bytes 786432 | tf_op jit(solution)/shard_map/all_to_all | solution.py:32
  57.2 0.1 convert_reduce_fusion.1
  57.4 0.1 broadcast_in_dim.9
  57.5 23.2 %all_to_all.50 = bf16[64,96,32]{1,2,0:T(8,128)(2,1)S(1)} all-to-all(bf16[64,96,32]{1,2,0:T(8,128)(2,1)S(1)} %broadcast_in_dim.9), channel_id=1, replica_groups=mesh['dp'=4,'kv'=32,'tp'=2] {'kv','tp'}, dimensions={0} | all-to-all | bytes 786432 | tf_op jit(solution)/shard_map/all_to_all | solution.py:11
  80.6 0.3 multiply_reduce_fusion.1
  80.9 0.1 convert_element_type.152
  81.1 0.0 copy-start.8
  81.1 0.0 copy-start.9
  81.1 0.3 copy.95
  81.4 0.2 copy-done.15
  81.6 0.1 fusion.8
  81.8 0.2 copy-done.8
  82.0 0.2 convolution_convert_fusion.2
  82.2 0.2 convolution_convert_fusion.3
  82.5 0.1 copy-done.10
  82.6 0.2 convolution_convert_fusion.4
  82.8 0.2 convolution_convert_fusion.5
  83.1 0.1 copy.100
  83.2 0.7 reshape.78
  83.9 4.5 %all-to-all-start.3 = ((bf16[32,2,192]{2,1,0:T(2,128)(2,1)}), bf16[32,2,192]{2,1,0:T(2,128)(2,1)S(1)}, u32[]{:S(2)}, u32[]{:S(2)}) async-start(bf16[32,2,192]{2,1,0:T(2,128)(2,1)} %reshape.78), calls=%async_computation.3 | async-start | bytes 65536 | tf_op jit(solution)/shard_map/all_to_all | solution.py:39
  88.5 8.7 %all-to-all-done.3 = bf16[32,2,192]{2,1,0:T(2,128)(2,1)S(1)} async-done(((bf16[32,2,192]{2,1,0:T(2,128)(2,1)}), bf16[32,2,192]{2,1,0:T(2,128)(2,1)S(1)}, u32[]{:S(2)}, u32[]{:S(2)}) %all-to-all-start.3) | async-done | bytes 24608 | tf_op jit(solution)/shard_map/all_to_all | solution.py:39
  97.1 0.1 reshape.79
  97.3 0.1 fusion.44
  97.5 0.1 copy.114
  97.6 0.1 copy.115
  97.6 0.1 copy.116
  97.7 0.1 copy.110
  97.9 1.0 multiply_add_fusion
  98.9 0.0 copy-start.1
  98.9 0.0 copy-start.17
  98.9 0.8 fusion.46
  99.8 0.1 multiply_reduce_fusion.3
  99.9 0.1 fusion.41
  100.0 0.1 broadcast_in_dim.10
  100.1 23.2 %all_to_all.51 = bf16[64,1,3,1024]{3,2,1,0:T(4,128)(2,1)S(1)} all-to-all(bf16[64,1,3,1024]{3,2,1,0:T(4,128)(2,1)S(1)} %broadcast_in_dim.10), channel_id=1, replica_groups=mesh['dp'=4,'kv'=32,'tp'=2] {'kv','tp'}, dimensions={0} | all-to-all | bytes 786432 | tf_op jit(solution)/shard_map/all_to_all | solution.py:11
  123.3 0.3 copy.113
  123.7 0.0 copy-start.16
  123.7 0.2 fusion.3
  123.9 0.0 copy-start.4
  124.0 0.1 broadcast_in_dim.11
  124.0 0.0 copy-start.6
  124.0 0.0 copy-start.7
  124.1 23.3 %all_to_all.52 = bf16[64,96,32]{1,2,0:T(8,128)(2,1)S(1)} all-to-all(bf16[64,96,32]{1,2,0:T(8,128)(2,1)S(1)} %broadcast_in_dim.11), channel_id=1, replica_groups=mesh['dp'=4,'kv'=32,'tp'=2] {'kv','tp'}, dimensions={0} | all-to-all | bytes 786432 | tf_op jit(solution)/shard_map/all_to_all | solution.py:11
  147.4 0.3 multiply_reduce_fusion
  147.7 0.3 fusion.5
  148.0 0.2 fusion.47
  148.3 0.5 convolution_convert_fusion
  148.8 0.3 copy.109
  149.1 23.2 %all_to_all.53 = bf16[64,96,32]{1,2,0:T(8,128)(2,1)S(1)} all-to-all(bf16[64,96,32]{1,2,0:T(8,128)(2,1)S(1)} %bitcast.77), channel_id=1, replica_groups=mesh['dp'=4,'kv'=32,'tp'=2] {'kv','tp'}, dimensions={0} | all-to-all | bytes 786432 | tf_op jit(solution)/shard_map/all_to_all | solution.py:32
  172.3 0.1 convert_reduce_fusion
  172.4 0.6 add_convert_fusion
  (32 shorter events, 0.2 us)
Async XLA Ops:
  0.6 32.6 %copy-start = (bf16[88,2048]{1,0:T(8,128)(2,1)S(1)}, bf16[88,2048]{1,0:T(8,128)(2,1)}, u32[]{:S(2)}) copy-start(bf16[88,2048]{1,0:T(8,128)(2,1)} %param.24) | copy-start | bytes 1081348
  0.6 31.9 %copy-start.14 = (f32[2048]{0:T(1024)S(1)}, f32[2048]{0:T(1024)}, u32[]{:S(2)}) copy-start(f32[2048]{0:T(1024)} %param.21) | copy-start | bytes 24580
  0.7 32.3 %copy-start.3 = (bf16[2048,88]{0,1:T(8,128)(2,1)S(1)}, bf16[2048,88]{0,1:T(8,128)(2,1)}, u32[]{:S(2)}) copy-start(bf16[2048,88]{0,1:T(8,128)(2,1)} %param.22) | copy-start | bytes 1081348
  1.5 31.7 %copy-start.5 = (bf16[2048,88]{0,1:T(8,128)(2,1)S(1)}, bf16[2048,88]{0,1:T(8,128)(2,1)}, u32[]{:S(2)}) copy-start(bf16[2048,88]{0,1:T(8,128)(2,1)} %param.23) | copy-start | bytes 1081348
  33.8 23.6 %copy-start.12 = (bf16[96,32]{0,1:T(8,128)(2,1)S(1)}, bf16[96,32]{0,1:T(8,128)(2,1)}, u32[]{:S(2)}) copy-start(bf16[96,32]{0,1:T(8,128)(2,1)} %param.18) | copy-start | bytes 18436
  80.9 0.7 copy-start.15
  81.1 0.9 copy-start.8
  81.1 1.1 copy-start.9
  81.6 0.9 copy-start.10
  81.6 1.2 copy-start.11
  81.6 6.8 %copy-start.13 = (f32[8,128]{1,0:T(8,128)S(1)}, f32[8,128]{1,0:T(8,128)}, u32[]{:S(2)}) copy-start(f32[8,128]{1,0:T(8,128)} %param.20) | copy-start | bytes 12292
  82.6 15.3 %copy-start.2 = (f32[3,8,128,128]{3,2,1,0:T(8,128)S(1)}, f32[3,8,128,128]{3,2,1,0:T(8,128)}, u32[]{:S(2)}) copy-start(f32[3,8,128,128]{3,2,1,0:T(8,128)} %param.19) | copy-start | bytes 4718596
  83.9 13.2 %all-to-all-start.3 = ((bf16[32,2,192]{2,1,0:T(2,128)(2,1)}), bf16[32,2,192]{2,1,0:T(2,128)(2,1)S(1)}, u32[]{:S(2)}, u32[]{:S(2)}) async-start(bf16[32,2,192]{2,1,0:T(2,128)(2,1)} %reshape.78), calls=%async_computation.3 | async-start | bytes 65536 | tf_op jit(solution)/shard_map/all_to_all | solution.py:39
  98.9 24.4 %copy-start.1 = (f32[3,8,128,128]{3,2,1,0:T(8,128)}, f32[3,8,128,128]{3,2,1,0:T(8,128)S(1)}, u32[]{:S(2)}) copy-start(f32[3,8,128,128]{3,2,1,0:T(8,128)S(1)} %multiply_add_fusion) | copy-start | bytes 4718596
  98.9 0.9 copy-start.17
  99.8 23.9 %copy-start.18 = (bf16[2048,32]{0,1:T(8,128)(2,1)S(1)}, bf16[2048,32]{0,1:T(8,128)(2,1)}, u32[]{:S(2)}) copy-start(bf16[2048,32]{0,1:T(8,128)(2,1)} %param.31) | copy-start | bytes 393220
  123.7 24.0 %copy-start.16 = (f32[2048]{0:T(1024)S(1)}, f32[2048]{0:T(1024)}, u32[]{:S(2)}) copy-start(f32[2048]{0:T(1024)} %param.32) | copy-start | bytes 24580
  123.9 24.1 %copy-start.4 = (bf16[2048,88]{0,1:T(8,128)(2,1)S(1)}, bf16[2048,88]{0,1:T(8,128)(2,1)}, u32[]{:S(2)}) copy-start(bf16[2048,88]{0,1:T(8,128)(2,1)} %param.33) | copy-start | bytes 1081348
  124.0 24.2 %copy-start.6 = (bf16[88,2048]{1,0:T(8,128)(2,1)S(1)}, bf16[88,2048]{1,0:T(8,128)(2,1)}, u32[]{:S(2)}) copy-start(bf16[88,2048]{1,0:T(8,128)(2,1)} %param.35) | copy-start | bytes 1081348
  124.0 24.2 %copy-start.7 = (bf16[2048,88]{0,1:T(8,128)(2,1)S(1)}, bf16[2048,88]{0,1:T(8,128)(2,1)}, u32[]{:S(2)}) copy-start(bf16[2048,88]{0,1:T(8,128)(2,1)} %param.34) | copy-start | bytes 1081348
where the time goes:
time: 173 us
  blocking collectives  147 us (85%)
  waiting for transfers between devices  8.68 us (5%)
  local copies, waits for them, and re-layouts  4.5 us (3%)
  starting transfers between devices  4.49 us (3%)
  other arithmetic  3.93 us (2%)
  matrix products  3.59 us (2%)
    all_to_all x4, blocking collectives, copy_for_each(): return lax.all_to_all(copies, axis, split_axis=0, concat_axis=0, tiled=True)  100 us
    all_to_all x2, blocking collectives, sent_and_summed(): lax.all_to_all(tiles, axis, split_axis=0, concat_axis=0, tiled=True)  46.3 us
    all_to_all x1, waiting for transfers between devices, sent_together(): lax.all_to_all(both, axis, split_axis=split_dim, concat_axis=concat_dim,...  8.68 us
    all_to_all x1, starting transfers between devices, sent_together(): lax.all_to_all(both, axis, split_axis=split_dim, concat_axis=concat_dim,...  4.49 us
  transfers between devices with their start and end apart: 1, of which 1 were waited for; matrix products, arithmetic and copies ran while one was open for 0% of the time, Pallas kernels for 0%

commit v1 on v0

--- a/solution.py
+++ b/solution.py
@@ -11,25 +11,32 @@
     return lax.all_to_all(copies, axis, split_axis=0, concat_axis=0, tiled=True)
 
 
-def in_order(tiles, dim):
-    tiles = jnp.moveaxis(tiles, 0, dim)
-    lengths = tiles.shape
-    return tiles.reshape(*lengths[:dim], lengths[dim] * lengths[dim + 1], *lengths[dim + 2 :])
+def swap_cores(x):
+    return lax.ppermute(x, "tp", [(0, 1), (1, 0)])
 
 
-def gathered_copies(x, axis, dim):
-    tiles = copy_for_each(x, axis)
-    return in_order(tiles, dim)
+def pair_of_cores(own, other, dim):
+    first = lax.axis_index("tp") == 0
+    return jnp.stack([jnp.where(first, own, other), jnp.where(first, other, own)], axis=dim)
 
 
-def in_blocks(x, dim, devices):
-    before, after = (x.shape[:dim], x.shape[dim + 1 :])
-    return jnp.moveaxis(x.reshape(*before, devices, -1, *after), dim, 0)
+def gathered_columns(x):
+    own = copy_for_each(x, "kv")
+    tiles = pair_of_cores(own, swap_cores(own), 1)
+    return jnp.moveaxis(tiles, 2, 0).reshape(x.shape[0], -1)
 
 
-def sent_and_summed(x, axis, dim):
-    tiles = in_blocks(x, dim, lax.axis_size(axis))
-    arrived = lax.all_to_all(tiles, axis, split_axis=0, concat_axis=0, tiled=True)
+def sent_and_summed(partial):
+    rows = partial.shape[0]
+    kv_count, tp_count = (lax.axis_size("kv"), lax.axis_size("tp"))
+    blocks = partial.reshape(rows, kv_count, tp_count, -1)
+    first = lax.axis_index("tp") == 0
+    own = jnp.where(first, blocks[:, :, 0], blocks[:, :, 1])
+    other = jnp.where(first, blocks[:, :, 1], blocks[:, :, 0])
+    from_other = swap_cores(other.astype(jnp.bfloat16))
+    both = (own + from_other.astype(jnp.float32)).astype(jnp.bfloat16)
+    tiles = jnp.moveaxis(both, 1, 0)
+    arrived = lax.all_to_all(tiles, "kv", split_axis=0, concat_axis=0, tiled=True)
     return arrived.astype(jnp.float32).sum(axis=0)
 
 
@@ -47,7 +54,7 @@
 
 
 def spread_norm(shard_in, gain_vec):
-    full_rows = gathered_copies(shard_in, ("kv", "tp"), 1)
+    full_rows = gathered_columns(shard_in)
     return local_norm(full_rows, gain_vec)
 
 
@@ -86,9 +93,9 @@
     columns = hidden_in.shape[1]
     normed_one = spread_norm(hidden_in, ffn_gain_one)
     ffn_term = mlp_term(normed_one, w_gate_one, w_up_one, w_down_one)
-    summed_one = sent_and_summed(ffn_term.astype(jnp.bfloat16), ("kv", "tp"), 1)
+    summed_one = sent_and_summed(ffn_term)
     after_own = (hidden_in.astype(jnp.float32) + 0.5 * summed_one).astype(jnp.bfloat16)
-    after_rows = gathered_copies(after_own, ("kv", "tp"), 1)
+    after_rows = gathered_columns(after_own)
     normed_mix = local_norm(after_rows, mix_gain)
     projected = (
         project(normed_mix, w_query),
@@ -112,18 +119,13 @@
     gated = readout * head_scale * head_gain[None] * jax.nn.silu(out_gate.astype(jnp.float32))
     seq_count = gated.shape[0]
     merged = gated.reshape(seq_count, -1).astype(jnp.bfloat16)
-    gathered = gathered_copies(merged[None], ("kv", "tp"), 0)
-    kv_count = lax.axis_size("kv")
-    tp_count = lax.axis_size("tp")
-    blocks = gathered.reshape(kv_count, tp_count, seq_count, merged.shape[1])
-    weight_blocks = w_mix_out.reshape(tp_count, merged.shape[1], columns)
-    mixed = jnp.einsum("ktsc,tcd->ksd", blocks, weight_blocks, preferred_element_type=jnp.float32)
-    mixed = mixed.reshape(kv_count * seq_count, columns)
+    own_heads = copy_for_each(merged, "kv").reshape(-1, merged.shape[1])
+    heads = pair_of_cores(own_heads, swap_cores(own_heads), 1)
+    weight_blocks = w_mix_out.reshape(lax.axis_size("tp"), merged.shape[1], columns)
+    mixed = jnp.einsum("rtc,tcd->rd", heads, weight_blocks, preferred_element_type=jnp.float32)
     after_mix = (after_own.astype(jnp.float32) + mixed).astype(jnp.bfloat16)
     normed_two = spread_norm(after_mix, ffn_gain_two)
-    summed_two = sent_and_summed(
-        mlp_term(normed_two, w_gate_two, w_up_two, w_down_two).astype(jnp.bfloat16), ("kv", "tp"), 1
-    )
+    summed_two = sent_and_summed(mlp_term(normed_two, w_gate_two, w_up_two, w_down_two))
     output_rows = (after_mix.astype(jnp.float32) + 0.5 * summed_two).astype(jnp.bfloat16)
     return (output_rows, new_state)
 

time: 173 us -> 144 us (0.83)
  blocking collectives: 147 us -> 96.5 us
  starting transfers between devices: 4.49 us -> 16.4 us
  waiting for transfers between devices: 8.68 us -> 15.6 us
    all_to_all x4, blocking collectives: 100 us -> 66.5 us  [copy_for_each(): return lax.all_to_all(copies, axis, split_axis=0, concat_axis=0, tiled=True)]
    all_to_all x2, blocking collectives: 46.3 us -> 30 us  [sent_and_summed(): lax.all_to_all(tiles, 'kv', split_axis=0, concat_axis=0, tiled=True)]
    ppermute x0 -> x6, starting transfers between devices: none -> 12.5 us  [swap_cores(): return lax.ppermute(x, 'tp', [(0, 1), (1, 0)])]
    ppermute x0 -> x6, waiting for transfers between devices: none -> 6.89 us  [swap_cores(): return lax.ppermute(x, 'tp', [(0, 1), (1, 0)])]
  transfers between devices with their start and end apart: 1 -> 7, of which waited for: 1 -> 7; matrix products, arithmetic and copies ran while one was open for 0% -> 0% of each run, Pallas kernels for 0% -> 0%
where the time goes in v1:
time: 144 us; the launch traced here: 143 us
  blocking collectives  96.5 us (67%)
  starting transfers between devices  16.4 us (11%)
  waiting for transfers between devices  15.6 us (11%)
  local copies, waits for them, and re-layouts  5.46 us (4%)
  other arithmetic  4.61 us (3%)
  matrix products  3.52 us (2%)
    all_to_all x4, blocking collectives, copy_for_each(): return lax.all_to_all(copies, axis, split_axis=0, concat_axis=0, tiled=True)  66.5 us
    all_to_all x2, blocking collectives, sent_and_summed(): lax.all_to_all(tiles, 'kv', split_axis=0, concat_axis=0, tiled=True)  30 us
    ppermute x6, starting transfers between devices, swap_cores(): return lax.ppermute(x, 'tp', [(0, 1), (1, 0)])  12.5 us
    all_to_all x1, waiting for transfers between devices, sent_together(): lax.all_to_all(both, axis, split_axis=split_dim, concat_axis=concat_dim,...  8.69 us
    ppermute x6, waiting for transfers between devices, swap_cores(): return lax.ppermute(x, 'tp', [(0, 1), (1, 0)])  6.89 us
    all_to_all x1, starting transfers between devices, sent_together(): lax.all_to_all(both, axis, split_axis=split_dim, concat_axis=concat_dim,...  3.85 us
    unnamed x44, local copies, waits for them, and re-layouts  3.43 us
  transfers between devices with their start and end apart: 7, of which 7 were waited for; matrix products, arithmetic and copies ran while one was open for 0% of the time, Pallas kernels for 0%

profile of v1, /device:TPU:1, one launch (start us, length us, event | category | flops | bytes accessed | tf_op | source)
XLA Modules:
  0.0 143.1 jit_solution(8889357689644710936)
XLA Ops:
  0.6 0.8 broadcast_in_dim.8
  1.4 23.1 %all_to_all.48 = bf16[32,96,32]{1,2,0:T(8,128)(2,1)S(1)} all-to-all(bf16[32,96,32]{1,2,0:T(8,128)(2,1)S(1)} %broadcast_in_dim.8), channel_id=1, replica_groups=mesh['dp'=4,'kv'=32,'tp'=2] {'kv'}, dimensions={0} | all-to-all | bytes 393216 | tf_op jit(solution)/shard_map/all_to_all | solution.py:11
  24.6 2.5 %collective-permute-start = (bf16[32,96,32]{1,2,0:T(8,128)(2,1)S(1)}, bf16[32,96,32]{1,2,0:T(8,128)(2,1)S(1)}, u32[]{:S(2)}, u32[]{:S(2)}) collective-permute-start(bf16[32,96,32]{1,2,0:T(8,128)(2,1)S(1)} %all_to_all.48), channel_id=1, source_target_pairs={{0,1},{1,0},{2,3},{3,2},{4,5},{5,4},{6,7},{7,6},{8,9},{9,8},{10,11... | collective-permute-start | bytes 589832 | tf_op jit(solution)/shard_map/ppermute | solution.py:15
  27.0 1.2 collective-permute-done
  28.2 0.3 fusion.6
  28.5 0.2 convert_bitcast_fusion.1
  28.8 0.4 copy-done.14
  29.2 0.3 fusion.11
  29.6 0.1 copy-done.6
  29.7 0.2 fusion.60
  29.9 0.3 copy-done.3
  30.2 0.5 fusion.3
  30.8 0.5 collective-permute-start.1
  31.3 1.2 collective-permute-done.1
  32.4 0.1 fusion.22
  32.5 15.1 %all_to_all.49 = bf16[32,96,32]{1,2,0:T(8,128)(2,1)S(1)} all-to-all(bf16[32,96,32]{1,2,0:T(8,128)(2,1)S(1)} %fusion.22), channel_id=1, replica_groups=mesh['dp'=4,'kv'=32,'tp'=2] {'kv'}, dimensions={0} | all-to-all | bytes 393216 | tf_op jit(solution)/shard_map/all_to_all | solution.py:39
  47.8 15.1 %all_to_all.50 = bf16[32,96,32]{1,2,0:T(8,128)(2,1)S(1)} all-to-all(bf16[32,96,32]{1,2,0:T(8,128)(2,1)S(1)} %broadcast_in_dim.9), channel_id=1, replica_groups=mesh['dp'=4,'kv'=32,'tp'=2] {'kv'}, dimensions={0} | all-to-all | bytes 393216 | tf_op jit(solution)/shard_map/all_to_all | solution.py:11
  62.8 3.2 %collective-permute-start.2 = (bf16[32,96,32]{1,2,0:T(8,128)(2,1)S(1)}, bf16[32,96,32]{1,2,0:T(8,128)(2,1)S(1)}, u32[]{:S(2)}, u32[]{:S(2)}) collective-permute-start(bf16[32,96,32]{1,2,0:T(8,128)(2,1)S(1)} %all_to_all.50), channel_id=1, source_target_pairs={{0,1},{1,0},{2,3},{3,2},{4,5},{5,4},{6,7},{7,6},{8,9},{9,8},{10,11... | collective-permute-start | bytes 589832 | tf_op jit(solution)/shard_map/ppermute | solution.py:15
  66.0 1.2 collective-permute-done.2
  67.3 0.3 multiply_reduce_fusion
  67.5 0.1 maximum_convert_fusion
  67.7 0.3 copy.117
  68.1 0.2 copy-done.15
  68.2 0.1 fusion.16
  68.4 0.2 copy-done.8
  68.6 0.2 convolution_convert_fusion
  68.8 0.2 convolution_convert_fusion.1
  69.1 0.1 copy-done.10
  69.2 0.2 convolution_convert_fusion.2
  69.4 0.2 convolution_convert_fusion.3
  69.7 0.1 copy.122
  69.8 0.7 reshape.90
  70.5 3.9 %all-to-all-start.3 = ((bf16[32,2,192]{2,1,0:T(2,128)(2,1)}), bf16[32,2,192]{2,1,0:T(2,128)(2,1)S(1)}, u32[]{:S(2)}, u32[]{:S(2)}) async-start(bf16[32,2,192]{2,1,0:T(2,128)(2,1)} %reshape.90), calls=%async_computation.3 | async-start | bytes 65536 | tf_op jit(solution)/shard_map/all_to_all | solution.py:46
  74.4 8.7 %all-to-all-done.3 = bf16[32,2,192]{2,1,0:T(2,128)(2,1)S(1)} async-done(((bf16[32,2,192]{2,1,0:T(2,128)(2,1)}), bf16[32,2,192]{2,1,0:T(2,128)(2,1)S(1)}, u32[]{:S(2)}, u32[]{:S(2)}) %all-to-all-start.3) | async-done | bytes 24608 | tf_op jit(solution)/shard_map/all_to_all | solution.py:46
  83.1 0.1 reshape.91
  83.3 0.1 fusion.59
  83.5 0.1 copy.140
  83.6 0.1 copy.141
  83.7 0.1 copy.136
  83.9 1.0 multiply_add_fusion
  84.9 0.8 fusion.61
  85.7 0.1 multiply_reduce_fusion.1
  86.0 13.5 %all_to_all.51 = bf16[32,3,1024]{2,1,0:T(4,128)(2,1)S(1)} all-to-all(bf16[32,3,1024]{2,1,0:T(4,128)(2,1)S(1)} %broadcast_in_dim.10), channel_id=1, replica_groups=mesh['dp'=4,'kv'=32,'tp'=2] {'kv'}, dimensions={0} | all-to-all | bytes 393216 | tf_op jit(solution)/shard_map/all_to_all | solution.py:11
  99.5 0.2 reshape.80
  99.7 3.6 %collective-permute-start.3 = (bf16[96,1024]{1,0:T(8,128)(2,1)S(1)}, bf16[96,1024]{1,0:T(8,128)(2,1)S(1)}, u32[]{:S(2)}, u32[]{:S(2)}) collective-permute-start(bf16[96,1024]{1,0:T(8,128)(2,1)S(1)} %reshape.80), channel_id=1, source_target_pairs={{0,1},{1,0},{2,3},{3,2},{4,5},{5,4},{6,7},{7,6},{8,9},{9,8},{10,11... | collective-permute-start | bytes 589832 | tf_op jit(solution)/shard_map/ppermute | solution.py:15
  103.3 1.1 collective-permute-done.3
  104.5 0.2 fusion.5
  104.8 14.8 %all_to_all.52 = bf16[32,96,32]{1,2,0:T(8,128)(2,1)S(1)} all-to-all(bf16[32,96,32]{1,2,0:T(8,128)(2,1)S(1)} %broadcast_in_dim.11), channel_id=1, replica_groups=mesh['dp'=4,'kv'=32,'tp'=2] {'kv'}, dimensions={0} | all-to-all | bytes 393216 | tf_op jit(solution)/shard_map/all_to_all | solution.py:11
  119.5 2.3 %collective-permute-start.4 = (bf16[32,96,32]{1,2,0:T(8,128)(2,1)S(1)}, bf16[32,96,32]{1,2,0:T(8,128)(2,1)S(1)}, u32[]{:S(2)}, u32[]{:S(2)}) collective-permute-start(bf16[32,96,32]{1,2,0:T(8,128)(2,1)S(1)} %all_to_all.52), channel_id=1, source_target_pairs={{0,1},{1,0},{2,3},{3,2},{4,5},{5,4},{6,7},{7,6},{8,9},{9,8},{10,11... | collective-permute-start | bytes 589832 | tf_op jit(solution)/shard_map/ppermute | solution.py:15
  121.8 1.2 collective-permute-done.4
  123.0 0.3 fusion.7
  123.3 0.2 convert_bitcast_fusion
  123.6 0.4 copy-done.16
  124.0 0.3 fusion.9
  124.4 0.1 copy-done.7
  124.5 0.2 fusion.62
  124.7 0.3 copy-done.4
  125.0 0.1 copy-done.5
  125.1 0.5 fusion.2
  125.7 0.5 collective-permute-start.5
  126.2 1.2 collective-permute-done.5
  127.3 0.1 fusion.23
  127.5 14.9 %all_to_all.53 = bf16[32,96,32]{1,2,0:T(8,128)(2,1)S(1)} all-to-all(bf16[32,96,32]{1,2,0:T(8,128)(2,1)S(1)} %fusion.23), channel_id=1, replica_groups=mesh['dp'=4,'kv'=32,'tp'=2] {'kv'}, dimensions={0} | all-to-all | bytes 393216 | tf_op jit(solution)/shard_map/all_to_all | solution.py:39
  142.5 0.6 add_convert_fusion
  (54 shorter events, 1.1 us)
Async XLA Ops:
  0.6 29.3 %copy-start = (bf16[88,2048]{1,0:T(8,128)(2,1)S(1)}, bf16[88,2048]{1,0:T(8,128)(2,1)}, u32[]{:S(2)}) copy-start(bf16[88,2048]{1,0:T(8,128)(2,1)} %param.24) | copy-start | bytes 1081348
  24.6 3.6 %collective-permute-start = (bf16[32,96,32]{1,2,0:T(8,128)(2,1)S(1)}, bf16[32,96,32]{1,2,0:T(8,128)(2,1)S(1)}, u32[]{:S(2)}, u32[]{:S(2)}) collective-permute-start(bf16[32,96,32]{1,2,0:T(8,128)(2,1)S(1)} %all_to_all.48), channel_id=1, source_target_pairs={{0,1},{1,0},{2,3},{3,2},{4,5},{5,4},{6,7},{7,6},{8,9},{9,8},{10,11... | collective-permute-start | bytes 589832 | tf_op jit(solution)/shard_map/ppermute | solution.py:15
  28.5 0.7 copy-start.14
  28.7 1.0 copy-start.6
  29.2 1.0 copy-start.3
  30.7 17.0 %copy-start.12 = (bf16[96,32]{0,1:T(8,128)(2,1)S(1)}, bf16[96,32]{0,1:T(8,128)(2,1)}, u32[]{:S(2)}) copy-start(bf16[96,32]{0,1:T(8,128)(2,1)} %param.18) | copy-start | bytes 18436
  30.8 1.6 %collective-permute-start.1 = (bf16[96,32,32]{0,2,1:T(8,128)(2,1)S(1)}, bf16[96,32,32]{0,2,1:T(8,128)(2,1)S(1)}, u32[]{:S(2)}, u32[]{:S(2)}) collective-permute-start(bf16[96,32,32]{0,2,1:T(8,128)(2,1)S(1)} %fusion.20), channel_id=1, source_target_pairs={{0,1},{1,0},{2,3},{3,2},{4,5},{5,4},{6,7},{7,6},{8,9},{9,8},{10,11... | collective-permute-start | bytes 589832 | tf_op jit(solution)/shard_map/ppermute | solution.py:15
  62.8 4.4 %collective-permute-start.2 = (bf16[32,96,32]{1,2,0:T(8,128)(2,1)S(1)}, bf16[32,96,32]{1,2,0:T(8,128)(2,1)S(1)}, u32[]{:S(2)}, u32[]{:S(2)}) collective-permute-start(bf16[32,96,32]{1,2,0:T(8,128)(2,1)S(1)} %all_to_all.50), channel_id=1, source_target_pairs={{0,1},{1,0},{2,3},{3,2},{4,5},{5,4},{6,7},{7,6},{8,9},{9,8},{10,11... | collective-permute-start | bytes 589832 | tf_op jit(solution)/shard_map/ppermute | solution.py:15
  67.5 0.7 copy-start.15
  67.7 0.9 copy-start.8
  67.7 1.1 copy-start.9
  68.2 0.9 copy-start.10
  68.2 1.2 copy-start.11
  68.2 6.2 %copy-start.13 = (f32[8,128]{1,0:T(8,128)S(1)}, f32[8,128]{1,0:T(8,128)}, u32[]{:S(2)}) copy-start(f32[8,128]{1,0:T(8,128)} %param.20) | copy-start | bytes 12292
  69.2 14.7 %copy-start.2 = (f32[3,8,128,128]{3,2,1,0:T(8,128)S(1)}, f32[3,8,128,128]{3,2,1,0:T(8,128)}, u32[]{:S(2)}) copy-start(f32[3,8,128,128]{3,2,1,0:T(8,128)} %param.19) | copy-start | bytes 4718596
  70.5 12.6 %all-to-all-start.3 = ((bf16[32,2,192]{2,1,0:T(2,128)(2,1)}), bf16[32,2,192]{2,1,0:T(2,128)(2,1)S(1)}, u32[]{:S(2)}, u32[]{:S(2)}) async-start(bf16[32,2,192]{2,1,0:T(2,128)(2,1)} %reshape.90), calls=%async_computation.3 | async-start | bytes 65536 | tf_op jit(solution)/shard_map/all_to_all | solution.py:46
  84.9 19.6 %copy-start.1 = (f32[3,8,128,128]{3,2,1,0:T(8,128)}, f32[3,8,128,128]{3,2,1,0:T(8,128)S(1)}, u32[]{:S(2)}) copy-start(f32[3,8,128,128]{3,2,1,0:T(8,128)S(1)} %multiply_add_fusion) | copy-start | bytes 4718596
  84.9 1.0 copy-start.17
  84.9 19.5 %copy-start.18 = (bf16[2048,32]{0,1:T(8,128)(2,1)S(1)}, bf16[2048,32]{0,1:T(8,128)(2,1)}, u32[]{:S(2)}) copy-start(bf16[2048,32]{0,1:T(8,128)(2,1)} %param.31) | copy-start | bytes 393220
  99.7 4.7 %collective-permute-start.3 = (bf16[96,1024]{1,0:T(8,128)(2,1)S(1)}, bf16[96,1024]{1,0:T(8,128)(2,1)S(1)}, u32[]{:S(2)}, u32[]{:S(2)}) collective-permute-start(bf16[96,1024]{1,0:T(8,128)(2,1)S(1)} %reshape.80), channel_id=1, source_target_pairs={{0,1},{1,0},{2,3},{3,2},{4,5},{5,4},{6,7},{7,6},{8,9},{9,8},{10,11... | collective-permute-start | bytes 589832 | tf_op jit(solution)/shard_map/ppermute | solution.py:15
  119.5 3.5 %collective-permute-start.4 = (bf16[32,96,32]{1,2,0:T(8,128)(2,1)S(1)}, bf16[32,96,32]{1,2,0:T(8,128)(2,1)S(1)}, u32[]{:S(2)}, u32[]{:S(2)}) collective-permute-start(bf16[32,96,32]{1,2,0:T(8,128)(2,1)S(1)} %all_to_all.52), channel_id=1, source_target_pairs={{0,1},{1,0},{2,3},{3,2},{4,5},{5,4},{6,7},{7,6},{8,9},{9,8},{10,11... | collective-permute-start | bytes 589832 | tf_op jit(solution)/shard_map/ppermute | solution.py:15
  123.3 0.7 copy-start.16
  123.5 1.0 copy-start.7
  124.0 1.0 copy-start.4
  124.0 1.1 copy-start.5
  125.7 1.6 %collective-permute-start.5 = (bf16[96,32,32]{0,2,1:T(8,128)(2,1)S(1)}, bf16[96,32,32]{0,2,1:T(8,128)(2,1)S(1)}, u32[]{:S(2)}, u32[]{:S(2)}) collective-permute-start(bf16[96,32,32]{0,2,1:T(8,128)(2,1)S(1)} %fusion.21), channel_id=1, source_target_pairs={{0,1},{1,0},{2,3},{3,2},{4,5},{5,4},{6,7},{7,6},{8,9},{9,8},{10,11... | collective-permute-start | bytes 589832 | tf_op jit(solution)/shard_map/ppermute | solution.py:15

commit v2 on v1

v2 whole, which is shorter than its diff:
```python
import jax
import jax.numpy as jnp
from jax import lax
from jax.experimental import pallas as pl
from jax.experimental.pallas import tpu as pltpu
from jax.sharding import PartitionSpec as P

EPS = 1e-06
LANES = 128
Z_COUNT, Y_COUNT, TP_COUNT = 8, 4, 2
KV_COUNT = Z_COUNT * Y_COUNT
NN, NT = ((1,), (0,)), ((1,), (1,))


def bf(x):
    return x.astype(jnp.bfloat16)


def f32(x):
    return x.astype(jnp.float32)


def matmul(a, b, dims):
    return lax.dot_general(a, b, (dims, ((), ())), preferred_element_type=jnp.float32)


def exchange(tiles, axis, groups=None):
    return lax.all_to_all(
        tiles, axis, split_axis=0, concat_axis=0, axis_index_groups=groups, tiled=True
    )


def copies(x, count):
    return jnp.broadcast_to(x, (count, *x.shape))


def swap_cores(x):
    return lax.ppermute(x, "tp", [(0, 1), (1, 0)])


def shift_y(x, step):
    pairs = [
        (z * Y_COUNT + y, z * Y_COUNT + (y + step) % Y_COUNT)
        for z in range(Z_COUNT)
        for y in range(Y_COUNT)
    ]
    return lax.ppermute(x, "kv", pairs)


def slab_exchange(x):
    groups = [
        [(z * Y_COUNT + y) * TP_COUNT + t for z in range(Z_COUNT) for t in range(TP_COUNT)]
        for y in range(Y_COUNT)
    ]
    return exchange(copies(x, Z_COUNT * TP_COUNT), ("kv", "tp"), groups)


def place():
    kv = lax.axis_index("kv")
    return lax.div(kv, Y_COUNT), lax.rem(kv, Y_COUNT), lax.axis_index("tp")


def iota(shape, axis):
    return lax.broadcasted_iota(jnp.int32, shape, axis)


def hot(mask):
    return jnp.where(mask, 1.0, 0.0).astype(jnp.bfloat16)


def local(body, outs, *args, scratch=(), outside=(), vmem=False, flops=1 << 20):
    kind = pltpu.VMEM if vmem else jax.ShapeDtypeStruct
    shapes = [kind(s, d) for s, d in outs]
    held = pl.BlockSpec(memory_space=pltpu.VMEM)
    specs = [pl.BlockSpec(memory_space=pl.ANY) if k in outside else held for k in range(len(args))]
    args = [
        pltpu.with_memory_space_constraint(a, pltpu.HBM) if k in outside else a
        for k, a in enumerate(args)
    ]
    size = sum(a.size * a.dtype.itemsize for a in args)
    return pl.pallas_call(
        body,
        out_shape=shapes,
        in_specs=specs,
        out_specs=[held] * len(outs),
        scratch_shapes=list(scratch),
        compiler_params=pltpu.CompilerParams(vmem_limit_bytes=VMEM_LIMIT),
        cost_estimate=pl.CostEstimate(flops=flops, bytes_accessed=size, transcendentals=0),
    )(*args)


VMEM_LIMIT = 24 * 1024 * 1024


def first_block(
    own, other, gain, w_gate, w_up, w_down, mine, theirs, slab, xt, low, gate_w, up_w, down_w, sems
):
    z, y, core = place()
    moves = [
        pltpu.make_async_copy(src, dst, sems.at[k])
        for k, (src, dst) in enumerate(((w_gate, gate_w), (w_up, up_w), (w_down, down_w)))
    ]
    for move in moves:
        move.start()
    cols = own.shape[1]
    for kv in range(KV_COUNT):
        base = kv * TP_COUNT * cols
        xt[pl.ds(pl.multiple_of(base + core * cols, cols), cols), :] = own[kv]
        xt[pl.ds(pl.multiple_of(base + (1 - core) * cols, cols), cols), :] = other[kv]
    width, rows = xt.shape
    square = jnp.zeros((8, rows), jnp.float32)
    for c in range(width // LANES):
        part = f32(xt[c * LANES : (c + 1) * LANES, :])
        square += (part * part).reshape(LANES // 8, 8, rows).sum(axis=0)
    scale = lax.rsqrt(square.sum(axis=0, keepdims=True) * (1.0 / width) + EPS)
    gains = gain[...].T
    normed = []
    for c in range(width // LANES):
        part = f32(xt[c * LANES : (c + 1) * LANES, :])
        normed.append(bf(part * scale * gains[:, c : c + 1]))
    normed = jnp.concatenate(normed, axis=0)
    moves[0].wait()
    gate = matmul(gate_w[...], normed, NN)
    moves[1].wait()
    upper = matmul(up_w[...], normed, NN)
    mid = bf(jax.nn.silu(gate) * upper)
    count = slab.shape[0]
    seqs = count // Z_COUNT
    new, old = iota((rows, rows), 0), iota((rows, rows), 1)
    wanted = (
        lax.div(lax.rem(new, count), seqs) * (Y_COUNT * seqs)
        + lax.div(new, count) * seqs
        + lax.rem(new, seqs)
    )
    mid = bf(matmul(hot(old == wanted), mid, NT))
    moves[2].wait()
    low[...] = matmul(mid, down_w[...], NN)
    for k in range(Z_COUNT):
        at = pl.multiple_of((k * TP_COUNT + core) * LANES, LANES)
        to = pl.multiple_of((k * TP_COUNT + 1 - core) * LANES, LANES)
        mine[k] = low[:, pl.ds(at, LANES)]
        theirs[k] = bf(low[:, pl.ds(to, LANES)])
    at = pl.multiple_of((z * TP_COUNT + core) * LANES, LANES)
    new, old = iota((count, rows), 0), iota((count, rows), 1)
    pick = hot(old == lax.div(new, seqs) * (Y_COUNT * seqs) + y * seqs + lax.rem(new, seqs))
    slab[...] = matmul(pick, xt[pl.ds(at, LANES), :], NT)


def load_mix(a0, a1, a2, a3, w_mix, sems):
    _, y, _ = place()
    moves = []
    for k, part in enumerate((a0, a1, a2, a3)):
        to = lax.rem(y - k + Y_COUNT, Y_COUNT)
        moves.append(
            pltpu.make_async_copy(
                part.at[pl.ds(LANES, w_mix.shape[1])], w_mix.at[to], sems.at[k]
            )
        )
    for move in moves:
        move.start()
    for move in moves:
        move.wait()


def load_state(state, held, sem):
    move = pltpu.make_async_copy(state, held, sem)
    move.start()
    move.wait()


def load_parts(*refs):
    *parts, held, sems = refs
    moves = [
        pltpu.make_async_copy(part.at[pl.ds(0, held.shape[1])], held.at[k], sems.at[k])
        for k, part in enumerate(parts)
    ]
    for move in moves:
        move.start()
    for move in moves:
        move.wait()


def flipped(x, out):
    out[...] = x[...].T


def assemble(tiles, rows):
    count = tiles.shape[0]
    for k in range(count):
        rows[:, k * LANES : (k + 1) * LANES] = tiles[k]


def normed_of(rows, gain):
    values = f32(rows[...])
    scale = lax.rsqrt(jnp.mean(values * values, axis=1, keepdims=True) + EPS)
    return bf(values * scale * gain[...])


def projections(tiles, gain, w_held, a3, channels, residual, rows, weights, sems):
    z, y, core = place()
    last = pltpu.make_async_copy(a3.at[pl.ds(0, LANES)], weights, sems.at[0])
    last.start()
    assemble(tiles, rows)
    normed = normed_of(rows, gain)
    flats = []
    for k in range(Y_COUNT - 1):
        flats.append(bf(matmul(normed, w_held[k], NT)))
    last.wait()
    flats.append(bf(matmul(normed, weights[...], NT)))
    count = rows.shape[0]
    seqs = count // Z_COUNT
    stacked = jnp.concatenate(flats, axis=0)
    shape = (Z_COUNT * 16, Y_COUNT * count)
    new, old = iota(shape, 0), iota(shape, 1)
    row = lax.div(new, 16) * seqs + lax.div(lax.rem(new, 16), Y_COUNT)
    wanted = lax.rem(y - lax.rem(new, Y_COUNT) + Y_COUNT, Y_COUNT) * count + row
    real = lax.div(lax.rem(new, 16), Y_COUNT) < seqs
    channels[...] = bf(matmul(hot((old == wanted) & real), stacked, NN))
    at = pl.multiple_of(z * TP_COUNT * LANES, 2 * LANES)
    both = rows[:, pl.ds(at, TP_COUNT * LANES)]
    shape = (TP_COUNT * LANES, LANES)
    old, new = iota(shape, 0), iota(shape, 1)
    each = LANES // Y_COUNT
    wanted = lax.div(new, each) * (TP_COUNT * each) + core * each + lax.rem(new, each)
    residual[...] = matmul(both, hot(old == wanted), NN)


def channel_views(arrived, k):
    per = LANES // KV_COUNT
    shape = (LANES, Z_COUNT * 16)
    channel, source = iota(shape, 0), iota(shape, 1)
    kv = lax.div(channel, per)
    wanted = lax.div(kv, Y_COUNT) * 16 + k * Y_COUNT + lax.rem(kv, Y_COUNT)
    wide = matmul(hot(source == wanted), arrived, NN)
    shape = (LANES, LANES)
    own = lax.rem(iota(shape, 0), per) == lax.rem(iota(shape, 1), per)
    wide = bf(jnp.where(own, wide, 0.0))
    shape = (LANES, KV_COUNT)
    gather = hot(lax.div(iota(shape, 0), per) == iota(shape, 1))
    shape = (KV_COUNT, LANES)
    gather_rows = hot(lax.div(iota(shape, 1), per) == iota(shape, 0))
    return matmul(wide, gather, NN), matmul(gather_rows, wide, NT)


def read_state(arrived, floor_rows, floor_t, gain, state, merged, vectors):
    seqs, heads = state.shape[:2]
    floor = floor_t[...]
    for k in range(seqs):
        columns, lines = channel_views(arrived[...], k)
        query = columns[:, :heads]
        raw = columns[:, heads : 2 * heads]
        forget = floor + (1.0 - floor) * jax.nn.sigmoid(raw)
        keep = (1.0 - floor) * jax.nn.sigmoid(-raw)
        line = lines[2 * heads : 3 * heads]
        raw = lines[heads : 2 * heads]
        low = floor_rows[...]
        vectors[k, :heads] = low + (1.0 - low) * jax.nn.sigmoid(raw)
        vectors[k, heads : 2 * heads] = (1.0 - low) * jax.nn.sigmoid(-raw)
        vectors[k, 2 * heads :] = line
        weight = query * forget
        added = jnp.sum(query * keep, axis=0, keepdims=True)
        outs = []
        for h in range(heads):
            term = weight[:, h : h + 1] * state[k, h]
            outs.append(
                jnp.sum(term, axis=0, keepdims=True) + added[:, h : h + 1] * line[h : h + 1]
            )
        readout = jnp.concatenate(outs, axis=0)
        scale = lax.rsqrt(jnp.mean(readout * readout, axis=1, keepdims=True) + EPS)
        gated = readout * scale * gain[...] * jax.nn.silu(lines[3 * heads : 4 * heads])
        merged[k * heads : (k + 1) * heads, :] = gated


def next_state(state, vectors, out):
    heads = out.shape[1]
    columns = vectors[0].T
    for h in range(heads):
        line = vectors[0, 2 * heads + h : 2 * heads + h + 1, :]
        out[0, h] = (
            columns[:, h : h + 1] * state[0, h] + columns[:, heads + h : heads + h + 1] * line
        )


def mix_out(tiles, w_mix, residual, after, rows):
    _, heads_rows, _ = tiles.shape
    slab_rows = rows.shape[0]
    seqs = slab_rows // Z_COUNT
    heads = heads_rows // seqs
    total = Z_COUNT * heads_rows
    shape = (total, total)
    new, old = iota(shape, 0), iota(shape, 1)
    row = lax.rem(new, slab_rows)
    wanted = (
        lax.div(row, seqs) * heads_rows + lax.rem(row, seqs) * heads + lax.div(new, slab_rows)
    )
    order = hot(old == wanted)
    for t in range(TP_COUNT):
        stacked = jnp.concatenate([tiles[z * TP_COUNT + t] for z in range(Z_COUNT)], axis=0)
        moved = bf(matmul(order, stacked, NN))
        for h in range(heads):
            at = (t * heads + h) * LANES
            rows[:, at : at + LANES] = moved[h * slab_rows : (h + 1) * slab_rows]
    weights = w_mix[...].reshape(LANES, rows.shape[1])
    after[...] = bf(residual[...] + matmul(rows[...], weights, NT))


def lane_order(transposed):
    shape = (TP_COUNT * LANES, TP_COUNT * LANES)
    each = LANES // Y_COUNT
    a, b = (0, 1) if not transposed else (1, 0)
    old, new = iota(shape, a), iota(shape, b)
    wanted = (
        lax.rem(lax.div(new, each), TP_COUNT) * LANES
        + lax.div(new, TP_COUNT * each) * each
        + lax.rem(new, each)
    )
    return hot(old == wanted)


def second_block(
    tiles, gain, after, w_held, t3, d0, d1, d2, d3, mine, theirs, rows, w_last, w_down, sems
):
    z, _, core = place()
    moves = [
        pltpu.make_async_copy(part, w_down.at[k], sems.at[k])
        for k, part in enumerate((d0, d1, d2, d3))
    ]
    last = pltpu.make_async_copy(t3, w_last, sems.at[Y_COUNT])
    last.start()
    for move in moves:
        move.start()
    order = lane_order(False)
    wide = TP_COUNT * LANES
    for k in range(Z_COUNT):
        both = jnp.concatenate([tiles[k * TP_COUNT], tiles[k * TP_COUNT + 1]], axis=1)
        rows[:, k * wide : (k + 1) * wide] = bf(matmul(both, order, NN))
    normed = normed_of(rows, gain)
    hidden = w_down.shape[1]
    mids = []
    for k in range(Y_COUNT):
        if k == Y_COUNT - 1:
            last.wait()
            w_top = w_last[...]
        else:
            w_top = w_held[k]
        tops = matmul(normed, w_top, NT)
        mids.append(bf(jax.nn.silu(tops[:, :hidden]) * tops[:, hidden:]))
    total = jnp.zeros(rows.shape, jnp.float32)
    for k, move in enumerate(moves):
        move.wait()
        total += matmul(mids[k], w_down[k], NN)
    total = bf(0.5 * total)
    back = lane_order(True)
    for k in range(Z_COUNT):
        split = matmul(total[:, k * wide : (k + 1) * wide], back, NN)
        low, high = split[:, :LANES], split[:, LANES:]
        kept = jnp.where(core == 0, low, high)
        home = jnp.where(z == k, f32(after[...]), 0.0)
        mine[k] = kept + home
        theirs[k] = bf(jnp.where(core == 0, high, low))


def finish(arrived, out):
    _, y, _ = place()
    slab_rows = arrived.shape[1]
    cols, rows = out.shape
    seqs = slab_rows // Z_COUNT
    parts = []
    for k in range(Y_COUNT):
        part = f32(arrived[k])
        for n in range(1, Z_COUNT):
            part += f32(arrived[n * Y_COUNT + k])
        parts.append(bf(part))
    result = jnp.concatenate(parts, axis=0)
    shape = (cols, LANES)
    pick = hot(iota(shape, 1) == y * cols + iota(shape, 0))
    picked = bf(matmul(pick, result, NT))
    shape = (rows, rows)
    old, new = iota(shape, 0), iota(shape, 1)
    wanted = (
        lax.rem(lax.div(new, seqs), Y_COUNT) * slab_rows
        + lax.div(new, seqs * Y_COUNT) * seqs
        + lax.rem(new, seqs)
    )
    out[...] = bf(matmul(picked, hot(old == wanted), NN))


def along_y(w):
    below, above = shift_y(w, 1), shift_y(w, -1)
    return below, above


def shards(
    hidden_in,
    state,
    forget_floor,
    ffn_gain_one,
    w_gate_one,
    w_up_one,
    w_down_one,
    mix_gain,
    w_query,
    w_forget,
    w_input,
    w_outgate,
    head_gain,
    w_mix_out,
    ffn_gain_two,
    w_gate_two,
    w_up_two,
    w_down_two,
):
    rows, own_cols = hidden_in.shape
    width, hidden = w_gate_one.shape
    seqs, heads = state.shape[:2]
    slab_rows = rows // Y_COUNT
    half16, half32 = jnp.bfloat16, jnp.float32
    dma = pltpu.SemaphoreType.DMA

    kinds = [jnp.transpose(w, (1, 2, 0)) for w in (w_query, w_forget, w_input, w_outgate)]
    early = jnp.concatenate([*(k.reshape(-1, width) for k in kinds), w_mix_out.T], axis=0)
    late_top = jnp.concatenate([w_gate_two.T, w_up_two.T], axis=0)

    (floor_t,) = local(flipped, [((LANES, heads), half32)], forget_floor)

    own = exchange(copies(hidden_in.T, KV_COUNT), "kv")
    other = swap_cores(own)
    mine, theirs, slab = local(
        first_block,
        [
            ((Z_COUNT, rows, LANES), half32),
            ((Z_COUNT, rows, LANES), half16),
            ((slab_rows, LANES), half32),
        ],
        own,
        other,
        ffn_gain_one.reshape(-1, LANES),
        w_gate_one.T,
        w_up_one.T,
        w_down_one,
        scratch=(
            pltpu.VMEM((width, rows), half16),
            pltpu.VMEM((rows, width), half32),
            pltpu.VMEM((hidden, width), half16),
            pltpu.VMEM((hidden, width), half16),
            pltpu.VMEM((hidden, width), half16),
            dma((3,)),
        ),
        outside=(3, 4, 5),
    )
    both = bf(mine + f32(swap_cores(theirs)))
    summed = exchange(both.reshape(KV_COUNT, slab_rows, LANES), "kv")
    below, above = shift_y(early, 1), shift_y(early, -1)
    twice = shift_y(below, 1)
    after_own = bf(slab + 0.5 * f32(summed).sum(axis=0))

    tops = [late_top, *along_y(late_top)]
    lows = [w_down_two, *along_y(w_down_two)]
    tops.append(shift_y(tops[1], 1))
    lows.append(shift_y(lows[2], -1))

    after_tiles = slab_exchange(after_own)
    parts = (early, below, twice, above)
    (w_held,) = local(
        load_parts,
        [((Y_COUNT - 1, LANES, width), half16)],
        *parts[:-1],
        scratch=(dma((Y_COUNT - 1,)),),
        outside=(0, 1, 2),
        vmem=True,
    )
    channels, residual = local(
        projections,
        [((Z_COUNT * 16, LANES), half16), ((slab_rows, LANES), half32)],
        after_tiles,
        mix_gain.reshape(1, -1),
        w_held,
        parts[-1],
        scratch=(
            pltpu.VMEM((slab_rows, width), half16),
            pltpu.VMEM((LANES, width), half16),
            dma((1,)),
        ),
        outside=(3,),
    )
    zgroups = [[a * Y_COUNT + b for a in range(Z_COUNT)] for b in range(Y_COUNT)]
    arrived = exchange(channels.reshape(Z_COUNT, 16, LANES), "kv", zgroups)
    (held,) = local(
        load_state,
        [(state.shape, half32)],
        state,
        scratch=(dma,),
        outside=(0,),
        vmem=True,
    )
    gated, vectors = local(
        read_state,
        [((seqs * heads, LANES), half32), ((seqs, 3 * heads, LANES), half32)],
        arrived.reshape(Z_COUNT * 16, LANES),
        forget_floor,
        floor_t,
        head_gain,
        held,
    )
    merged_tiles = slab_exchange(bf(gated))
    whole = lambda *dims: pl.BlockSpec((1, *dims), lambda k: (k, *(0 for _ in dims)))
    new_state = pl.pallas_call(
        next_state,
        grid=(seqs,),
        out_shape=jax.ShapeDtypeStruct(state.shape, half32),
        in_specs=[
            whole(*state.shape[1:]),
            whole(3 * heads, LANES),
        ],
        out_specs=whole(*state.shape[1:]),
        compiler_params=pltpu.CompilerParams(vmem_limit_bytes=VMEM_LIMIT),
        cost_estimate=pl.CostEstimate(flops=1 << 20, bytes_accessed=1 << 22, transcendentals=0),
        name="next_state",
    )(held, vectors)
    (w_mix,) = local(
        load_mix,
        [((Y_COUNT, own_cols, width), half16)],
        *parts,
        scratch=(dma((Y_COUNT,)),),
        outside=(0, 1, 2, 3),
        vmem=True,
    )
    (after_mix,) = local(
        mix_out,
        [((slab_rows, LANES), half16)],
        merged_tiles,
        w_mix,
        residual,
        scratch=(pltpu.VMEM((slab_rows, width), half16),),
    )

    mix_tiles = slab_exchange(after_mix)
    (w_held,) = local(
        load_parts,
        [((Y_COUNT - 1, 2 * hidden, width), half16)],
        *tops[:-1],
        scratch=(dma((Y_COUNT - 1,)),),
        outside=(0, 1, 2),
        vmem=True,
    )
    mine, theirs = local(
        second_block,
        [((Z_COUNT, slab_rows, LANES), half32), ((Z_COUNT, slab_rows, LANES), half16)],
        mix_tiles,
        ffn_gain_two.reshape(1, -1),
        after_mix,
        w_held,
        tops[-1],
        *lows,
        scratch=(
            pltpu.VMEM((slab_rows, width), half16),
            pltpu.VMEM((2 * hidden, width), half16),
            pltpu.VMEM((Y_COUNT, hidden, width), half16),
            dma((Y_COUNT + 1,)),
        ),
        outside=(4, 5, 6, 7, 8),
    )
    both = bf(mine + f32(swap_cores(theirs)))
    tiles = jnp.broadcast_to(both[:, None], (Z_COUNT, Y_COUNT, slab_rows, LANES))
    arrived = exchange(tiles.reshape(KV_COUNT, slab_rows, LANES), "kv")
    (result,) = local(finish, [((own_cols, rows), half16)], arrived)
    return (result.T, new_state)


def solution(mesh):
    return jax.shard_map(
        shards,
        mesh=mesh,
        in_specs=(
            P("dp", ("kv", "tp")),
            P(("dp", "kv"), "tp", None, None),
            P("tp", None),
            P(),
            P(None, ("kv", "tp")),
            P(None, ("kv", "tp")),
            P(("kv", "tp"), None),
            P(),
            P(None, "tp", "kv"),
            P(None, "tp", "kv"),
            P(None, "tp", "kv"),
            P(None, "tp", "kv"),
            P("tp", None),
            P(None, ("kv", "tp")),
            P(),
            P(None, ("kv", "tp")),
            P(None, ("kv", "tp")),
            P(("kv", "tp"), None),
        ),
        out_specs=(P("dp", ("kv", "tp")), P(("dp", "kv"), "tp", None, None)),
        check_vma=False,
    )
```

time: 144 us -> 143 us (level)
  blocking collectives: 96.5 us -> 0 us
  waiting for transfers between devices: 15.6 us -> 65.4 us
  starting transfers between devices: 16.4 us -> 46.6 us
  Pallas kernels: 0 us -> 17.7 us
  local copies, waits for them, and re-layouts: 5.46 us -> 9.23 us
  matrix products: 3.52 us -> 0 us
  other arithmetic: 4.61 us -> 1.73 us
    all_to_all x6 -> x0, blocking collectives: 96.5 us -> none  [the longest x4 66.5 us: copy_for_each(): return lax.all_to_all(copies, axis, split_axis=0, concat_axis=0, tiled=True)]
    all_to_all x1 -> x7, starting transfers between devices: 3.85 us -> 38.1 us  [exchange(): lax.all_to_all(tiles, axis, split_axis=0, concat_axis=0, axis_index_group...]
    ppermute x0 -> x9, waiting for transfers between devices: none -> 30.3 us  [shift_y(): return lax.ppermute(x, 'kv', pairs)]
    all_to_all x1 -> x7, waiting for transfers between devices: 8.69 us -> 32.7 us  [exchange(): lax.all_to_all(tiles, axis, split_axis=0, concat_axis=0, axis_index_group...]
    pallas_call x0 -> x12, Pallas kernels: none -> 17.7 us  [the longest x11 15.2 us: local(): pl.pallas_call(body, out_shape=shapes, in_specs=specs, out_specs=[held] *...]
    ppermute x6 -> x3, starting transfers between devices: 12.5 us -> 3 us  [swap_cores(): return lax.ppermute(x, 'tp', [(0, 1), (1, 0)])]
    ppermute x0 -> x9, starting transfers between devices: none -> 5.52 us  [shift_y(): return lax.ppermute(x, 'kv', pairs)]
    ppermute x6 -> x3, waiting for transfers between devices: 6.89 us -> 2.41 us  [swap_cores(): return lax.ppermute(x, 'tp', [(0, 1), (1, 0)])]
  transfers between devices with their start and end apart: 7 -> 19, of which waited for: 7 -> 12; matrix products, arithmetic and copies ran while one was open for 0% -> 4% of each run, Pallas kernels for 0% -> 10%
where the time goes in v2:
time: 143 us; the launch traced here: 142 us
  waiting for transfers between devices  65.4 us (46%)
  starting transfers between devices  46.6 us (33%)
  Pallas kernels  17.7 us (12%)
  local copies, waits for them, and re-layouts  9.23 us (6%)
  other arithmetic  1.73 us (1%)
    all_to_all x7, starting transfers between devices, exchange(): lax.all_to_all(tiles, axis, split_axis=0, concat_axis=0, axis_index_group...  38.1 us
    all_to_all x7, waiting for transfers between devices, exchange(): lax.all_to_all(tiles, axis, split_axis=0, concat_axis=0, axis_index_group...  32.7 us
    ppermute x9, waiting for transfers between devices, shift_y(): return lax.ppermute(x, 'kv', pairs)  30.3 us
    pallas_call x11, Pallas kernels, local(): pl.pallas_call(body, out_shape=shapes, in_specs=specs, out_specs=[held] *...  15.2 us
    ppermute x9, starting transfers between devices, shift_y(): return lax.ppermute(x, 'kv', pairs)  5.52 us
    broadcast_in_dim x4, local copies, waits for them, and re-layouts, copies(): return jnp.broadcast_to(x, (count, *x.shape))  3.46 us
    unnamed x36, local copies, waits for them, and re-layouts  3.1 us
    ppermute x3, starting transfers between devices, swap_cores(): return lax.ppermute(x, 'tp', [(0, 1), (1, 0)])  3 us
  transfers between devices with their start and end apart: 19, of which 12 were waited for; matrix products, arithmetic and copies ran while one was open for 4% of the time, Pallas kernels for 10%

profile of v2, /device:TPU:1, one launch (start us, length us, event | category | flops | bytes accessed | tf_op | source)
XLA Modules:
  0.0 141.7 jit_solution(13684825180796638373)
XLA Ops:
  0.7 1.5 %broadcast_in_dim.18 = bf16[32,32,96]{2,1,0:T(8,128)(2,1)} broadcast(bf16[32,96]{1,0:T(8,128)(2,1)} %bitcast.31), dimensions={1,2} | broadcast | bytes 202752 | tf_op jit(solution)/shard_map/broadcast_in_dim | solution.py:34
  2.2 12.0 %all-to-all-start = ((bf16[32,32,96]{2,1,0:T(8,128)(2,1)}), bf16[32,32,96]{2,1,0:T(8,128)(2,1)S(1)}, u32[]{:S(2)}, u32[]{:S(2)}) async-start(bf16[32,32,96]{2,1,0:T(8,128)(2,1)} %broadcast_in_dim.18), calls=%async_computation | async-start | bytes 524288 | tf_op jit(solution)/shard_map/all_to_all | solution.py:28
  14.2 0.9 reshape.41
  15.2 0.9 reshape.42
  16.1 0.0 copy-start.9
  16.1 0.0 copy-start.10
  16.3 9.2 %all-to-all-done.own = bf16[32,32,96]{2,1,0:T(8,128)(2,1)S(1)} async-done(((bf16[32,32,96]{2,1,0:T(8,128)(2,1)}), bf16[32,32,96]{2,1,0:T(8,128)(2,1)S(1)}, u32[]{:S(2)}, u32[]{:S(2)}) %all-to-all-start) | async-done | bytes 196640 | tf_op jit(solution)/shard_map/all_to_all | solution.py:28
  25.5 2.5 %collective-permute-start = (bf16[32,32,96]{2,1,0:T(8,128)(2,1)S(1)}, bf16[32,32,96]{2,1,0:T(8,128)(2,1)S(1)}, u32[]{:S(2)}, u32[]{:S(2)}) collective-permute-start(bf16[32,32,96]{2,1,0:T(8,128)(2,1)S(1)} %all-to-all-done.own), channel_id=1, source_target_pairs={{0,1},{1,0},{2,3},{3,2},{4,5},{5,4},{6,7},{7,6},{8,9},{9,8},{10,11... | collective-permute-start | bytes 589832 | tf_op jit(solution)/shard_map/ppermute | solution.py:38
  28.0 0.1 collective-permute-start.2
  28.1 1.0 collective-permute-done.other
  29.1 2.2 %shard_map.185 = (f32[8,96,128]{2,1,0:T(8,128)S(1)}, bf16[8,96,128]{2,1,0:T(8,128)(2,1)S(1)}, f32[24,128]{1,0:T(8,128)S(1)}) custom-call(bf16[32,32,96]{2,1,0:T(8,128)(2,1)S(1)} %all-to-all-done.own, bf16[32,32,96]{2,1,0:T(8,128)(2,1)S(1)} %collective-permute-done.other, f32[16,128]{1,0:T(8,128)S(1)} %bitcast.20, bf16[88,2048]{1,0:T(8,128)(2,1)} %bitcast.23, ...), custom_call_target="tpu_custom_call" | custom-call | flops 1048576 | bytes 1482752 | tf_op jit(solution)/shard_map/pallas_call | solution.py:81
  31.3 0.0 copy-start.11
  31.3 0.4 collective-permute-start.1
  31.8 0.9 pad_maximum_fusion.refs_0_
  32.7 0.0 collective-permute-start.5
  32.7 0.1 collective-permute-done.1
  32.9 0.7 add_convert_fusion
  33.6 5.1 %all-to-all-start.1 = ((bf16[32,24,128]{2,1,0:T(8,128)(2,1)}), bf16[32,24,128]{2,1,0:T(8,128)(2,1)S(1)}, u32[]{:S(2)}, u32[]{:S(2)}) async-start(bf16[32,24,128]{2,1,0:T(8,128)(2,1)} %bitcast.4), calls=%async_computation.1 | async-start | bytes 393216 | tf_op jit(solution)/shard_map/all_to_all | solution.py:28
  38.8 7.4 %collective-permute-done.2.refs_1_.a1 = bf16[160,2048]{1,0:T(8,128)(2,1)S(1)} collective-permute-done((bf16[160,2048]{1,0:T(8,128)(2,1)S(1)}, bf16[160,2048]{1,0:T(8,128)(2,1)S(1)}, u32[]{:S(2)}, u32[]{:S(2)}) %collective-permute-start.2) | collective-permute-done | bytes 655392 | tf_op jit(solution)/shard_map/ppermute | solution.py:47
  46.2 0.0 collective-permute-start.3
  46.2 2.7 %collective-permute-start.4 = (bf16[160,2048]{1,0:T(8,128)(2,1)S(1)}, bf16[160,2048]{1,0:T(8,128)(2,1)}, u32[]{:S(2)}, u32[]{:S(2)}) collective-permute-start(bf16[160,2048]{1,0:T(8,128)(2,1)S(1)} %bitcast_dynamic-update-slice_fusion.refs_0_.a0), channel_id=1, source_target_pairs={{0,6},{2,0},{4,2},{6,4},{8,14},{10,8},{12,10},{14,12},{16,22},{18,... | collective-permute-start | bytes 1966088 | tf_op jit(solution)/shard_map/ppermute | solution.py:47
  48.8 0.0 collective-permute-start.6
  48.9 0.1 collective-permute-start.9
  48.9 14.1 %collective-permute-done.5.refs_1_ = bf16[176,2048]{1,0:T(8,128)(2,1)} collective-permute-done((bf16[176,2048]{1,0:T(8,128)(2,1)}, bf16[176,2048]{1,0:T(8,128)(2,1)}, u32[]{:S(2)}, u32[]{:S(2)}) %collective-permute-start.5) | collective-permute-done | bytes 720928 | tf_op jit(solution)/shard_map/ppermute | solution.py:47
  63.0 0.0 collective-permute-start.7
  63.0 0.1 all-to-all-done.1
  63.2 0.7 broadcast_in_dim.19
  63.9 4.6 %all-to-all-start.2 = ((bf16[16,24,128]{2,1,0:T(8,128)(2,1)}), bf16[16,24,128]{2,1,0:T(8,128)(2,1)S(1)}, u32[]{:S(2)}, u32[]{:S(2)}) async-start(bf16[16,24,128]{2,1,0:T(8,128)(2,1)} %broadcast_in_dim.19), calls=%async_computation.2 | async-start | bytes 196608 | tf_op jit(solution)/shard_map/all_to_all | solution.py:28
  68.4 0.0 copy-start.4
  68.5 8.8 %collective-permute-done.3.refs_2_.a2 = bf16[160,2048]{1,0:T(8,128)(2,1)} collective-permute-done((bf16[160,2048]{1,0:T(8,128)(2,1)S(1)}, bf16[160,2048]{1,0:T(8,128)(2,1)}, u32[]{:S(2)}, u32[]{:S(2)}) %collective-permute-start.3) | collective-permute-done | bytes 655392 | tf_op jit(solution)/shard_map/ppermute | solution.py:47
  77.3 1.4 shard_map.186.w_held
  78.7 2.2 %shard_map.187 = (bf16[128,128]{1,0:T(8,128)(2,1)}, f32[24,128]{1,0:T(8,128)S(1)}) custom-call(bf16[16,24,128]{2,1,0:T(8,128)(2,1)S(1)} %all-to-all-done.2.tiles, f32[1,2048]{1,0:T(1,128)S(1)} %bitcast.21, bf16[3,128,2048]{2,1,0:T(8,128)(2,1)S(1)} %shard_map.186.w_held, bf16[160,2048]{1,0:T(8,128)(2,1)} %collective-permute-done.4.a3), custom_call_target="tpu_custom_call" | custom-call | flops 1048576 | bytes 2334720 | tf_op jit(solution)/shard_map/pallas_call | solution.py:81
  80.9 3.3 %all-to-all-start.3 = ((bf16[8,16,128]{2,1,0:T(8,128)(2,1)}), bf16[8,16,128]{2,1,0:T(8,128)(2,1)S(1)}, u32[]{:S(2)}, u32[]{:S(2)}) async-start(bf16[8,16,128]{2,1,0:T(8,128)(2,1)} %bitcast.11), calls=%async_computation.3 | async-start | bytes 65536 | tf_op jit(solution)/shard_map/all_to_all | solution.py:28
  84.2 0.0 copy-start.2
  84.3 0.0 copy-start.6
  84.3 1.4 %shard_map.189.state = f32[3,8,128,128]{3,2,1,0:T(8,128)S(1)} custom-call(f32[3,8,128,128]{3,2,1,0:T(8,128)} %state.1), custom_call_target="tpu_custom_call" | custom-call | flops 1048576 | bytes 1572864 | tf_op jit(solution)/shard_map/pallas_call | solution.py:81
  85.7 0.1 shard_map.188.floor_t
  85.8 5.2 %all-to-all-done.3 = bf16[8,16,128]{2,1,0:T(8,128)(2,1)S(1)} async-done(((bf16[8,16,128]{2,1,0:T(8,128)(2,1)}), bf16[8,16,128]{2,1,0:T(8,128)(2,1)S(1)}, u32[]{:S(2)}, u32[]{:S(2)}) %all-to-all-start.3) | async-done | bytes 32800 | tf_op jit(solution)/shard_map/all_to_all | solution.py:28
  91.0 1.2 shard_map.190
  92.3 0.7 broadcast_in_dim.20
  92.9 5.8 %all-to-all-start.4 = ((bf16[16,24,128]{2,1,0:T(8,128)(2,1)}), bf16[16,24,128]{2,1,0:T(8,128)(2,1)S(1)}, u32[]{:S(2)}, u32[]{:S(2)}) async-start(bf16[16,24,128]{2,1,0:T(8,128)(2,1)} %broadcast_in_dim.20), calls=%async_computation.4 | async-start | bytes 196608 | tf_op jit(solution)/shard_map/all_to_all | solution.py:28
  98.7 0.0 collective-permute-start.8
  98.7 0.0 collective-permute-done.9.d2
  98.7 2.7 %collective-permute-start.10 = (bf16[88,2048]{1,0:T(8,128)(2,1)}, bf16[88,2048]{1,0:T(8,128)(2,1)}, u32[]{:S(2)}, u32[]{:S(2)}) collective-permute-start(bf16[88,2048]{1,0:T(8,128)(2,1)} %collective-permute-done.9.d2), channel_id=1, source_target_pairs={{0,6},{2,0},{4,2},{6,4},{8,14},{10,8},{12,10},{14,12},{16,22},{18,... | collective-permute-start | bytes 1081352 | tf_op jit(solution)/shard_map/ppermute | solution.py:47
  101.4 1.1 shard_map.191.w_mix
  102.5 4.7 %all-to-all-done.4.tiles = bf16[16,24,128]{2,1,0:T(8,128)(2,1)S(1)} async-done(((bf16[16,24,128]{2,1,0:T(8,128)(2,1)}), bf16[16,24,128]{2,1,0:T(8,128)(2,1)S(1)}, u32[]{:S(2)}, u32[]{:S(2)}) %all-to-all-start.4) | async-done | bytes 98336 | tf_op jit(solution)/shard_map/all_to_all | solution.py:28
  107.2 0.4 shard_map.192.after
  107.6 0.7 broadcast_in_dim.21
  108.2 3.4 %all-to-all-start.5 = ((bf16[16,24,128]{2,1,0:T(8,128)(2,1)}), bf16[16,24,128]{2,1,0:T(8,128)(2,1)S(1)}, u32[]{:S(2)}, u32[]{:S(2)}) async-start(bf16[16,24,128]{2,1,0:T(8,128)(2,1)} %broadcast_in_dim.21), calls=%async_computation.5 | async-start | bytes 196608 | tf_op jit(solution)/shard_map/all_to_all | solution.py:28
  111.7 0.0 copy-start.5
  111.7 1.6 %shard_map.193.w_held = bf16[3,176,2048]{2,1,0:T(8,128)(2,1)S(1)} custom-call(bf16[176,2048]{1,0:T(8,128)(2,1)} %pad_maximum_fusion.refs_0_, bf16[176,2048]{1,0:T(8,128)(2,1)} %collective-permute-done.5.refs_1_, bf16[176,2048]{1,0:T(8,128)(2,1)} %collective-permute-done.6.refs_2_), custom_call_target="tpu_custom_call" | custom-call | flops 1048576 | bytes 2162688 | tf_op jit(solution)/shard_map/pallas_call | solution.py:81
  113.3 1.4 copy-done
  114.6 0.0 collective-permute-done.8.d1
  114.7 0.0 collective-permute-done.7.t3
  114.7 5.3 %all-to-all-done.5.tiles = bf16[16,24,128]{2,1,0:T(8,128)(2,1)S(1)} async-done(((bf16[16,24,128]{2,1,0:T(8,128)(2,1)}), bf16[16,24,128]{2,1,0:T(8,128)(2,1)S(1)}, u32[]{:S(2)}, u32[]{:S(2)}) %all-to-all-start.5) | async-done | bytes 98336 | tf_op jit(solution)/shard_map/all_to_all | solution.py:28
  120.0 1.6 %copy-done.1 = bf16[3,176,2048]{2,1,0:T(8,128)(2,1)S(1)} copy-done((bf16[3,176,2048]{2,1,0:T(8,128)(2,1)S(1)}, bf16[3,176,2048]{2,1,0:T(8,128)(2,1)}, u32[]{:S(2)}) %copy-start.1) | copy-done | bytes 2162712
  121.6 2.7 %shard_map.194 = (f32[8,24,128]{2,1,0:T(8,128)S(1)}, bf16[8,24,128]{2,1,0:T(8,128)(2,1)S(1)}) custom-call(bf16[16,24,128]{2,1,0:T(8,128)(2,1)S(1)} %all-to-all-done.5.tiles, f32[1,2048]{1,0:T(1,128)S(1)} %bitcast.22, bf16[24,128]{1,0:T(8,128)(2,1)S(1)} %shard_map.192.after, bf16[3,176,2048]{2,1,0:T(8,128)(2,1)S(1)} %copy-done.1, ...), custom_call_target="tpu_custom_call" | custom-call | flops 1048576 | bytes 4438016 | tf_op jit(solution)/shard_map/pallas_call | solution.py:81
  124.3 0.1 collective-permute-start.11
  124.4 1.2 collective-permute-done.11
  125.6 0.7 broadcast_in_dim.22
  126.3 3.9 %all-to-all-start.6 = ((bf16[32,24,128]{2,1,0:T(8,128)(2,1)}), bf16[32,24,128]{2,1,0:T(8,128)(2,1)S(1)}, u32[]{:S(2)}, u32[]{:S(2)}) async-start(bf16[32,24,128]{2,1,0:T(8,128)(2,1)} %bitcast.16), calls=%async_computation.6 | async-start | bytes 393216 | tf_op jit(solution)/shard_map/all_to_all | solution.py:28
  130.2 2.6 %next_state.1 = f32[3,8,128,128]{3,2,1,0:T(8,128)} custom-call(f32[3,8,128,128]{3,2,1,0:T(8,128)S(1)} %shard_map.189.state, f32[3,24,128]{2,1,0:T(8,128)S(1)} %get-tuple-element.19.vectors), custom_call_target="tpu_custom_call" | custom-call | flops 1048576 | bytes 4194304 | tf_op jit(solution)/shard_map/next_state/pallas_call | solution.py:507
  132.8 8.1 %all-to-all-done.6.arrived = bf16[32,24,128]{2,1,0:T(8,128)(2,1)S(1)} async-done(((bf16[32,24,128]{2,1,0:T(8,128)(2,1)}), bf16[32,24,128]{2,1,0:T(8,128)(2,1)S(1)}, u32[]{:S(2)}, u32[]{:S(2)}) %all-to-all-start.6) | async-done | bytes 196640 | tf_op jit(solution)/shard_map/all_to_all | solution.py:28
  140.9 0.9 shard_map.195
  (38 shorter events, 0.2 us)
Async XLA Ops:
  0.6 15.5 %copy-start.13 = (bf16[2048,8,4]{0,2,1:T(4,128)(2,1)S(1)}, bf16[2048,8,4]{0,2,1:T(4,128)(2,1)}, u32[]{:S(2)}) copy-start(bf16[2048,8,4]{0,2,1:T(4,128)(2,1)} %param.28) | copy-start | bytes 393220
  0.6 15.5 %copy-start.14 = (bf16[2048,8,4]{0,2,1:T(4,128)(2,1)S(1)}, bf16[2048,8,4]{0,2,1:T(4,128)(2,1)}, u32[]{:S(2)}) copy-start(bf16[2048,8,4]{0,2,1:T(4,128)(2,1)} %param.29) | copy-start | bytes 393220
  0.7 27.3 %copy-start.15 = (bf16[2048,32]{0,1:T(8,128)(2,1)S(1)}, bf16[2048,32]{0,1:T(8,128)(2,1)}, u32[]{:S(2)}) copy-start(bf16[2048,32]{0,1:T(8,128)(2,1)} %param.31) | copy-start | bytes 393220
  0.7 28.5 %copy-start.3 = (f32[2048]{0:T(1024)S(1)}, f32[2048]{0:T(1024)}, u32[]{:S(2)}) copy-start(f32[2048]{0:T(1024)} %param.21) | copy-start | bytes 24580
  2.2 23.3 %all-to-all-start = ((bf16[32,32,96]{2,1,0:T(8,128)(2,1)}), bf16[32,32,96]{2,1,0:T(8,128)(2,1)S(1)}, u32[]{:S(2)}, u32[]{:S(2)}) async-start(bf16[32,32,96]{2,1,0:T(8,128)(2,1)} %broadcast_in_dim.18), calls=%async_computation | async-start | bytes 524288 | tf_op jit(solution)/shard_map/all_to_all | solution.py:28
  16.1 15.7 %copy-start.9 = (bf16[2048,88]{0,1:T(8,128)(2,1)S(1)}, bf16[2048,88]{0,1:T(8,128)(2,1)}, u32[]{:S(2)}) copy-start(bf16[2048,88]{0,1:T(8,128)(2,1)} %param.34) | copy-start | bytes 1081348
  16.1 15.7 %copy-start.10 = (bf16[2048,88]{0,1:T(8,128)(2,1)S(1)}, bf16[2048,88]{0,1:T(8,128)(2,1)}, u32[]{:S(2)}) copy-start(bf16[2048,88]{0,1:T(8,128)(2,1)} %param.33) | copy-start | bytes 1081348
  25.5 3.6 %collective-permute-start = (bf16[32,32,96]{2,1,0:T(8,128)(2,1)S(1)}, bf16[32,32,96]{2,1,0:T(8,128)(2,1)S(1)}, u32[]{:S(2)}, u32[]{:S(2)}) collective-permute-start(bf16[32,32,96]{2,1,0:T(8,128)(2,1)S(1)} %all-to-all-done.own), channel_id=1, source_target_pairs={{0,1},{1,0},{2,3},{3,2},{4,5},{5,4},{6,7},{7,6},{8,9},{9,8},{10,11... | collective-permute-start | bytes 589832 | tf_op jit(solution)/shard_map/ppermute | solution.py:38
  28.0 18.2 %copy-start.7 = (bf16[160,2048]{1,0:T(8,128)(2,1)}, bf16[160,2048]{1,0:T(8,128)(2,1)S(1)}, u32[]{:S(2)}) copy-start(bf16[160,2048]{1,0:T(8,128)(2,1)S(1)} %bitcast_dynamic-update-slice_fusion.refs_0_.a0) | copy-start | bytes 1966084
  28.0 18.2 %collective-permute-start.2 = (bf16[160,2048]{1,0:T(8,128)(2,1)S(1)}, bf16[160,2048]{1,0:T(8,128)(2,1)S(1)}, u32[]{:S(2)}, u32[]{:S(2)}) collective-permute-start(bf16[160,2048]{1,0:T(8,128)(2,1)S(1)} %bitcast_dynamic-update-slice_fusion.refs_0_.a0), channel_id=1, source_target_pairs={{0,2},{2,4},{4,6},{6,0},{8,10},{10,12},{12,14},{14,8},{16,18},{18,... | collective-permute-start | bytes 1966088 | tf_op jit(solution)/shard_map/ppermute | solution.py:47
  31.3 17.5 %copy-start.11 = (bf16[88,2048]{1,0:T(8,128)(2,1)S(1)}, bf16[88,2048]{1,0:T(8,128)(2,1)}, u32[]{:S(2)}) copy-start(bf16[88,2048]{1,0:T(8,128)(2,1)} %d0.1) | copy-start | bytes 1081348
  31.3 1.5 %collective-permute-start.1 = (bf16[8,96,128]{2,1,0:T(8,128)(2,1)S(1)}, bf16[8,96,128]{2,1,0:T(8,128)(2,1)S(1)}, u32[]{:S(2)}, u32[]{:S(2)}) collective-permute-start(bf16[8,96,128]{2,1,0:T(8,128)(2,1)S(1)} %get-tuple-element.13), channel_id=1, source_target_pairs={{0,1},{1,0},{2,3},{3,2},{4,5},{5,4},{6,7},{7,6},{8,9},{9,8},{10,11... | collective-permute-start | bytes 589832 | tf_op jit(solution)/shard_map/ppermute | solution.py:38
  32.7 30.3 %collective-permute-start.5 = (bf16[176,2048]{1,0:T(8,128)(2,1)}, bf16[176,2048]{1,0:T(8,128)(2,1)}, u32[]{:S(2)}, u32[]{:S(2)}) collective-permute-start(bf16[176,2048]{1,0:T(8,128)(2,1)} %pad_maximum_fusion.refs_0_), channel_id=1, source_target_pairs={{0,2},{2,4},{4,6},{6,0},{8,10},{10,12},{12,14},{14,8},{16,18},{18,... | collective-permute-start | bytes 2162696 | tf_op jit(solution)/shard_map/ppermute | solution.py:47
  33.6 29.5 %all-to-all-start.1 = ((bf16[32,24,128]{2,1,0:T(8,128)(2,1)}), bf16[32,24,128]{2,1,0:T(8,128)(2,1)S(1)}, u32[]{:S(2)}, u32[]{:S(2)}) async-start(bf16[32,24,128]{2,1,0:T(8,128)(2,1)} %bitcast.4), calls=%async_computation.1 | async-start | bytes 393216 | tf_op jit(solution)/shard_map/all_to_all | solution.py:28
  46.2 22.3 %copy-start.8 = (bf16[160,2048]{1,0:T(8,128)(2,1)}, bf16[160,2048]{1,0:T(8,128)(2,1)S(1)}, u32[]{:S(2)}) copy-start(bf16[160,2048]{1,0:T(8,128)(2,1)S(1)} %collective-permute-done.2.refs_1_.a1) | copy-start | bytes 1966084
  46.2 31.1 %collective-permute-start.3 = (bf16[160,2048]{1,0:T(8,128)(2,1)S(1)}, bf16[160,2048]{1,0:T(8,128)(2,1)}, u32[]{:S(2)}, u32[]{:S(2)}) collective-permute-start(bf16[160,2048]{1,0:T(8,128)(2,1)S(1)} %collective-permute-done.2.refs_1_.a1), channel_id=1, source_target_pairs={{0,2},{2,4},{4,6},{6,0},{8,10},{10,12},{12,14},{14,8},{16,18},{18,... | collective-permute-start | bytes 1966088 | tf_op jit(solution)/shard_map/ppermute | solution.py:47
  46.2 32.5 %collective-permute-start.4 = (bf16[160,2048]{1,0:T(8,128)(2,1)S(1)}, bf16[160,2048]{1,0:T(8,128)(2,1)}, u32[]{:S(2)}, u32[]{:S(2)}) collective-permute-start(bf16[160,2048]{1,0:T(8,128)(2,1)S(1)} %bitcast_dynamic-update-slice_fusion.refs_0_.a0), channel_id=1, source_target_pairs={{0,6},{2,0},{4,2},{6,4},{8,14},{10,8},{12,10},{14,12},{16,22},{18,... | collective-permute-start | bytes 1966088 | tf_op jit(solution)/shard_map/ppermute | solution.py:47
  48.8 62.8 %collective-permute-start.6 = (bf16[176,2048]{1,0:T(8,128)(2,1)}, bf16[176,2048]{1,0:T(8,128)(2,1)}, u32[]{:S(2)}, u32[]{:S(2)}) collective-permute-start(bf16[176,2048]{1,0:T(8,128)(2,1)} %pad_maximum_fusion.refs_0_), channel_id=1, source_target_pairs={{0,6},{2,0},{4,2},{6,4},{8,14},{10,8},{12,10},{14,12},{16,22},{18,... | collective-permute-start | bytes 2162696 | tf_op jit(solution)/shard_map/ppermute | solution.py:47
  48.9 49.8 %collective-permute-start.9 = (bf16[88,2048]{1,0:T(8,128)(2,1)S(1)}, bf16[88,2048]{1,0:T(8,128)(2,1)}, u32[]{:S(2)}, u32[]{:S(2)}) collective-permute-start(bf16[88,2048]{1,0:T(8,128)(2,1)S(1)} %copy-done.11), channel_id=1, source_target_pairs={{0,6},{2,0},{4,2},{6,4},{8,14},{10,8},{12,10},{14,12},{16,22},{18,... | collective-permute-start | bytes 1081352 | tf_op jit(solution)/shard_map/ppermute | solution.py:47
  63.0 51.6 %collective-permute-start.7 = (bf16[176,2048]{1,0:T(8,128)(2,1)}, bf16[176,2048]{1,0:T(8,128)(2,1)}, u32[]{:S(2)}, u32[]{:S(2)}) collective-permute-start(bf16[176,2048]{1,0:T(8,128)(2,1)} %collective-permute-done.5.refs_1_), channel_id=1, source_target_pairs={{0,2},{2,4},{4,6},{6,0},{8,10},{10,12},{12,14},{14,8},{16,18},{18,... | collective-permute-start | bytes 2162696 | tf_op jit(solution)/shard_map/ppermute | solution.py:47
  63.9 14.8 %all-to-all-start.2 = ((bf16[16,24,128]{2,1,0:T(8,128)(2,1)}), bf16[16,24,128]{2,1,0:T(8,128)(2,1)S(1)}, u32[]{:S(2)}, u32[]{:S(2)}) async-start(bf16[16,24,128]{2,1,0:T(8,128)(2,1)} %broadcast_in_dim.19), calls=%async_computation.2 | async-start | bytes 196608 | tf_op jit(solution)/shard_map/all_to_all | solution.py:28
  68.4 10.2 %copy-start.4 = (f32[2048]{0:T(1024)S(1)}, f32[2048]{0:T(1024)}, u32[]{:S(2)}) copy-start(f32[2048]{0:T(1024)} %param.25) | copy-start | bytes 24580
  80.9 10.1 %all-to-all-start.3 = ((bf16[8,16,128]{2,1,0:T(8,128)(2,1)}), bf16[8,16,128]{2,1,0:T(8,128)(2,1)S(1)}, u32[]{:S(2)}, u32[]{:S(2)}) async-start(bf16[8,16,128]{2,1,0:T(8,128)(2,1)} %bitcast.11), calls=%async_computation.3 | async-start | bytes 65536 | tf_op jit(solution)/shard_map/all_to_all | solution.py:28
  84.2 1.5 %copy-start.2 = (f32[8,128]{1,0:T(8,128)S(1)}, f32[8,128]{1,0:T(8,128)}, u32[]{:S(2)}) copy-start(f32[8,128]{1,0:T(8,128)} %floor_rows.1) | copy-start | bytes 12292
  84.3 6.8 %copy-start.6 = (f32[8,128]{1,0:T(8,128)S(1)}, f32[8,128]{1,0:T(8,128)}, u32[]{:S(2)}) copy-start(f32[8,128]{1,0:T(8,128)} %gain.1) | copy-start | bytes 12292
  92.9 14.3 %all-to-all-start.4 = ((bf16[16,24,128]{2,1,0:T(8,128)(2,1)}), bf16[16,24,128]{2,1,0:T(8,128)(2,1)S(1)}, u32[]{:S(2)}, u32[]{:S(2)}) async-start(bf16[16,24,128]{2,1,0:T(8,128)(2,1)} %broadcast_in_dim.20), calls=%async_computation.4 | async-start | bytes 196608 | tf_op jit(solution)/shard_map/all_to_all | solution.py:28
  98.7 16.0 %collective-permute-start.8 = (bf16[88,2048]{1,0:T(8,128)(2,1)S(1)}, bf16[88,2048]{1,0:T(8,128)(2,1)S(1)}, u32[]{:S(2)}, u32[]{:S(2)}) collective-permute-start(bf16[88,2048]{1,0:T(8,128)(2,1)S(1)} %copy-done.11), channel_id=1, source_target_pairs={{0,2},{2,4},{4,6},{6,0},{8,10},{10,12},{12,14},{14,8},{16,18},{18,... | collective-permute-start | bytes 1081352 | tf_op jit(solution)/shard_map/ppermute | solution.py:47
  98.7 15.9 %collective-permute-start.10 = (bf16[88,2048]{1,0:T(8,128)(2,1)}, bf16[88,2048]{1,0:T(8,128)(2,1)}, u32[]{:S(2)}, u32[]{:S(2)}) collective-permute-start(bf16[88,2048]{1,0:T(8,128)(2,1)} %collective-permute-done.9.d2), channel_id=1, source_target_pairs={{0,6},{2,0},{4,2},{6,4},{8,14},{10,8},{12,10},{14,12},{16,22},{18,... | collective-permute-start | bytes 1081352 | tf_op jit(solution)/shard_map/ppermute | solution.py:47
  108.2 11.7 %all-to-all-start.5 = ((bf16[16,24,128]{2,1,0:T(8,128)(2,1)}), bf16[16,24,128]{2,1,0:T(8,128)(2,1)S(1)}, u32[]{:S(2)}, u32[]{:S(2)}) async-start(bf16[16,24,128]{2,1,0:T(8,128)(2,1)} %broadcast_in_dim.21), calls=%async_computation.5 | async-start | bytes 196608 | tf_op jit(solution)/shard_map/all_to_all | solution.py:28
  111.7 8.3 %copy-start.5 = (f32[2048]{0:T(1024)S(1)}, f32[2048]{0:T(1024)}, u32[]{:S(2)}) copy-start(f32[2048]{0:T(1024)} %param.32) | copy-start | bytes 24580
  113.3 1.4 copy-start
  114.6 5.3 %copy-start.12 = (bf16[88,2048]{1,0:T(8,128)(2,1)}, bf16[88,2048]{1,0:T(8,128)(2,1)S(1)}, u32[]{:S(2)}) copy-start(bf16[88,2048]{1,0:T(8,128)(2,1)S(1)} %collective-permute-done.8.d1) | copy-start | bytes 1081348
  120.0 1.6 %copy-start.1 = (bf16[3,176,2048]{2,1,0:T(8,128)(2,1)S(1)}, bf16[3,176,2048]{2,1,0:T(8,128)(2,1)}, u32[]{:S(2)}) copy-start(bf16[3,176,2048]{2,1,0:T(8,128)(2,1)} %copy-done) | copy-start | bytes 6488068
  124.3 1.3 collective-permute-start.11
  126.3 14.5 %all-to-all-start.6 = ((bf16[32,24,128]{2,1,0:T(8,128)(2,1)}), bf16[32,24,128]{2,1,0:T(8,128)(2,1)S(1)}, u32[]{:S(2)}, u32[]{:S(2)}) async-start(bf16[32,24,128]{2,1,0:T(8,128)(2,1)} %bitcast.16), calls=%async_computation.6 | async-start | bytes 393216 | tf_op jit(solution)/shard_map/all_to_all | solution.py:28

commit v3 on v2

--- a/solution.py
+++ b/solution.py
@@ -68,13 +68,13 @@
     return jnp.where(mask, 1.0, 0.0).astype(jnp.bfloat16)
 
 
-def local(body, outs, *args, scratch=(), outside=(), vmem=False, flops=1 << 20):
+def local(body, outs, *args, scratch=(), outside=(), held_out=False, vmem=False, flops=1 << 20):
     kind = pltpu.VMEM if vmem else jax.ShapeDtypeStruct
     shapes = [kind(s, d) for s, d in outs]
     held = pl.BlockSpec(memory_space=pltpu.VMEM)
     specs = [pl.BlockSpec(memory_space=pl.ANY) if k in outside else held for k in range(len(args))]
     args = [
-        pltpu.with_memory_space_constraint(a, pltpu.HBM) if k in outside else a
+        pltpu.with_memory_space_constraint(a, pltpu.HBM) if held_out and k in outside else a
         for k, a in enumerate(args)
     ]
     size = sum(a.size * a.dtype.itemsize for a in args)
@@ -385,11 +385,6 @@
     out[...] = bf(matmul(picked, hot(old == wanted), NN))
 
 
-def along_y(w):
-    below, above = shift_y(w, 1), shift_y(w, -1)
-    return below, above
-
-
 def shards(
     hidden_in,
     state,
@@ -447,6 +442,7 @@
             dma((3,)),
         ),
         outside=(3, 4, 5),
+        held_out=True,
     )
     both = bf(mine + f32(swap_cores(theirs)))
     summed = exchange(both.reshape(KV_COUNT, slab_rows, LANES), "kv")
@@ -454,10 +450,14 @@
     twice = shift_y(below, 1)
     after_own = bf(slab + 0.5 * f32(summed).sum(axis=0))
 
-    tops = [late_top, *along_y(late_top)]
-    lows = [w_down_two, *along_y(w_down_two)]
-    tops.append(shift_y(tops[1], 1))
-    lows.append(shift_y(lows[2], -1))
+    top_above = shift_y(late_top, -1)
+    top_below = shift_y(late_top, 1)
+    low_above = shift_y(w_down_two, -1)
+    low_below = shift_y(w_down_two, 1)
+    top_far = shift_y(top_above, -1)
+    low_far = shift_y(low_above, -1)
+    tops = (late_top, top_below, top_above, top_far)
+    lows = (w_down_two, low_below, low_above, low_far)
 
     after_tiles = slab_exchange(after_own)
     parts = (early, below, twice, above)
@@ -467,6 +467,7 @@
         *parts[:-1],
         scratch=(dma((Y_COUNT - 1,)),),
         outside=(0, 1, 2),
+        held_out=True,
         vmem=True,
     )
     channels, residual = local(
@@ -482,6 +483,7 @@
             dma((1,)),
         ),
         outside=(3,),
+        held_out=True,
     )
     zgroups = [[a * Y_COUNT + b for a in range(Z_COUNT)] for b in range(Y_COUNT)]
     arrived = exchange(channels.reshape(Z_COUNT, 16, LANES), "kv", zgroups)
@@ -523,6 +525,7 @@
         *parts,
         scratch=(dma((Y_COUNT,)),),
         outside=(0, 1, 2, 3),
+        held_out=True,
         vmem=True,
     )
     (after_mix,) = local(

time: 143 us -> 135 us (0.944)
  waiting for transfers between devices: 65.4 us -> 47.3 us
  local copies, waits for them, and re-layouts: 9.23 us -> 15.1 us
  starting transfers between devices: 46.6 us -> 51.7 us
    ppermute x9, waiting for transfers between devices: 30.3 us -> 12.7 us  [shift_y(): return lax.ppermute(x, 'kv', pairs)]
    ppermute x9, starting transfers between devices: 5.52 us -> 11.7 us  [shift_y(): return lax.ppermute(x, 'kv', pairs)]
    unnamed x36 -> x40, local copies, waits for them, and re-layouts: 3.1 us -> 8.34 us
  transfers between devices with their start and end apart: 19 -> 19, of which waited for: 12 -> 10; matrix products, arithmetic and copies ran while one was open for 4% -> 6% of each run, Pallas kernels for 10% -> 10%
where the time goes in v3:
time: 135 us; the launch traced here: 134 us
  starting transfers between devices  51.7 us (38%)
  waiting for transfers between devices  47.3 us (35%)
  Pallas kernels  17.8 us (13%)
  local copies, waits for them, and re-layouts  15.1 us (11%)
    all_to_all x7, starting transfers between devices, exchange(): lax.all_to_all(tiles, axis, split_axis=0, concat_axis=0, axis_index_group...  37 us
    all_to_all x7, waiting for transfers between devices, exchange(): lax.all_to_all(tiles, axis, split_axis=0, concat_axis=0, axis_index_group...  32.9 us
    pallas_call x11, Pallas kernels, local(): pl.pallas_call(body, out_shape=shapes, in_specs=specs, out_specs=[held] *...  15.3 us
    ppermute x9, waiting for transfers between devices, shift_y(): return lax.ppermute(x, 'kv', pairs)  12.7 us
    ppermute x9, starting transfers between devices, shift_y(): return lax.ppermute(x, 'kv', pairs)  11.7 us
    unnamed x40, local copies, waits for them, and re-layouts  8.34 us
    broadcast_in_dim x4, local copies, waits for them, and re-layouts, copies(): return jnp.broadcast_to(x, (count, *x.shape))  3.49 us
    ppermute x3, starting transfers between devices, swap_cores(): return lax.ppermute(x, 'tp', [(0, 1), (1, 0)])  3 us
  transfers between devices with their start and end apart: 19, of which 10 were waited for; matrix products, arithmetic and copies ran while one was open for 6% of the time, Pallas kernels for 10%

profile of v3, /device:TPU:1, one launch (start us, length us, event | category | flops | bytes accessed | tf_op | source)
XLA Modules:
  0.0 133.7 jit_solution(12056990768917565005)
XLA Ops:
  0.7 1.5 %broadcast_in_dim.18 = bf16[32,32,96]{2,1,0:T(8,128)(2,1)} broadcast(bf16[32,96]{1,0:T(8,128)(2,1)} %bitcast.31), dimensions={1,2} | broadcast | bytes 202752 | tf_op jit(solution)/shard_map/broadcast_in_dim | solution.py:34
  2.2 12.0 %all-to-all-start = ((bf16[32,32,96]{2,1,0:T(8,128)(2,1)}), bf16[32,32,96]{2,1,0:T(8,128)(2,1)S(1)}, u32[]{:S(2)}, u32[]{:S(2)}) async-start(bf16[32,32,96]{2,1,0:T(8,128)(2,1)} %broadcast_in_dim.18), calls=%async_computation | async-start | bytes 524288 | tf_op jit(solution)/shard_map/all_to_all | solution.py:28
  14.2 0.9 reshape.41
  15.1 0.7 constant_dynamic-update-slice_fusion.3
  15.8 0.9 reshape.42
  16.7 0.0 copy-start.13
  16.8 0.0 copy-start.14
  16.9 0.7 constant_dynamic-update-slice_fusion.2
  17.5 0.7 constant_dynamic-update-slice_fusion.1
  18.2 0.7 constant_dynamic-update-slice_fusion
  18.9 6.6 %all-to-all-done.own = bf16[32,32,96]{2,1,0:T(8,128)(2,1)S(1)} async-done(((bf16[32,32,96]{2,1,0:T(8,128)(2,1)}), bf16[32,32,96]{2,1,0:T(8,128)(2,1)S(1)}, u32[]{:S(2)}, u32[]{:S(2)}) %all-to-all-start) | async-done | bytes 196640 | tf_op jit(solution)/shard_map/all_to_all | solution.py:28
  25.5 2.5 %collective-permute-start = (bf16[32,32,96]{2,1,0:T(8,128)(2,1)S(1)}, bf16[32,32,96]{2,1,0:T(8,128)(2,1)S(1)}, u32[]{:S(2)}, u32[]{:S(2)}) collective-permute-start(bf16[32,32,96]{2,1,0:T(8,128)(2,1)S(1)} %all-to-all-done.own), channel_id=1, source_target_pairs={{0,1},{1,0},{2,3},{3,2},{4,5},{5,4},{6,7},{7,6},{8,9},{9,8},{10,11... | collective-permute-start | bytes 589832 | tf_op jit(solution)/shard_map/ppermute | solution.py:38
  28.0 0.7 bitcast_dynamic-update-slice_fusion.refs_0_.a0
  28.6 0.5 collective-permute-done.other
  29.1 2.2 %shard_map.185 = (f32[8,96,128]{2,1,0:T(8,128)S(1)}, bf16[8,96,128]{2,1,0:T(8,128)(2,1)S(1)}, f32[24,128]{1,0:T(8,128)S(1)}) custom-call(bf16[32,32,96]{2,1,0:T(8,128)(2,1)S(1)} %all-to-all-done.own, bf16[32,32,96]{2,1,0:T(8,128)(2,1)S(1)} %collective-permute-done.other, f32[16,128]{1,0:T(8,128)S(1)} %bitcast.20, bf16[88,2048]{1,0:T(8,128)(2,1)} %bitcast.23, ...), custom_call_target="tpu_custom_call" | custom-call | flops 1048576 | bytes 1482752 | tf_op jit(solution)/shard_map/pallas_call | solution.py:81
  31.3 0.4 collective-permute-start.1
  31.8 2.2 %collective-permute-start.6 = (bf16[176,2048]{1,0:T(8,128)(2,1)S(1)}, bf16[176,2048]{1,0:T(8,128)(2,1)}, u32[]{:S(2)}, u32[]{:S(2)}) collective-permute-start(bf16[176,2048]{1,0:T(8,128)(2,1)S(1)} %pad_maximum_fusion.refs_0_), channel_id=1, source_target_pairs={{0,6},{2,0},{4,2},{6,4},{8,14},{10,8},{12,10},{14,12},{16,22},{18,... | collective-permute-start | bytes 2162696 | tf_op jit(solution)/shard_map/ppermute | solution.py:47
  34.0 0.7 add_convert_fusion
  34.7 3.9 %all-to-all-start.1 = ((bf16[32,24,128]{2,1,0:T(8,128)(2,1)}), bf16[32,24,128]{2,1,0:T(8,128)(2,1)S(1)}, u32[]{:S(2)}, u32[]{:S(2)}) async-start(bf16[32,24,128]{2,1,0:T(8,128)(2,1)} %bitcast.4), calls=%async_computation.1 | async-start | bytes 393216 | tf_op jit(solution)/shard_map/all_to_all | solution.py:28
  38.6 9.2 %collective-permute-done.2.refs_1_.a1 = bf16[160,2048]{1,0:T(8,128)(2,1)S(1)} collective-permute-done((bf16[160,2048]{1,0:T(8,128)(2,1)}, bf16[160,2048]{1,0:T(8,128)(2,1)S(1)}, u32[]{:S(2)}, u32[]{:S(2)}) %collective-permute-start.2) | collective-permute-done | bytes 655392 | tf_op jit(solution)/shard_map/ppermute | solution.py:47
  47.9 0.0 collective-permute-start.3
  47.9 2.7 %collective-permute-start.4 = (bf16[160,2048]{1,0:T(8,128)(2,1)}, bf16[160,2048]{1,0:T(8,128)(2,1)}, u32[]{:S(2)}, u32[]{:S(2)}) collective-permute-start(bf16[160,2048]{1,0:T(8,128)(2,1)} %bitcast_dynamic-update-slice_fusion.refs_0_.a0), channel_id=1, source_target_pairs={{0,6},{2,0},{4,2},{6,4},{8,14},{10,8},{12,10},{14,12},{16,22},{18,... | collective-permute-start | bytes 1966088 | tf_op jit(solution)/shard_map/ppermute | solution.py:47
  50.5 2.7 %collective-permute-start.9 = (bf16[88,2048]{1,0:T(8,128)(2,1)}, bf16[88,2048]{1,0:T(8,128)(2,1)}, u32[]{:S(2)}, u32[]{:S(2)}) collective-permute-start(bf16[88,2048]{1,0:T(8,128)(2,1)} %d0.1), channel_id=1, source_target_pairs={{0,6},{2,0},{4,2},{6,4},{8,14},{10,8},{12,10},{14,12},{16,22},{18,... | collective-permute-start | bytes 1081352 | tf_op jit(solution)/shard_map/ppermute | solution.py:47
  53.2 0.0 collective-permute-done.6.refs_2_
  53.2 1.5 %collective-permute-start.7 = (bf16[176,2048]{1,0:T(8,128)(2,1)}, bf16[176,2048]{1,0:T(8,128)(2,1)S(1)}, u32[]{:S(2)}, u32[]{:S(2)}) collective-permute-start(bf16[176,2048]{1,0:T(8,128)(2,1)} %collective-permute-done.6.refs_2_), channel_id=1, source_target_pairs={{0,6},{2,0},{4,2},{6,4},{8,14},{10,8},{12,10},{14,12},{16,22},{18,... | collective-permute-start | bytes 2162696 | tf_op jit(solution)/shard_map/ppermute | solution.py:47
  54.8 0.7 broadcast_in_dim.19
  55.4 5.4 %all-to-all-start.2 = ((bf16[16,24,128]{2,1,0:T(8,128)(2,1)}), bf16[16,24,128]{2,1,0:T(8,128)(2,1)S(1)}, u32[]{:S(2)}, u32[]{:S(2)}) async-start(bf16[16,24,128]{2,1,0:T(8,128)(2,1)} %broadcast_in_dim.19), calls=%async_computation.2 | async-start | bytes 196608 | tf_op jit(solution)/shard_map/all_to_all | solution.py:28
  60.8 0.0 copy-start.9
  60.9 3.5 %collective-permute-done.3.refs_2_.a2 = bf16[160,2048]{1,0:T(8,128)(2,1)} collective-permute-done((bf16[160,2048]{1,0:T(8,128)(2,1)S(1)}, bf16[160,2048]{1,0:T(8,128)(2,1)}, u32[]{:S(2)}, u32[]{:S(2)}) %collective-permute-start.3) | collective-permute-done | bytes 655392 | tf_op jit(solution)/shard_map/ppermute | solution.py:47
  64.3 1.4 %shard_map.186.w_held = bf16[3,128,2048]{2,1,0:T(8,128)(2,1)S(1)} custom-call(bf16[160,2048]{1,0:T(8,128)(2,1)} %bitcast_dynamic-update-slice_fusion.refs_0_.a0, bf16[160,2048]{1,0:T(8,128)(2,1)} %copy-done.12, bf16[160,2048]{1,0:T(8,128)(2,1)} %collective-permute-done.3.refs_2_.a2), custom_call_target="tpu_custom_call" | custom-call | flops 1048576 | bytes 1966080 | tf_op jit(solution)/shard_map/pallas_call | solution.py:81
  65.7 3.6 %all-to-all-done.2.tiles = bf16[16,24,128]{2,1,0:T(8,128)(2,1)S(1)} async-done(((bf16[16,24,128]{2,1,0:T(8,128)(2,1)}), bf16[16,24,128]{2,1,0:T(8,128)(2,1)S(1)}, u32[]{:S(2)}, u32[]{:S(2)}) %all-to-all-start.2) | async-done | bytes 98336 | tf_op jit(solution)/shard_map/all_to_all | solution.py:28
  69.3 2.2 %shard_map.187 = (bf16[128,128]{1,0:T(8,128)(2,1)}, f32[24,128]{1,0:T(8,128)S(1)}) custom-call(bf16[16,24,128]{2,1,0:T(8,128)(2,1)S(1)} %all-to-all-done.2.tiles, f32[1,2048]{1,0:T(1,128)S(1)} %bitcast.21, bf16[3,128,2048]{2,1,0:T(8,128)(2,1)S(1)} %shard_map.186.w_held, bf16[160,2048]{1,0:T(8,128)(2,1)} %collective-permute-done.4.a3), custom_call_target="tpu_custom_call" | custom-call | flops 1048576 | bytes 2334720 | tf_op jit(solution)/shard_map/pallas_call | solution.py:81
  71.6 3.3 %all-to-all-start.3 = ((bf16[8,16,128]{2,1,0:T(8,128)(2,1)}), bf16[8,16,128]{2,1,0:T(8,128)(2,1)S(1)}, u32[]{:S(2)}, u32[]{:S(2)}) async-start(bf16[8,16,128]{2,1,0:T(8,128)(2,1)} %bitcast.11), calls=%async_computation.3 | async-start | bytes 65536 | tf_op jit(solution)/shard_map/all_to_all | solution.py:28
  74.9 0.0 copy-start.2
  74.9 1.4 %copy-done.2 = f32[3,8,128,128]{3,2,1,0:T(8,128)S(1)} copy-done((f32[3,8,128,128]{3,2,1,0:T(8,128)S(1)}, f32[3,8,128,128]{3,2,1,0:T(8,128)}, u32[]{:S(2)}) %copy-start.2) | copy-done | bytes 1572888
  76.3 0.1 shard_map.189.state
  76.5 0.5 copy-done.5
  77.0 0.1 shard_map.188.floor_t
  77.1 4.6 %all-to-all-done.3 = bf16[8,16,128]{2,1,0:T(8,128)(2,1)S(1)} async-done(((bf16[8,16,128]{2,1,0:T(8,128)(2,1)}), bf16[8,16,128]{2,1,0:T(8,128)(2,1)S(1)}, u32[]{:S(2)}, u32[]{:S(2)}) %all-to-all-start.3) | async-done | bytes 32800 | tf_op jit(solution)/shard_map/all_to_all | solution.py:28
  81.7 1.2 shard_map.190
  82.9 0.7 broadcast_in_dim.20
  83.6 5.0 %all-to-all-start.4 = ((bf16[16,24,128]{2,1,0:T(8,128)(2,1)}), bf16[16,24,128]{2,1,0:T(8,128)(2,1)}, u32[]{:S(2)}, u32[]{:S(2)}) async-start(bf16[16,24,128]{2,1,0:T(8,128)(2,1)} %broadcast_in_dim.20), calls=%async_computation.4 | async-start | bytes 196608 | tf_op jit(solution)/shard_map/all_to_all | solution.py:28
  88.6 0.3 collective-permute-start.8
  89.0 2.3 %collective-permute-start.10 = (bf16[88,2048]{1,0:T(8,128)(2,1)}, bf16[88,2048]{1,0:T(8,128)(2,1)}, u32[]{:S(2)}, u32[]{:S(2)}) collective-permute-start(bf16[88,2048]{1,0:T(8,128)(2,1)} %collective-permute-done.9.d2), channel_id=1, source_target_pairs={{0,6},{2,0},{4,2},{6,4},{8,14},{10,8},{12,10},{14,12},{16,22},{18,... | collective-permute-start | bytes 1081352 | tf_op jit(solution)/shard_map/ppermute | solution.py:47
  91.3 1.1 shard_map.191.w_mix
  92.4 4.8 %all-to-all-done.4.tiles = bf16[16,24,128]{2,1,0:T(8,128)(2,1)} async-done(((bf16[16,24,128]{2,1,0:T(8,128)(2,1)}), bf16[16,24,128]{2,1,0:T(8,128)(2,1)}, u32[]{:S(2)}, u32[]{:S(2)}) %all-to-all-start.4) | async-done | bytes 98336 | tf_op jit(solution)/shard_map/all_to_all | solution.py:28
  97.2 0.7 copy-done.7
  97.9 1.3 shard_map.192.after
  99.2 0.7 broadcast_in_dim.21
  99.9 3.4 %all-to-all-start.5 = ((bf16[16,24,128]{2,1,0:T(8,128)(2,1)}), bf16[16,24,128]{2,1,0:T(8,128)(2,1)S(1)}, u32[]{:S(2)}, u32[]{:S(2)}) async-start(bf16[16,24,128]{2,1,0:T(8,128)(2,1)} %broadcast_in_dim.21), calls=%async_computation.5 | async-start | bytes 196608 | tf_op jit(solution)/shard_map/all_to_all | solution.py:28
  103.3 0.0 copy-start.10
  103.3 1.6 %shard_map.193.w_held = bf16[3,176,2048]{2,1,0:T(8,128)(2,1)S(1)} custom-call(bf16[176,2048]{1,0:T(8,128)(2,1)S(1)} %pad_maximum_fusion.refs_0_, bf16[176,2048]{1,0:T(8,128)(2,1)} %collective-permute-done.5.refs_1_, bf16[176,2048]{1,0:T(8,128)(2,1)} %collective-permute-done.6.refs_2_), custom_call_target="tpu_custom_call" | custom-call | flops 1048576 | bytes 2162688 | tf_op jit(solution)/shard_map/pallas_call | solution.py:81
  105.0 1.3 %copy-done = bf16[3,176,2048]{2,1,0:T(8,128)(2,1)} copy-done((bf16[3,176,2048]{2,1,0:T(8,128)(2,1)}, bf16[3,176,2048]{2,1,0:T(8,128)(2,1)S(1)}, u32[]{:S(2)}) %copy-start) | copy-done | bytes 2162712
  106.3 0.0 collective-permute-done.8.d1
  106.3 5.3 %all-to-all-done.5.tiles = bf16[16,24,128]{2,1,0:T(8,128)(2,1)S(1)} async-done(((bf16[16,24,128]{2,1,0:T(8,128)(2,1)}), bf16[16,24,128]{2,1,0:T(8,128)(2,1)S(1)}, u32[]{:S(2)}, u32[]{:S(2)}) %all-to-all-start.5) | async-done | bytes 98336 | tf_op jit(solution)/shard_map/all_to_all | solution.py:28
  111.6 1.6 %copy-done.1 = bf16[3,176,2048]{2,1,0:T(8,128)(2,1)S(1)} copy-done((bf16[3,176,2048]{2,1,0:T(8,128)(2,1)S(1)}, bf16[3,176,2048]{2,1,0:T(8,128)(2,1)}, u32[]{:S(2)}) %copy-start.1) | copy-done | bytes 2162712
  113.3 3.1 %shard_map.194 = (f32[8,24,128]{2,1,0:T(8,128)S(1)}, bf16[8,24,128]{2,1,0:T(8,128)(2,1)S(1)}) custom-call(bf16[16,24,128]{2,1,0:T(8,128)(2,1)S(1)} %all-to-all-done.5.tiles, f32[1,2048]{1,0:T(1,128)S(1)} %bitcast.22, bf16[24,128]{1,0:T(8,128)(2,1)S(1)} %shard_map.192.after, bf16[3,176,2048]{2,1,0:T(8,128)(2,1)S(1)} %copy-done.1, ...), custom_call_target="tpu_custom_call" | custom-call | flops 1048576 | bytes 4438016 | tf_op jit(solution)/shard_map/pallas_call | solution.py:81
  116.4 0.1 collective-permute-start.11
  116.5 1.2 collective-permute-done.11
  117.7 0.7 broadcast_in_dim.22
  118.4 3.9 %all-to-all-start.6 = ((bf16[32,24,128]{2,1,0:T(8,128)(2,1)}), bf16[32,24,128]{2,1,0:T(8,128)(2,1)S(1)}, u32[]{:S(2)}, u32[]{:S(2)}) async-start(bf16[32,24,128]{2,1,0:T(8,128)(2,1)} %bitcast.16), calls=%async_computation.6 | async-start | bytes 393216 | tf_op jit(solution)/shard_map/all_to_all | solution.py:28
  122.3 2.6 %next_state.1 = f32[3,8,128,128]{3,2,1,0:T(8,128)} custom-call(f32[3,8,128,128]{3,2,1,0:T(8,128)S(1)} %shard_map.189.state, f32[3,24,128]{2,1,0:T(8,128)S(1)} %copy-done.4), custom_call_target="tpu_custom_call" | custom-call | flops 1048576 | bytes 4194304 | tf_op jit(solution)/shard_map/next_state/pallas_call | solution.py:509
  124.9 8.0 %all-to-all-done.6.arrived = bf16[32,24,128]{2,1,0:T(8,128)(2,1)S(1)} async-done(((bf16[32,24,128]{2,1,0:T(8,128)(2,1)}), bf16[32,24,128]{2,1,0:T(8,128)(2,1)S(1)}, u32[]{:S(2)}, u32[]{:S(2)}) %all-to-all-start.6) | async-done | bytes 196640 | tf_op jit(solution)/shard_map/all_to_all | solution.py:28
  132.8 0.9 shard_map.195
  (42 shorter events, 0.3 us)
Async XLA Ops:
  0.6 16.1 %copy-start.15 = (bf16[2048,8,4]{0,2,1:T(4,128)(2,1)S(1)}, bf16[2048,8,4]{0,2,1:T(4,128)(2,1)}, u32[]{:S(2)}) copy-start(bf16[2048,8,4]{0,2,1:T(4,128)(2,1)} %param.28) | copy-start | bytes 393220
  0.6 16.2 %copy-start.16 = (bf16[2048,8,4]{0,2,1:T(4,128)(2,1)S(1)}, bf16[2048,8,4]{0,2,1:T(4,128)(2,1)}, u32[]{:S(2)}) copy-start(bf16[2048,8,4]{0,2,1:T(4,128)(2,1)} %param.29) | copy-start | bytes 393220
  0.7 27.3 %copy-start.17 = (bf16[2048,32]{0,1:T(8,128)(2,1)S(1)}, bf16[2048,32]{0,1:T(8,128)(2,1)}, u32[]{:S(2)}) copy-start(bf16[2048,32]{0,1:T(8,128)(2,1)} %param.31) | copy-start | bytes 393220
  0.7 28.5 %copy-start.8 = (f32[2048]{0:T(1024)S(1)}, f32[2048]{0:T(1024)}, u32[]{:S(2)}) copy-start(f32[2048]{0:T(1024)} %param.21) | copy-start | bytes 24580
  2.2 23.3 %all-to-all-start = ((bf16[32,32,96]{2,1,0:T(8,128)(2,1)}), bf16[32,32,96]{2,1,0:T(8,128)(2,1)S(1)}, u32[]{:S(2)}, u32[]{:S(2)}) async-start(bf16[32,32,96]{2,1,0:T(8,128)(2,1)} %broadcast_in_dim.18), calls=%async_computation | async-start | bytes 524288 | tf_op jit(solution)/shard_map/all_to_all | solution.py:28
  16.7 15.0 %copy-start.13 = (bf16[2048,88]{0,1:T(8,128)(2,1)S(1)}, bf16[2048,88]{0,1:T(8,128)(2,1)}, u32[]{:S(2)}) copy-start(bf16[2048,88]{0,1:T(8,128)(2,1)} %param.34) | copy-start | bytes 1081348
  16.8 15.0 %copy-start.14 = (bf16[2048,88]{0,1:T(8,128)(2,1)S(1)}, bf16[2048,88]{0,1:T(8,128)(2,1)}, u32[]{:S(2)}) copy-start(bf16[2048,88]{0,1:T(8,128)(2,1)} %param.33) | copy-start | bytes 1081348
  25.5 3.6 %collective-permute-start = (bf16[32,32,96]{2,1,0:T(8,128)(2,1)S(1)}, bf16[32,32,96]{2,1,0:T(8,128)(2,1)S(1)}, u32[]{:S(2)}, u32[]{:S(2)}) collective-permute-start(bf16[32,32,96]{2,1,0:T(8,128)(2,1)S(1)} %all-to-all-done.own), channel_id=1, source_target_pairs={{0,1},{1,0},{2,3},{3,2},{4,5},{5,4},{6,7},{7,6},{8,9},{9,8},{10,11... | collective-permute-start | bytes 589832 | tf_op jit(solution)/shard_map/ppermute | solution.py:38
  28.6 19.2 %collective-permute-start.2 = (bf16[160,2048]{1,0:T(8,128)(2,1)}, bf16[160,2048]{1,0:T(8,128)(2,1)S(1)}, u32[]{:S(2)}, u32[]{:S(2)}) collective-permute-start(bf16[160,2048]{1,0:T(8,128)(2,1)} %bitcast_dynamic-update-slice_fusion.refs_0_.a0), channel_id=1, source_target_pairs={{0,2},{2,4},{4,6},{6,0},{8,10},{10,12},{12,14},{14,8},{16,18},{18,... | collective-permute-start | bytes 1966088 | tf_op jit(solution)/shard_map/ppermute | solution.py:47
  31.3 2.7 %collective-permute-start.1 = (bf16[8,96,128]{2,1,0:T(8,128)(2,1)S(1)}, bf16[8,96,128]{2,1,0:T(8,128)(2,1)S(1)}, u32[]{:S(2)}, u32[]{:S(2)}) collective-permute-start(bf16[8,96,128]{2,1,0:T(8,128)(2,1)S(1)} %get-tuple-element.13), channel_id=1, source_target_pairs={{0,1},{1,0},{2,3},{3,2},{4,5},{5,4},{6,7},{7,6},{8,9},{9,8},{10,11... | collective-permute-start | bytes 589832 | tf_op jit(solution)/shard_map/ppermute | solution.py:38
  31.8 21.4 %collective-permute-start.6 = (bf16[176,2048]{1,0:T(8,128)(2,1)S(1)}, bf16[176,2048]{1,0:T(8,128)(2,1)}, u32[]{:S(2)}, u32[]{:S(2)}) collective-permute-start(bf16[176,2048]{1,0:T(8,128)(2,1)S(1)} %pad_maximum_fusion.refs_0_), channel_id=1, source_target_pairs={{0,6},{2,0},{4,2},{6,4},{8,14},{10,8},{12,10},{14,12},{16,22},{18,... | collective-permute-start | bytes 2162696 | tf_op jit(solution)/shard_map/ppermute | solution.py:47
  34.7 19.9 %all-to-all-start.1 = ((bf16[32,24,128]{2,1,0:T(8,128)(2,1)}), bf16[32,24,128]{2,1,0:T(8,128)(2,1)S(1)}, u32[]{:S(2)}, u32[]{:S(2)}) async-start(bf16[32,24,128]{2,1,0:T(8,128)(2,1)} %bitcast.4), calls=%async_computation.1 | async-start | bytes 393216 | tf_op jit(solution)/shard_map/all_to_all | solution.py:28
  47.8 13.0 %copy-start.12 = (bf16[160,2048]{1,0:T(8,128)(2,1)}, bf16[160,2048]{1,0:T(8,128)(2,1)S(1)}, u32[]{:S(2)}) copy-start(bf16[160,2048]{1,0:T(8,128)(2,1)S(1)} %collective-permute-done.2.refs_1_.a1) | copy-start | bytes 1966084
  47.9 16.5 %collective-permute-start.3 = (bf16[160,2048]{1,0:T(8,128)(2,1)S(1)}, bf16[160,2048]{1,0:T(8,128)(2,1)}, u32[]{:S(2)}, u32[]{:S(2)}) collective-permute-start(bf16[160,2048]{1,0:T(8,128)(2,1)S(1)} %collective-permute-done.2.refs_1_.a1), channel_id=1, source_target_pairs={{0,2},{2,4},{4,6},{6,0},{8,10},{10,12},{12,14},{14,8},{16,18},{18,... | collective-permute-start | bytes 1966088 | tf_op jit(solution)/shard_map/ppermute | solution.py:47
  47.9 17.9 %collective-permute-start.4 = (bf16[160,2048]{1,0:T(8,128)(2,1)}, bf16[160,2048]{1,0:T(8,128)(2,1)}, u32[]{:S(2)}, u32[]{:S(2)}) collective-permute-start(bf16[160,2048]{1,0:T(8,128)(2,1)} %bitcast_dynamic-update-slice_fusion.refs_0_.a0), channel_id=1, source_target_pairs={{0,6},{2,0},{4,2},{6,4},{8,14},{10,8},{12,10},{14,12},{16,22},{18,... | collective-permute-start | bytes 1966088 | tf_op jit(solution)/shard_map/ppermute | solution.py:47
  50.5 52.8 %collective-permute-start.5 = (bf16[176,2048]{1,0:T(8,128)(2,1)S(1)}, bf16[176,2048]{1,0:T(8,128)(2,1)}, u32[]{:S(2)}, u32[]{:S(2)}) collective-permute-start(bf16[176,2048]{1,0:T(8,128)(2,1)S(1)} %pad_maximum_fusion.refs_0_), channel_id=1, source_target_pairs={{0,2},{2,4},{4,6},{6,0},{8,10},{10,12},{12,14},{14,8},{16,18},{18,... | collective-permute-start | bytes 2162696 | tf_op jit(solution)/shard_map/ppermute | solution.py:47
  50.5 38.4 %collective-permute-start.9 = (bf16[88,2048]{1,0:T(8,128)(2,1)}, bf16[88,2048]{1,0:T(8,128)(2,1)}, u32[]{:S(2)}, u32[]{:S(2)}) collective-permute-start(bf16[88,2048]{1,0:T(8,128)(2,1)} %d0.1), channel_id=1, source_target_pairs={{0,6},{2,0},{4,2},{6,4},{8,14},{10,8},{12,10},{14,12},{16,22},{18,... | collective-permute-start | bytes 1081352 | tf_op jit(solution)/shard_map/ppermute | solution.py:47
  53.2 53.1 %collective-permute-start.7 = (bf16[176,2048]{1,0:T(8,128)(2,1)}, bf16[176,2048]{1,0:T(8,128)(2,1)S(1)}, u32[]{:S(2)}, u32[]{:S(2)}) collective-permute-start(bf16[176,2048]{1,0:T(8,128)(2,1)} %collective-permute-done.6.refs_2_), channel_id=1, source_target_pairs={{0,6},{2,0},{4,2},{6,4},{8,14},{10,8},{12,10},{14,12},{16,22},{18,... | collective-permute-start | bytes 2162696 | tf_op jit(solution)/shard_map/ppermute | solution.py:47
  55.4 13.9 %all-to-all-start.2 = ((bf16[16,24,128]{2,1,0:T(8,128)(2,1)}), bf16[16,24,128]{2,1,0:T(8,128)(2,1)S(1)}, u32[]{:S(2)}, u32[]{:S(2)}) async-start(bf16[16,24,128]{2,1,0:T(8,128)(2,1)} %broadcast_in_dim.19), calls=%async_computation.2 | async-start | bytes 196608 | tf_op jit(solution)/shard_map/all_to_all | solution.py:28
  60.8 8.5 %copy-start.9 = (f32[2048]{0:T(1024)S(1)}, f32[2048]{0:T(1024)}, u32[]{:S(2)}) copy-start(f32[2048]{0:T(1024)} %param.25) | copy-start | bytes 24580
  71.5 4.9 %copy-start.6 = (f32[24,128]{1,0:T(8,128)}, f32[24,128]{1,0:T(8,128)S(1)}, u32[]{:S(2)}) copy-start(f32[24,128]{1,0:T(8,128)S(1)} %get-tuple-element.16.residual) | copy-start | bytes 36868
  71.6 10.1 %all-to-all-start.3 = ((bf16[8,16,128]{2,1,0:T(8,128)(2,1)}), bf16[8,16,128]{2,1,0:T(8,128)(2,1)S(1)}, u32[]{:S(2)}, u32[]{:S(2)}) async-start(bf16[8,16,128]{2,1,0:T(8,128)(2,1)} %bitcast.11), calls=%async_computation.3 | async-start | bytes 65536 | tf_op jit(solution)/shard_map/all_to_all | solution.py:28
  74.9 1.4 %copy-start.2 = (f32[3,8,128,128]{3,2,1,0:T(8,128)S(1)}, f32[3,8,128,128]{3,2,1,0:T(8,128)}, u32[]{:S(2)}) copy-start(f32[3,8,128,128]{3,2,1,0:T(8,128)} %state.1) | copy-start | bytes 4718596
  76.3 0.7 copy-start.5
  76.3 5.4 %copy-start.11 = (f32[8,128]{1,0:T(8,128)S(1)}, f32[8,128]{1,0:T(8,128)}, u32[]{:S(2)}) copy-start(f32[8,128]{1,0:T(8,128)} %gain.1) | copy-start | bytes 12292
  82.9 6.1 %copy-start.3 = (f32[3,24,128]{2,1,0:T(8,128)}, f32[3,24,128]{2,1,0:T(8,128)S(1)}, u32[]{:S(2)}) copy-start(f32[3,24,128]{2,1,0:T(8,128)S(1)} %get-tuple-element.19.vectors) | copy-start | bytes 110596
  83.6 13.6 %all-to-all-start.4 = ((bf16[16,24,128]{2,1,0:T(8,128)(2,1)}), bf16[16,24,128]{2,1,0:T(8,128)(2,1)}, u32[]{:S(2)}, u32[]{:S(2)}) async-start(bf16[16,24,128]{2,1,0:T(8,128)(2,1)} %broadcast_in_dim.20), calls=%async_computation.4 | async-start | bytes 196608 | tf_op jit(solution)/shard_map/all_to_all | solution.py:28
  88.6 17.7 %collective-permute-start.8 = (bf16[88,2048]{1,0:T(8,128)(2,1)}, bf16[88,2048]{1,0:T(8,128)(2,1)}, u32[]{:S(2)}, u32[]{:S(2)}) collective-permute-start(bf16[88,2048]{1,0:T(8,128)(2,1)} %d0.1), channel_id=1, source_target_pairs={{0,2},{2,4},{4,6},{6,0},{8,10},{10,12},{12,14},{14,8},{16,18},{18,... | collective-permute-start | bytes 1081352 | tf_op jit(solution)/shard_map/ppermute | solution.py:47
  89.0 17.4 %collective-permute-start.10 = (bf16[88,2048]{1,0:T(8,128)(2,1)}, bf16[88,2048]{1,0:T(8,128)(2,1)}, u32[]{:S(2)}, u32[]{:S(2)}) collective-permute-start(bf16[88,2048]{1,0:T(8,128)(2,1)} %collective-permute-done.9.d2), channel_id=1, source_target_pairs={{0,6},{2,0},{4,2},{6,4},{8,14},{10,8},{12,10},{14,12},{16,22},{18,... | collective-permute-start | bytes 1081352 | tf_op jit(solution)/shard_map/ppermute | solution.py:47
  97.2 0.7 copy-start.7
  99.9 11.7 %all-to-all-start.5 = ((bf16[16,24,128]{2,1,0:T(8,128)(2,1)}), bf16[16,24,128]{2,1,0:T(8,128)(2,1)S(1)}, u32[]{:S(2)}, u32[]{:S(2)}) async-start(bf16[16,24,128]{2,1,0:T(8,128)(2,1)} %broadcast_in_dim.21), calls=%async_computation.5 | async-start | bytes 196608 | tf_op jit(solution)/shard_map/all_to_all | solution.py:28
  103.3 8.3 %copy-start.10 = (f32[2048]{0:T(1024)S(1)}, f32[2048]{0:T(1024)}, u32[]{:S(2)}) copy-start(f32[2048]{0:T(1024)} %param.32) | copy-start | bytes 24580
  105.0 1.4 %copy-start = (bf16[3,176,2048]{2,1,0:T(8,128)(2,1)}, bf16[3,176,2048]{2,1,0:T(8,128)(2,1)S(1)}, u32[]{:S(2)}) copy-start(bf16[3,176,2048]{2,1,0:T(8,128)(2,1)S(1)} %shard_map.193.w_held) | copy-start | bytes 6488068
  111.6 1.6 %copy-start.1 = (bf16[3,176,2048]{2,1,0:T(8,128)(2,1)S(1)}, bf16[3,176,2048]{2,1,0:T(8,128)(2,1)}, u32[]{:S(2)}) copy-start(bf16[3,176,2048]{2,1,0:T(8,128)(2,1)} %copy-done) | copy-start | bytes 6488068
  113.3 9.0 %copy-start.4 = (f32[3,24,128]{2,1,0:T(8,128)S(1)}, f32[3,24,128]{2,1,0:T(8,128)}, u32[]{:S(2)}) copy-start(f32[3,24,128]{2,1,0:T(8,128)} %copy-done.3) | copy-start | bytes 110596
  116.4 1.3 collective-permute-start.11
  118.4 14.4 %all-to-all-start.6 = ((bf16[32,24,128]{2,1,0:T(8,128)(2,1)}), bf16[32,24,128]{2,1,0:T(8,128)(2,1)S(1)}, u32[]{:S(2)}, u32[]{:S(2)}) async-start(bf16[32,24,128]{2,1,0:T(8,128)(2,1)} %bitcast.16), calls=%async_computation.6 | async-start | bytes 393216 | tf_op jit(solution)/shard_map/all_to_all | solution.py:28

commit v4 on v3

--- a/solution.py
+++ b/solution.py
@@ -55,9 +55,19 @@
     return exchange(copies(x, Z_COUNT * TP_COUNT), ("kv", "tp"), groups)
 
 
+def div(v, d):
+    if d & (d - 1) == 0:
+        return v >> (d.bit_length() - 1)
+    return (v * (65536 // d + 1)) >> 16
+
+
+def rem(v, d):
+    return v & (d - 1) if d & (d - 1) == 0 else v - div(v, d) * d
+
+
 def place():
     kv = lax.axis_index("kv")
-    return lax.div(kv, Y_COUNT), lax.rem(kv, Y_COUNT), lax.axis_index("tp")
+    return div(kv, Y_COUNT), rem(kv, Y_COUNT), lax.axis_index("tp")
 
 
 def iota(shape, axis):
@@ -92,16 +102,19 @@
 VMEM_LIMIT = 24 * 1024 * 1024
 
 
-def first_block(
-    own, other, gain, w_gate, w_up, w_down, mine, theirs, slab, xt, low, gate_w, up_w, down_w, sems
-):
-    z, y, core = place()
+def load_first(w_gate, w_up, w_down, gate, upper, down, sems):
     moves = [
         pltpu.make_async_copy(src, dst, sems.at[k])
-        for k, (src, dst) in enumerate(((w_gate, gate_w), (w_up, up_w), (w_down, down_w)))
+        for k, (src, dst) in enumerate(((w_gate, gate), (w_up, upper), (w_down, down)))
     ]
     for move in moves:
         move.start()
+    for move in moves:
+        move.wait()
+
+
+def first_block(own, other, gain, w_gate, w_up, w_down, mine, theirs, slab, xt, low):
+    z, y, core = place()
     cols = own.shape[1]
     for kv in range(KV_COUNT):
         base = kv * TP_COUNT * cols
@@ -119,22 +132,19 @@
         part = f32(xt[c * LANES : (c + 1) * LANES, :])
         normed.append(bf(part * scale * gains[:, c : c + 1]))
     normed = jnp.concatenate(normed, axis=0)
-    moves[0].wait()
-    gate = matmul(gate_w[...], normed, NN)
-    moves[1].wait()
-    upper = matmul(up_w[...], normed, NN)
+    gate = matmul(w_gate[...], normed, NN)
+    upper = matmul(w_up[...], normed, NN)
     mid = bf(jax.nn.silu(gate) * upper)
     count = slab.shape[0]
     seqs = count // Z_COUNT
     new, old = iota((rows, rows), 0), iota((rows, rows), 1)
     wanted = (
-        lax.div(lax.rem(new, count), seqs) * (Y_COUNT * seqs)
-        + lax.div(new, count) * seqs
-        + lax.rem(new, seqs)
+        div(rem(new, count), seqs) * (Y_COUNT * seqs)
+        + div(new, count) * seqs
+        + rem(new, seqs)
     )
     mid = bf(matmul(hot(old == wanted), mid, NT))
-    moves[2].wait()
-    low[...] = matmul(mid, down_w[...], NN)
+    low[...] = matmul(mid, w_down[...], NN)
     for k in range(Z_COUNT):
         at = pl.multiple_of((k * TP_COUNT + core) * LANES, LANES)
         to = pl.multiple_of((k * TP_COUNT + 1 - core) * LANES, LANES)
@@ -142,7 +152,7 @@
         theirs[k] = bf(low[:, pl.ds(to, LANES)])
     at = pl.multiple_of((z * TP_COUNT + core) * LANES, LANES)
     new, old = iota((count, rows), 0), iota((count, rows), 1)
-    pick = hot(old == lax.div(new, seqs) * (Y_COUNT * seqs) + y * seqs + lax.rem(new, seqs))
+    pick = hot(old == div(new, seqs) * (Y_COUNT * seqs) + y * seqs + rem(new, seqs))
     slab[...] = matmul(pick, xt[pl.ds(at, LANES), :], NT)
 
 
@@ -150,7 +160,7 @@
     _, y, _ = place()
     moves = []
     for k, part in enumerate((a0, a1, a2, a3)):
-        to = lax.rem(y - k + Y_COUNT, Y_COUNT)
+        to = rem(y - k + Y_COUNT, Y_COUNT)
         moves.append(
             pltpu.make_async_copy(
                 part.at[pl.ds(LANES, w_mix.shape[1])], w_mix.at[to], sems.at[k]
@@ -178,6 +188,26 @@
         move.start()
     for move in moves:
         move.wait()
+
+
+def pack_early(query, forget, inputs, out_gate, mix, out, *scratch):
+    *held, sems = scratch
+    moves = [
+        pltpu.make_async_copy(w, held[k], sems.at[k])
+        for k, w in enumerate((query, forget, inputs, out_gate))
+    ]
+    rest = out.shape[0] - LANES
+    moves.append(pltpu.make_async_copy(mix, out.at[pl.ds(LANES, rest)], sems.at[4]))
+    for move in moves:
+        move.start()
+    heads, per, _ = query.shape
+    for k in range(4):
+        moves[k].wait()
+        for h in range(0, heads, 4):
+            block = jnp.concatenate([f32(held[k][h + n]) for n in range(4)], axis=0)
+            at = (k * heads + h) * per
+            out[at : at + 4 * per, :] = bf(block)
+    moves[4].wait()
 
 
 def flipped(x, out):
@@ -212,16 +242,16 @@
     stacked = jnp.concatenate(flats, axis=0)
     shape = (Z_COUNT * 16, Y_COUNT * count)
     new, old = iota(shape, 0), iota(shape, 1)
-    row = lax.div(new, 16) * seqs + lax.div(lax.rem(new, 16), Y_COUNT)
-    wanted = lax.rem(y - lax.rem(new, Y_COUNT) + Y_COUNT, Y_COUNT) * count + row
-    real = lax.div(lax.rem(new, 16), Y_COUNT) < seqs
+    row = div(new, 16) * seqs + div(rem(new, 16), Y_COUNT)
+    wanted = rem(y - rem(new, Y_COUNT) + Y_COUNT, Y_COUNT) * count + row
+    real = div(rem(new, 16), Y_COUNT) < seqs
     channels[...] = bf(matmul(hot((old == wanted) & real), stacked, NN))
     at = pl.multiple_of(z * TP_COUNT * LANES, 2 * LANES)
     both = rows[:, pl.ds(at, TP_COUNT * LANES)]
     shape = (TP_COUNT * LANES, LANES)
     old, new = iota(shape, 0), iota(shape, 1)
     each = LANES // Y_COUNT
-    wanted = lax.div(new, each) * (TP_COUNT * each) + core * each + lax.rem(new, each)
+    wanted = div(new, each) * (TP_COUNT * each) + core * each + rem(new, each)
     residual[...] = matmul(both, hot(old == wanted), NN)
 
 
@@ -229,16 +259,16 @@
     per = LANES // KV_COUNT
     shape = (LANES, Z_COUNT * 16)
     channel, source = iota(shape, 0), iota(shape, 1)
-    kv = lax.div(channel, per)
-    wanted = lax.div(kv, Y_COUNT) * 16 + k * Y_COUNT + lax.rem(kv, Y_COUNT)
+    kv = div(channel, per)
+    wanted = div(kv, Y_COUNT) * 16 + k * Y_COUNT + rem(kv, Y_COUNT)
     wide = matmul(hot(source == wanted), arrived, NN)
     shape = (LANES, LANES)
-    own = lax.rem(iota(shape, 0), per) == lax.rem(iota(shape, 1), per)
+    own = rem(iota(shape, 0), per) == rem(iota(shape, 1), per)
     wide = bf(jnp.where(own, wide, 0.0))
     shape = (LANES, KV_COUNT)
-    gather = hot(lax.div(iota(shape, 0), per) == iota(shape, 1))
+    gather = hot(div(iota(shape, 0), per) == iota(shape, 1))
     shape = (KV_COUNT, LANES)
-    gather_rows = hot(lax.div(iota(shape, 1), per) == iota(shape, 0))
+    gather_rows = hot(div(iota(shape, 1), per) == iota(shape, 0))
     return matmul(wide, gather, NN), matmul(gather_rows, wide, NT)
 
 
@@ -289,9 +319,9 @@
     total = Z_COUNT * heads_rows
     shape = (total, total)
     new, old = iota(shape, 0), iota(shape, 1)
-    row = lax.rem(new, slab_rows)
+    row = rem(new, slab_rows)
     wanted = (
-        lax.div(row, seqs) * heads_rows + lax.rem(row, seqs) * heads + lax.div(new, slab_rows)
+        div(row, seqs) * heads_rows + rem(row, seqs) * heads + div(new, slab_rows)
     )
     order = hot(old == wanted)
     for t in range(TP_COUNT):
@@ -310,15 +340,15 @@
     a, b = (0, 1) if not transposed else (1, 0)
     old, new = iota(shape, a), iota(shape, b)
     wanted = (
-        lax.rem(lax.div(new, each), TP_COUNT) * LANES
-        + lax.div(new, TP_COUNT * each) * each
-        + lax.rem(new, each)
+        rem(div(new, each), TP_COUNT) * LANES
+        + div(new, TP_COUNT * each) * each
+        + rem(new, each)
     )
     return hot(old == wanted)
 
 
 def second_block(
-    tiles, gain, after, w_held, t3, d0, d1, d2, d3, mine, theirs, rows, w_last, w_down, sems
+    tiles, gain, after, w_held, t3, d0, d1, d2, d3, out, rows, w_last, w_down, sems
 ):
     z, _, core = place()
     moves = [
@@ -331,9 +361,14 @@
         move.start()
     order = lane_order(False)
     wide = TP_COUNT * LANES
+    count = rows.shape[0]
+    pairs = [
+        jnp.concatenate([tiles[k * TP_COUNT], tiles[k * TP_COUNT + 1]], axis=1)
+        for k in range(Z_COUNT)
+    ]
+    ordered = bf(matmul(jnp.concatenate(pairs, axis=0), order, NN))
     for k in range(Z_COUNT):
-        both = jnp.concatenate([tiles[k * TP_COUNT], tiles[k * TP_COUNT + 1]], axis=1)
-        rows[:, k * wide : (k + 1) * wide] = bf(matmul(both, order, NN))
+        rows[:, k * wide : (k + 1) * wide] = ordered[k * count : (k + 1) * count]
     normed = normed_of(rows, gain)
     hidden = w_down.shape[1]
     mids = []
@@ -349,40 +384,52 @@
     for k, move in enumerate(moves):
         move.wait()
         total += matmul(mids[k], w_down[k], NN)
-    total = bf(0.5 * total)
-    back = lane_order(True)
-    for k in range(Z_COUNT):
-        split = matmul(total[:, k * wide : (k + 1) * wide], back, NN)
-        low, high = split[:, :LANES], split[:, LANES:]
-        kept = jnp.where(core == 0, low, high)
-        home = jnp.where(z == k, f32(after[...]), 0.0)
-        mine[k] = kept + home
-        theirs[k] = bf(jnp.where(core == 0, high, low))
+    each = LANES // Y_COUNT
+    total = 0.5 * total
+    spare = jnp.zeros((each - count, LANES), jnp.float32)
+
+    def spread(block):
+        padded = jnp.concatenate([block, spare], axis=0)
+        return jnp.concatenate([padded] * Y_COUNT, axis=0).T
+
+    group = div(iota((8, LANES), 1), each)
+    home = spread(f32(after[...]))
+    for k in range(Z_COUNT * TP_COUNT):
+        block = spread(total[:, k * LANES : (k + 1) * LANES])
+        for n in range(Y_COUNT):
+            where = rem(k, TP_COUNT) * Y_COUNT + n
+            own_y, t = div(where, TP_COUNT), rem(where, TP_COUNT)
+            packed = jnp.zeros((8, LANES), jnp.float32)
+            extra = jnp.zeros((8, LANES), jnp.float32)
+            for g in range(Y_COUNT):
+                at, to = n * each + g * 8, own_y * each + g * 8
+                packed = jnp.where(group == g, block[at : at + 8], packed)
+                extra = jnp.where(group == g, home[to : to + 8], extra)
+            own = (z == div(k, TP_COUNT)) & (core == t)
+            packed = packed + jnp.where(own, extra, 0.0)
+            out[(div(k, TP_COUNT) * Y_COUNT + own_y) * TP_COUNT + t] = bf(packed)
 
 
 def finish(arrived, out):
-    _, y, _ = place()
-    slab_rows = arrived.shape[1]
     cols, rows = out.shape
+    slab_rows = rows // Y_COUNT
     seqs = slab_rows // Z_COUNT
+    lanes_each = LANES // Y_COUNT
     parts = []
     for k in range(Y_COUNT):
-        part = f32(arrived[k])
-        for n in range(1, Z_COUNT):
-            part += f32(arrived[n * Y_COUNT + k])
+        part = jnp.zeros(arrived.shape[1:], jnp.float32)
+        for n in range(Z_COUNT):
+            for t in range(TP_COUNT):
+                part += f32(arrived[(n * Y_COUNT + k) * TP_COUNT + t])
         parts.append(bf(part))
-    result = jnp.concatenate(parts, axis=0)
-    shape = (cols, LANES)
-    pick = hot(iota(shape, 1) == y * cols + iota(shape, 0))
-    picked = bf(matmul(pick, result, NT))
-    shape = (rows, rows)
+    sums = jnp.concatenate(parts, axis=1)
+    shape = (Y_COUNT * LANES, rows)
     old, new = iota(shape, 0), iota(shape, 1)
-    wanted = (
-        lax.rem(lax.div(new, seqs), Y_COUNT) * slab_rows
-        + lax.div(new, seqs * Y_COUNT) * seqs
-        + lax.rem(new, seqs)
-    )
-    out[...] = bf(matmul(picked, hot(old == wanted), NN))
+    y = rem(div(new, seqs), Y_COUNT)
+    row = div(new, seqs * Y_COUNT) * seqs + rem(new, seqs)
+    for g in range(cols // 8):
+        pick = hot(old == y * LANES + g * lanes_each + row)
+        out[g * 8 : (g + 1) * 8, :] = bf(matmul(sums, pick, NN))
 
 
 def shards(
@@ -413,12 +460,31 @@
     dma = pltpu.SemaphoreType.DMA
 
     kinds = [jnp.transpose(w, (1, 2, 0)) for w in (w_query, w_forget, w_input, w_outgate)]
-    early = jnp.concatenate([*(k.reshape(-1, width) for k in kinds), w_mix_out.T], axis=0)
+    (early,) = local(
+        pack_early,
+        [((LANES + own_cols, width), half16)],
+        *kinds,
+        w_mix_out.T,
+        scratch=(*[pltpu.VMEM(k.shape, half16) for k in kinds], dma((5,))),
+        outside=(0, 1, 2, 3, 4),
+        held_out=True,
+    )
     late_top = jnp.concatenate([w_gate_two.T, w_up_two.T], axis=0)
 
     (floor_t,) = local(flipped, [((LANES, heads), half32)], forget_floor)
 
     own = exchange(copies(hidden_in.T, KV_COUNT), "kv")
+    first_w = local(
+        load_first,
+        [((hidden, width), half16)] * 3,
+        w_gate_one.T,
+        w_up_one.T,
+        w_down_one,
+        scratch=(dma((3,)),),
+        outside=(0, 1, 2),
+        held_out=True,
+        vmem=True,
+    )
     other = swap_cores(own)
     mine, theirs, slab = local(
         first_block,
@@ -430,19 +496,8 @@
         own,
         other,
         ffn_gain_one.reshape(-1, LANES),
-        w_gate_one.T,
-        w_up_one.T,
-        w_down_one,
-        scratch=(
-            pltpu.VMEM((width, rows), half16),
-            pltpu.VMEM((rows, width), half32),
-            pltpu.VMEM((hidden, width), half16),
-            pltpu.VMEM((hidden, width), half16),
-            pltpu.VMEM((hidden, width), half16),
-            dma((3,)),
-        ),
-        outside=(3, 4, 5),
-        held_out=True,
+        *first_w,
+        scratch=(pltpu.VMEM((width, rows), half16), pltpu.VMEM((rows, width), half32)),
     )
     both = bf(mine + f32(swap_cores(theirs)))
     summed = exchange(both.reshape(KV_COUNT, slab_rows, LANES), "kv")
@@ -546,9 +601,9 @@
         outside=(0, 1, 2),
         vmem=True,
     )
-    mine, theirs = local(
+    (messages,) = local(
         second_block,
-        [((Z_COUNT, slab_rows, LANES), half32), ((Z_COUNT, slab_rows, LANES), half16)],
+        [((KV_COUNT * TP_COUNT, 8, LANES), half16)],
         mix_tiles,
         ffn_gain_two.reshape(1, -1),
         after_mix,
@@ -563,9 +618,7 @@
         ),
         outside=(4, 5, 6, 7, 8),
     )
-    both = bf(mine + f32(swap_cores(theirs)))
-    tiles = jnp.broadcast_to(both[:, None], (Z_COUNT, Y_COUNT, slab_rows, LANES))
-    arrived = exchange(tiles.reshape(KV_COUNT, slab_rows, LANES), "kv")
+    arrived = exchange(messages, ("kv", "tp"))
     (result,) = local(finish, [((own_cols, rows), half16)], arrived)
     return (result.T, new_state)
 

time: 135 us -> 132 us (0.978)
  blocking collectives: 0 us -> 23.1 us
  starting transfers between devices: 51.7 us -> 41 us
  waiting for transfers between devices: 47.3 us -> 38.1 us
  local copies, waits for them, and re-layouts: 15.1 us -> 7.64 us
  Pallas kernels: 17.8 us -> 19.2 us
    all_to_all x0 -> x1, blocking collectives: none -> 23.1 us  [exchange(): lax.all_to_all(tiles, axis, split_axis=0, concat_axis=0, axis_index_group...]
    all_to_all x7 -> x6, starting transfers between devices: 37 us -> 24.8 us  [exchange(): lax.all_to_all(tiles, axis, split_axis=0, concat_axis=0, axis_index_group...]
    all_to_all x7 -> x6, waiting for transfers between devices: 32.9 us -> 27 us  [exchange(): lax.all_to_all(tiles, axis, split_axis=0, concat_axis=0, axis_index_group...]
    unnamed x40 -> x26, local copies, waits for them, and re-layouts: 8.34 us -> 4.93 us
    ppermute x9, starting transfers between devices: 11.7 us -> 13.7 us  [shift_y(): return lax.ppermute(x, 'kv', pairs)]
    reshape x4 -> x0, local copies, waits for them, and re-layouts: 1.95 us -> none  [shards(): k.reshape(-1, width)]
    ppermute x3 -> x2, waiting for transfers between devices: 1.71 us -> 0.01 us  [swap_cores(): return lax.ppermute(x, 'tp', [(0, 1), (1, 0)])]
    ppermute x9, waiting for transfers between devices: 12.7 us -> 11.1 us  [shift_y(): return lax.ppermute(x, 'kv', pairs)]
  transfers between devices with their start and end apart: 19 -> 17, of which waited for: 10 -> 8; matrix products, arithmetic and copies ran while one was open for 6% -> 2% of each run, Pallas kernels for 10% -> 11%
where the time goes in v4:
time: 132 us; the launch traced here: 131 us
  starting transfers between devices  41 us (31%)
  waiting for transfers between devices  38.1 us (29%)
  blocking collectives  23.1 us (18%)
  Pallas kernels  19.2 us (15%)
  local copies, waits for them, and re-layouts  7.64 us (6%)
    all_to_all x6, waiting for transfers between devices, exchange(): lax.all_to_all(tiles, axis, split_axis=0, concat_axis=0, axis_index_group...  27 us
    all_to_all x6, starting transfers between devices, exchange(): lax.all_to_all(tiles, axis, split_axis=0, concat_axis=0, axis_index_group...  24.8 us
    all_to_all x1, blocking collectives, exchange(): lax.all_to_all(tiles, axis, split_axis=0, concat_axis=0, axis_index_group...  23.1 us
    pallas_call x13, Pallas kernels, local(): pl.pallas_call(body, out_shape=shapes, in_specs=specs, out_specs=[held] *...  16.7 us
    ppermute x9, starting transfers between devices, shift_y(): return lax.ppermute(x, 'kv', pairs)  13.7 us
    ppermute x9, waiting for transfers between devices, shift_y(): return lax.ppermute(x, 'kv', pairs)  11.1 us
    unnamed x26, local copies, waits for them, and re-layouts  4.93 us
    broadcast_in_dim x4, local copies, waits for them, and re-layouts, copies(): return jnp.broadcast_to(x, (count, *x.shape))  2.71 us
  transfers between devices with their start and end apart: 17, of which 8 were waited for; matrix products, arithmetic and copies ran while one was open for 2% of the time, Pallas kernels for 11%

profile of v4, /device:TPU:1, one launch (start us, length us, event | category | flops | bytes accessed | tf_op | source)
XLA Modules:
  0.0 130.8 jit_solution(3614902532547278032)
XLA Ops:
  0.6 0.7 broadcast_in_dim.12
  1.4 23.1 %all_to_all.35.own = bf16[32,32,96]{2,1,0:T(8,128)(2,1)S(1)} all-to-all(bf16[32,32,96]{2,1,0:T(8,128)(2,1)S(1)} %broadcast_in_dim.12), channel_id=1, replica_groups=mesh['dp'=4,'kv'=32,'tp'=2] {'kv'}, dimensions={0} | all-to-all | bytes 393216 | tf_op jit(solution)/shard_map/all_to_all | solution.py:28
  24.5 2.5 %collective-permute-start = (bf16[32,32,96]{2,1,0:T(8,128)(2,1)S(1)}, bf16[32,32,96]{2,1,0:T(8,128)(2,1)S(1)}, u32[]{:S(2)}, u32[]{:S(2)}) collective-permute-start(bf16[32,32,96]{2,1,0:T(8,128)(2,1)S(1)} %all_to_all.35.own), channel_id=1, source_target_pairs={{0,1},{1,0},{2,3},{3,2},{4,5},{5,4},{6,7},{7,6},{8,9},{9,8},{10,11... | collective-permute-start | bytes 589832 | tf_op jit(solution)/shard_map/ppermute | solution.py:38
  27.0 1.2 shard_map.187.refs_0_.a0
  28.2 0.0 copy-start.2
  28.2 0.0 copy-start.11
  28.2 0.0 copy-start.12
  28.2 0.1 collective-permute-start.2
  28.3 1.5 %shard_map.185 = (bf16[88,2048]{1,0:T(8,128)(2,1)S(1)}, bf16[88,2048]{1,0:T(8,128)(2,1)S(1)}, bf16[88,2048]{1,0:T(8,128)(2,1)S(1)}) custom-call(bf16[88,2048]{1,0:T(8,128)(2,1)} %bitcast.21, bf16[88,2048]{1,0:T(8,128)(2,1)} %bitcast.22, bf16[88,2048]{1,0:T(8,128)(2,1)} %w_down.1), custom_call_target="tpu_custom_call" | custom-call | flops 1048576 | bytes 1081344 | tf_op jit(solution)/shard_map/pallas_call | solution.py:91
  29.8 0.0 collective-permute-done.other
  29.9 1.4 %shard_map.186 = (f32[8,96,128]{2,1,0:T(8,128)S(1)}, bf16[8,96,128]{2,1,0:T(8,128)(2,1)S(1)}, f32[24,128]{1,0:T(8,128)S(1)}) custom-call(bf16[32,32,96]{2,1,0:T(8,128)(2,1)S(1)} %all_to_all.35.own, bf16[32,32,96]{2,1,0:T(8,128)(2,1)S(1)} %collective-permute-done.other, f32[16,128]{1,0:T(8,128)S(1)} %bitcast.18, ...), custom_call_target="tpu_custom_call" | custom-call | flops 1048576 | bytes 1482752 | tf_op jit(solution)/shard_map/pallas_call | solution.py:91
  31.3 0.0 copy-start.4
  31.3 0.1 collective-permute-start.1
  31.5 0.1 pad_maximum_fusion.refs_0_
  31.5 2.7 %collective-permute-start.6 = (bf16[176,2048]{1,0:T(8,128)(2,1)S(1)}, bf16[176,2048]{1,0:T(8,128)(2,1)}, u32[]{:S(2)}, u32[]{:S(2)}) collective-permute-start(bf16[176,2048]{1,0:T(8,128)(2,1)S(1)} %pad_maximum_fusion.refs_0_), channel_id=1, source_target_pairs={{0,6},{2,0},{4,2},{6,4},{8,14},{10,8},{12,10},{14,12},{16,22},{18,... | collective-permute-start | bytes 2162696 | tf_op jit(solution)/shard_map/ppermute | solution.py:47
  34.2 0.0 collective-permute-done.1
  34.2 0.7 add_convert_fusion
  35.0 3.9 %all-to-all-start.1 = ((bf16[32,24,128]{2,1,0:T(8,128)(2,1)}), bf16[32,24,128]{2,1,0:T(8,128)(2,1)S(1)}, u32[]{:S(2)}, u32[]{:S(2)}) async-start(bf16[32,24,128]{2,1,0:T(8,128)(2,1)} %bitcast.4), calls=%async_computation.1 | async-start | bytes 393216 | tf_op jit(solution)/shard_map/all_to_all | solution.py:28
  38.8 7.8 %collective-permute-done.2.refs_1_.a1 = bf16[160,2048]{1,0:T(8,128)(2,1)S(1)} collective-permute-done((bf16[160,2048]{1,0:T(8,128)(2,1)S(1)}, bf16[160,2048]{1,0:T(8,128)(2,1)S(1)}, u32[]{:S(2)}, u32[]{:S(2)}) %collective-permute-start.2) | collective-permute-done | bytes 655392 | tf_op jit(solution)/shard_map/ppermute | solution.py:47
  46.7 0.0 collective-permute-start.3
  46.7 2.7 %collective-permute-start.4 = (bf16[160,2048]{1,0:T(8,128)(2,1)S(1)}, bf16[160,2048]{1,0:T(8,128)(2,1)}, u32[]{:S(2)}, u32[]{:S(2)}) collective-permute-start(bf16[160,2048]{1,0:T(8,128)(2,1)S(1)} %shard_map.187.refs_0_.a0), channel_id=1, source_target_pairs={{0,6},{2,0},{4,2},{6,4},{8,14},{10,8},{12,10},{14,12},{16,22},{18,... | collective-permute-start | bytes 1966088 | tf_op jit(solution)/shard_map/ppermute | solution.py:47
  49.3 0.0 collective-permute-start.5
  49.4 2.7 %collective-permute-start.9 = (bf16[88,2048]{1,0:T(8,128)(2,1)S(1)}, bf16[88,2048]{1,0:T(8,128)(2,1)}, u32[]{:S(2)}, u32[]{:S(2)}) collective-permute-start(bf16[88,2048]{1,0:T(8,128)(2,1)S(1)} %copy-done.4), channel_id=1, source_target_pairs={{0,6},{2,0},{4,2},{6,4},{8,14},{10,8},{12,10},{14,12},{16,22},{18,... | collective-permute-start | bytes 1081352 | tf_op jit(solution)/shard_map/ppermute | solution.py:47
  52.0 0.0 collective-permute-done.6.refs_2_
  52.0 2.9 %collective-permute-start.7 = (bf16[176,2048]{1,0:T(8,128)(2,1)}, bf16[176,2048]{1,0:T(8,128)(2,1)}, u32[]{:S(2)}, u32[]{:S(2)}) collective-permute-start(bf16[176,2048]{1,0:T(8,128)(2,1)} %collective-permute-done.6.refs_2_), channel_id=1, source_target_pairs={{0,6},{2,0},{4,2},{6,4},{8,14},{10,8},{12,10},{14,12},{16,22},{18,... | collective-permute-start | bytes 2162696 | tf_op jit(solution)/shard_map/ppermute | solution.py:47
  54.9 0.0 all-to-all-done.1
  55.0 0.6 broadcast_in_dim.13
  55.6 5.4 %all-to-all-start.2 = ((bf16[16,24,128]{2,1,0:T(8,128)(2,1)}), bf16[16,24,128]{2,1,0:T(8,128)(2,1)S(1)}, u32[]{:S(2)}, u32[]{:S(2)}) async-start(bf16[16,24,128]{2,1,0:T(8,128)(2,1)} %broadcast_in_dim.13), calls=%async_computation.2 | async-start | bytes 196608 | tf_op jit(solution)/shard_map/all_to_all | solution.py:28
  61.0 0.0 copy-start.7
  61.0 1.8 %collective-permute-done.3.refs_2_.a2 = bf16[160,2048]{1,0:T(8,128)(2,1)} collective-permute-done((bf16[160,2048]{1,0:T(8,128)(2,1)S(1)}, bf16[160,2048]{1,0:T(8,128)(2,1)}, u32[]{:S(2)}, u32[]{:S(2)}) %collective-permute-start.3) | collective-permute-done | bytes 655392 | tf_op jit(solution)/shard_map/ppermute | solution.py:47
  62.8 1.4 %shard_map.188.w_held = bf16[3,128,2048]{2,1,0:T(8,128)(2,1)S(1)} custom-call(bf16[160,2048]{1,0:T(8,128)(2,1)} %copy-done.2, bf16[160,2048]{1,0:T(8,128)(2,1)} %copy-done.10, bf16[160,2048]{1,0:T(8,128)(2,1)} %collective-permute-done.3.refs_2_.a2), custom_call_target="tpu_custom_call" | custom-call | flops 1048576 | bytes 1966080 | tf_op jit(solution)/shard_map/pallas_call | solution.py:91
  64.2 1.4 %collective-permute-done.4.a3 = bf16[160,2048]{1,0:T(8,128)(2,1)} collective-permute-done((bf16[160,2048]{1,0:T(8,128)(2,1)S(1)}, bf16[160,2048]{1,0:T(8,128)(2,1)}, u32[]{:S(2)}, u32[]{:S(2)}) %collective-permute-start.4) | collective-permute-done | bytes 655392 | tf_op jit(solution)/shard_map/ppermute | solution.py:47
  65.6 3.9 %all-to-all-done.2.tiles = bf16[16,24,128]{2,1,0:T(8,128)(2,1)S(1)} async-done(((bf16[16,24,128]{2,1,0:T(8,128)(2,1)}), bf16[16,24,128]{2,1,0:T(8,128)(2,1)S(1)}, u32[]{:S(2)}, u32[]{:S(2)}) %all-to-all-start.2) | async-done | bytes 98336 | tf_op jit(solution)/shard_map/all_to_all | solution.py:28
  69.5 2.2 %shard_map.189 = (bf16[128,128]{1,0:T(8,128)(2,1)}, f32[24,128]{1,0:T(8,128)S(1)}) custom-call(bf16[16,24,128]{2,1,0:T(8,128)(2,1)S(1)} %all-to-all-done.2.tiles, f32[1,2048]{1,0:T(1,128)S(1)} %bitcast.19, bf16[3,128,2048]{2,1,0:T(8,128)(2,1)S(1)} %shard_map.188.w_held, bf16[160,2048]{1,0:T(8,128)(2,1)} %collective-permute-done.4.a3), custom_call_target="tpu_custom_call" | custom-call | flops 1048576 | bytes 2334720 | tf_op jit(solution)/shard_map/pallas_call | solution.py:91
  71.7 3.3 %all-to-all-start.3 = ((bf16[8,16,128]{2,1,0:T(8,128)(2,1)}), bf16[8,16,128]{2,1,0:T(8,128)(2,1)S(1)}, u32[]{:S(2)}, u32[]{:S(2)}) async-start(bf16[8,16,128]{2,1,0:T(8,128)(2,1)} %bitcast.11), calls=%async_computation.3 | async-start | bytes 65536 | tf_op jit(solution)/shard_map/all_to_all | solution.py:28
  75.1 0.0 copy-start.3
  75.1 1.4 %copy-done.3 = f32[3,8,128,128]{3,2,1,0:T(8,128)S(1)} copy-done((f32[3,8,128,128]{3,2,1,0:T(8,128)S(1)}, f32[3,8,128,128]{3,2,1,0:T(8,128)}, u32[]{:S(2)}) %copy-start.3) | copy-done | bytes 1572888
  76.5 0.1 shard_map.191.state
  76.6 0.6 copy-done.5
  77.2 0.1 shard_map.190.floor_t
  77.3 4.6 %all-to-all-done.3 = bf16[8,16,128]{2,1,0:T(8,128)(2,1)S(1)} async-done(((bf16[8,16,128]{2,1,0:T(8,128)(2,1)}), bf16[8,16,128]{2,1,0:T(8,128)(2,1)S(1)}, u32[]{:S(2)}, u32[]{:S(2)}) %all-to-all-start.3) | async-done | bytes 32800 | tf_op jit(solution)/shard_map/all_to_all | solution.py:28
  81.9 1.2 shard_map.192
  83.1 0.7 broadcast_in_dim.14
  83.7 4.4 %all-to-all-start.4 = ((bf16[16,24,128]{2,1,0:T(8,128)(2,1)}), bf16[16,24,128]{2,1,0:T(8,128)(2,1)S(1)}, u32[]{:S(2)}, u32[]{:S(2)}) async-start(bf16[16,24,128]{2,1,0:T(8,128)(2,1)} %broadcast_in_dim.14), calls=%async_computation.4 | async-start | bytes 196608 | tf_op jit(solution)/shard_map/all_to_all | solution.py:28
  88.1 0.0 collective-permute-start.8
  88.2 0.0 collective-permute-done.9.d2
  88.2 2.7 %collective-permute-start.10 = (bf16[88,2048]{1,0:T(8,128)(2,1)}, bf16[88,2048]{1,0:T(8,128)(2,1)}, u32[]{:S(2)}, u32[]{:S(2)}) collective-permute-start(bf16[88,2048]{1,0:T(8,128)(2,1)} %collective-permute-done.9.d2), channel_id=1, source_target_pairs={{0,6},{2,0},{4,2},{6,4},{8,14},{10,8},{12,10},{14,12},{16,22},{18,... | collective-permute-start | bytes 1081352 | tf_op jit(solution)/shard_map/ppermute | solution.py:47
  90.8 1.1 shard_map.193.w_mix
  92.0 4.7 %all-to-all-done.4.tiles = bf16[16,24,128]{2,1,0:T(8,128)(2,1)S(1)} async-done(((bf16[16,24,128]{2,1,0:T(8,128)(2,1)}), bf16[16,24,128]{2,1,0:T(8,128)(2,1)S(1)}, u32[]{:S(2)}, u32[]{:S(2)}) %all-to-all-start.4) | async-done | bytes 98336 | tf_op jit(solution)/shard_map/all_to_all | solution.py:28
  96.6 0.4 shard_map.194.after
  97.0 0.7 broadcast_in_dim.15
  97.7 3.4 %all-to-all-start.5 = ((bf16[16,24,128]{2,1,0:T(8,128)(2,1)}), bf16[16,24,128]{2,1,0:T(8,128)(2,1)S(1)}, u32[]{:S(2)}, u32[]{:S(2)}) async-start(bf16[16,24,128]{2,1,0:T(8,128)(2,1)} %broadcast_in_dim.15), calls=%async_computation.5 | async-start | bytes 196608 | tf_op jit(solution)/shard_map/all_to_all | solution.py:28
  101.1 0.0 copy-start.8
  101.1 1.6 %shard_map.195.w_held = bf16[3,176,2048]{2,1,0:T(8,128)(2,1)S(1)} custom-call(bf16[176,2048]{1,0:T(8,128)(2,1)S(1)} %pad_maximum_fusion.refs_0_, bf16[176,2048]{1,0:T(8,128)(2,1)} %collective-permute-done.5.refs_1_, bf16[176,2048]{1,0:T(8,128)(2,1)} %collective-permute-done.6.refs_2_), custom_call_target="tpu_custom_call" | custom-call | flops 1048576 | bytes 2162688 | tf_op jit(solution)/shard_map/pallas_call | solution.py:91
  102.8 1.3 copy-done
  104.1 0.0 collective-permute-done.8.d1
  104.1 0.0 collective-permute-done.10.d3
  104.1 5.3 %all-to-all-done.5.tiles = bf16[16,24,128]{2,1,0:T(8,128)(2,1)S(1)} async-done(((bf16[16,24,128]{2,1,0:T(8,128)(2,1)}), bf16[16,24,128]{2,1,0:T(8,128)(2,1)S(1)}, u32[]{:S(2)}, u32[]{:S(2)}) %all-to-all-start.5) | async-done | bytes 98336 | tf_op jit(solution)/shard_map/all_to_all | solution.py:28
  109.5 1.6 %copy-done.1 = bf16[3,176,2048]{2,1,0:T(8,128)(2,1)S(1)} copy-done((bf16[3,176,2048]{2,1,0:T(8,128)(2,1)S(1)}, bf16[3,176,2048]{2,1,0:T(8,128)(2,1)}, u32[]{:S(2)}) %copy-start.1) | copy-done | bytes 2162712
  111.1 3.5 %shard_map.196 = bf16[64,8,128]{2,1,0:T(8,128)(2,1)} custom-call(bf16[16,24,128]{2,1,0:T(8,128)(2,1)S(1)} %all-to-all-done.5.tiles, f32[1,2048]{1,0:T(1,128)S(1)} %bitcast.20, bf16[24,128]{1,0:T(8,128)(2,1)S(1)} %shard_map.194.after, bf16[3,176,2048]{2,1,0:T(8,128)(2,1)S(1)} %copy-done.1, bf16[176,2048]{1,0:T(8,128)(2,1)} %collective-permute-done.7.t3, ...), custom_call_target="tpu_custom_call" | custom-call | flops 1048576 | bytes 4438016 | tf_op jit(solution)/shard_map/pallas_call | solution.py:91
  114.6 4.3 %all-to-all-start.6 = ((bf16[64,8,128]{2,1,0:T(8,128)(2,1)}), bf16[64,8,128]{2,1,0:T(8,128)(2,1)S(1)}, u32[]{:S(2)}, u32[]{:S(2)}) async-start(bf16[64,8,128]{2,1,0:T(8,128)(2,1)} %shard_map.196), calls=%async_computation.6 | async-start | bytes 262144 | tf_op jit(solution)/shard_map/all_to_all | solution.py:28
  118.9 2.6 %next_state.1 = f32[3,8,128,128]{3,2,1,0:T(8,128)} custom-call(f32[3,8,128,128]{3,2,1,0:T(8,128)S(1)} %shard_map.191.state, f32[3,24,128]{2,1,0:T(8,128)S(1)} %get-tuple-element.21.vectors), custom_call_target="tpu_custom_call" | custom-call | flops 1048576 | bytes 4194304 | tf_op jit(solution)/shard_map/next_state/pallas_call | solution.py:564
  121.5 8.5 %all-to-all-done.6.arrived = bf16[64,8,128]{2,1,0:T(8,128)(2,1)S(1)} async-done(((bf16[64,8,128]{2,1,0:T(8,128)(2,1)}), bf16[64,8,128]{2,1,0:T(8,128)(2,1)S(1)}, u32[]{:S(2)}, u32[]{:S(2)}) %all-to-all-start.6) | async-done | bytes 131104 | tf_op jit(solution)/shard_map/all_to_all | solution.py:28
  130.0 0.8 shard_map.197
  (20 shorter events, 0.1 us)
Async XLA Ops:
  0.6 29.2 %copy-start.6 = (f32[2048]{0:T(1024)S(1)}, f32[2048]{0:T(1024)}, u32[]{:S(2)}) copy-start(f32[2048]{0:T(1024)} %param.21) | copy-start | bytes 24580
  24.5 5.3 %collective-permute-start = (bf16[32,32,96]{2,1,0:T(8,128)(2,1)S(1)}, bf16[32,32,96]{2,1,0:T(8,128)(2,1)S(1)}, u32[]{:S(2)}, u32[]{:S(2)}) collective-permute-start(bf16[32,32,96]{2,1,0:T(8,128)(2,1)S(1)} %all_to_all.35.own), channel_id=1, source_target_pairs={{0,1},{1,0},{2,3},{3,2},{4,5},{5,4},{6,7},{7,6},{8,9},{9,8},{10,11... | collective-permute-start | bytes 589832 | tf_op jit(solution)/shard_map/ppermute | solution.py:38
  28.2 18.5 %copy-start.2 = (bf16[160,2048]{1,0:T(8,128)(2,1)}, bf16[160,2048]{1,0:T(8,128)(2,1)S(1)}, u32[]{:S(2)}) copy-start(bf16[160,2048]{1,0:T(8,128)(2,1)S(1)} %shard_map.187.refs_0_.a0) | copy-start | bytes 1966084
  28.2 3.3 %copy-start.11 = (bf16[2048,88]{0,1:T(8,128)(2,1)S(1)}, bf16[2048,88]{0,1:T(8,128)(2,1)}, u32[]{:S(2)}) copy-start(bf16[2048,88]{0,1:T(8,128)(2,1)} %param.34) | copy-start | bytes 1081348
  28.2 3.3 %copy-start.12 = (bf16[2048,88]{0,1:T(8,128)(2,1)S(1)}, bf16[2048,88]{0,1:T(8,128)(2,1)}, u32[]{:S(2)}) copy-start(bf16[2048,88]{0,1:T(8,128)(2,1)} %param.33) | copy-start | bytes 1081348
  28.2 18.4 %collective-permute-start.2 = (bf16[160,2048]{1,0:T(8,128)(2,1)S(1)}, bf16[160,2048]{1,0:T(8,128)(2,1)S(1)}, u32[]{:S(2)}, u32[]{:S(2)}) collective-permute-start(bf16[160,2048]{1,0:T(8,128)(2,1)S(1)} %shard_map.187.refs_0_.a0), channel_id=1, source_target_pairs={{0,2},{2,4},{4,6},{6,0},{8,10},{10,12},{12,14},{14,8},{16,18},{18,... | collective-permute-start | bytes 1966088 | tf_op jit(solution)/shard_map/ppermute | solution.py:47
  31.3 18.0 %copy-start.4 = (bf16[88,2048]{1,0:T(8,128)(2,1)S(1)}, bf16[88,2048]{1,0:T(8,128)(2,1)}, u32[]{:S(2)}) copy-start(bf16[88,2048]{1,0:T(8,128)(2,1)} %d0.1) | copy-start | bytes 1081348
  31.3 2.9 %collective-permute-start.1 = (bf16[8,96,128]{2,1,0:T(8,128)(2,1)S(1)}, bf16[8,96,128]{2,1,0:T(8,128)(2,1)S(1)}, u32[]{:S(2)}, u32[]{:S(2)}) collective-permute-start(bf16[8,96,128]{2,1,0:T(8,128)(2,1)S(1)} %get-tuple-element.17), channel_id=1, source_target_pairs={{0,1},{1,0},{2,3},{3,2},{4,5},{5,4},{6,7},{7,6},{8,9},{9,8},{10,11... | collective-permute-start | bytes 589832 | tf_op jit(solution)/shard_map/ppermute | solution.py:38
  31.5 20.5 %collective-permute-start.6 = (bf16[176,2048]{1,0:T(8,128)(2,1)S(1)}, bf16[176,2048]{1,0:T(8,128)(2,1)}, u32[]{:S(2)}, u32[]{:S(2)}) collective-permute-start(bf16[176,2048]{1,0:T(8,128)(2,1)S(1)} %pad_maximum_fusion.refs_0_), channel_id=1, source_target_pairs={{0,6},{2,0},{4,2},{6,4},{8,14},{10,8},{12,10},{14,12},{16,22},{18,... | collective-permute-start | bytes 2162696 | tf_op jit(solution)/shard_map/ppermute | solution.py:47
  35.0 20.0 %all-to-all-start.1 = ((bf16[32,24,128]{2,1,0:T(8,128)(2,1)}), bf16[32,24,128]{2,1,0:T(8,128)(2,1)S(1)}, u32[]{:S(2)}, u32[]{:S(2)}) async-start(bf16[32,24,128]{2,1,0:T(8,128)(2,1)} %bitcast.4), calls=%async_computation.1 | async-start | bytes 393216 | tf_op jit(solution)/shard_map/all_to_all | solution.py:28
  46.7 14.4 %copy-start.10 = (bf16[160,2048]{1,0:T(8,128)(2,1)}, bf16[160,2048]{1,0:T(8,128)(2,1)S(1)}, u32[]{:S(2)}) copy-start(bf16[160,2048]{1,0:T(8,128)(2,1)S(1)} %collective-permute-done.2.refs_1_.a1) | copy-start | bytes 1966084
  46.7 16.2 %collective-permute-start.3 = (bf16[160,2048]{1,0:T(8,128)(2,1)S(1)}, bf16[160,2048]{1,0:T(8,128)(2,1)}, u32[]{:S(2)}, u32[]{:S(2)}) collective-permute-start(bf16[160,2048]{1,0:T(8,128)(2,1)S(1)} %collective-permute-done.2.refs_1_.a1), channel_id=1, source_target_pairs={{0,2},{2,4},{4,6},{6,0},{8,10},{10,12},{12,14},{14,8},{16,18},{18,... | collective-permute-start | bytes 1966088 | tf_op jit(solution)/shard_map/ppermute | solution.py:47
  46.7 19.0 %collective-permute-start.4 = (bf16[160,2048]{1,0:T(8,128)(2,1)S(1)}, bf16[160,2048]{1,0:T(8,128)(2,1)}, u32[]{:S(2)}, u32[]{:S(2)}) collective-permute-start(bf16[160,2048]{1,0:T(8,128)(2,1)S(1)} %shard_map.187.refs_0_.a0), channel_id=1, source_target_pairs={{0,6},{2,0},{4,2},{6,4},{8,14},{10,8},{12,10},{14,12},{16,22},{18,... | collective-permute-start | bytes 1966088 | tf_op jit(solution)/shard_map/ppermute | solution.py:47
  49.3 51.8 %collective-permute-start.5 = (bf16[176,2048]{1,0:T(8,128)(2,1)S(1)}, bf16[176,2048]{1,0:T(8,128)(2,1)}, u32[]{:S(2)}, u32[]{:S(2)}) collective-permute-start(bf16[176,2048]{1,0:T(8,128)(2,1)S(1)} %pad_maximum_fusion.refs_0_), channel_id=1, source_target_pairs={{0,2},{2,4},{4,6},{6,0},{8,10},{10,12},{12,14},{14,8},{16,18},{18,... | collective-permute-start | bytes 2162696 | tf_op jit(solution)/shard_map/ppermute | solution.py:47
  49.4 38.8 %collective-permute-start.9 = (bf16[88,2048]{1,0:T(8,128)(2,1)S(1)}, bf16[88,2048]{1,0:T(8,128)(2,1)}, u32[]{:S(2)}, u32[]{:S(2)}) collective-permute-start(bf16[88,2048]{1,0:T(8,128)(2,1)S(1)} %copy-done.4), channel_id=1, source_target_pairs={{0,6},{2,0},{4,2},{6,4},{8,14},{10,8},{12,10},{14,12},{16,22},{18,... | collective-permute-start | bytes 1081352 | tf_op jit(solution)/shard_map/ppermute | solution.py:47
  52.0 52.1 %collective-permute-start.7 = (bf16[176,2048]{1,0:T(8,128)(2,1)}, bf16[176,2048]{1,0:T(8,128)(2,1)}, u32[]{:S(2)}, u32[]{:S(2)}) collective-permute-start(bf16[176,2048]{1,0:T(8,128)(2,1)} %collective-permute-done.6.refs_2_), channel_id=1, source_target_pairs={{0,6},{2,0},{4,2},{6,4},{8,14},{10,8},{12,10},{14,12},{16,22},{18,... | collective-permute-start | bytes 2162696 | tf_op jit(solution)/shard_map/ppermute | solution.py:47
  55.6 13.9 %all-to-all-start.2 = ((bf16[16,24,128]{2,1,0:T(8,128)(2,1)}), bf16[16,24,128]{2,1,0:T(8,128)(2,1)S(1)}, u32[]{:S(2)}, u32[]{:S(2)}) async-start(bf16[16,24,128]{2,1,0:T(8,128)(2,1)} %broadcast_in_dim.13), calls=%async_computation.2 | async-start | bytes 196608 | tf_op jit(solution)/shard_map/all_to_all | solution.py:28
  61.0 8.5 %copy-start.7 = (f32[2048]{0:T(1024)S(1)}, f32[2048]{0:T(1024)}, u32[]{:S(2)}) copy-start(f32[2048]{0:T(1024)} %param.25) | copy-start | bytes 24580
  71.7 10.1 %all-to-all-start.3 = ((bf16[8,16,128]{2,1,0:T(8,128)(2,1)}), bf16[8,16,128]{2,1,0:T(8,128)(2,1)S(1)}, u32[]{:S(2)}, u32[]{:S(2)}) async-start(bf16[8,16,128]{2,1,0:T(8,128)(2,1)} %bitcast.11), calls=%async_computation.3 | async-start | bytes 65536 | tf_op jit(solution)/shard_map/all_to_all | solution.py:28
  75.1 1.4 %copy-start.3 = (f32[3,8,128,128]{3,2,1,0:T(8,128)S(1)}, f32[3,8,128,128]{3,2,1,0:T(8,128)}, u32[]{:S(2)}) copy-start(f32[3,8,128,128]{3,2,1,0:T(8,128)} %state.1) | copy-start | bytes 4718596
  76.5 0.7 copy-start.5
  76.5 5.4 %copy-start.9 = (f32[8,128]{1,0:T(8,128)S(1)}, f32[8,128]{1,0:T(8,128)}, u32[]{:S(2)}) copy-start(f32[8,128]{1,0:T(8,128)} %gain.1) | copy-start | bytes 12292
  83.7 12.9 %all-to-all-start.4 = ((bf16[16,24,128]{2,1,0:T(8,128)(2,1)}), bf16[16,24,128]{2,1,0:T(8,128)(2,1)S(1)}, u32[]{:S(2)}, u32[]{:S(2)}) async-start(bf16[16,24,128]{2,1,0:T(8,128)(2,1)} %broadcast_in_dim.14), calls=%async_computation.4 | async-start | bytes 196608 | tf_op jit(solution)/shard_map/all_to_all | solution.py:28
  88.1 16.0 %collective-permute-start.8 = (bf16[88,2048]{1,0:T(8,128)(2,1)S(1)}, bf16[88,2048]{1,0:T(8,128)(2,1)}, u32[]{:S(2)}, u32[]{:S(2)}) collective-permute-start(bf16[88,2048]{1,0:T(8,128)(2,1)S(1)} %copy-done.4), channel_id=1, source_target_pairs={{0,2},{2,4},{4,6},{6,0},{8,10},{10,12},{12,14},{14,8},{16,18},{18,... | collective-permute-start | bytes 1081352 | tf_op jit(solution)/shard_map/ppermute | solution.py:47
  88.2 15.9 %collective-permute-start.10 = (bf16[88,2048]{1,0:T(8,128)(2,1)}, bf16[88,2048]{1,0:T(8,128)(2,1)}, u32[]{:S(2)}, u32[]{:S(2)}) collective-permute-start(bf16[88,2048]{1,0:T(8,128)(2,1)} %collective-permute-done.9.d2), channel_id=1, source_target_pairs={{0,6},{2,0},{4,2},{6,4},{8,14},{10,8},{12,10},{14,12},{16,22},{18,... | collective-permute-start | bytes 1081352 | tf_op jit(solution)/shard_map/ppermute | solution.py:47
  97.7 11.8 %all-to-all-start.5 = ((bf16[16,24,128]{2,1,0:T(8,128)(2,1)}), bf16[16,24,128]{2,1,0:T(8,128)(2,1)S(1)}, u32[]{:S(2)}, u32[]{:S(2)}) async-start(bf16[16,24,128]{2,1,0:T(8,128)(2,1)} %broadcast_in_dim.15), calls=%async_computation.5 | async-start | bytes 196608 | tf_op jit(solution)/shard_map/all_to_all | solution.py:28
  101.1 8.3 %copy-start.8 = (f32[2048]{0:T(1024)S(1)}, f32[2048]{0:T(1024)}, u32[]{:S(2)}) copy-start(f32[2048]{0:T(1024)} %param.32) | copy-start | bytes 24580
  102.8 1.3 %copy-start = (bf16[3,176,2048]{2,1,0:T(8,128)(2,1)}, bf16[3,176,2048]{2,1,0:T(8,128)(2,1)S(1)}, u32[]{:S(2)}) copy-start(bf16[3,176,2048]{2,1,0:T(8,128)(2,1)S(1)} %shard_map.195.w_held) | copy-start | bytes 6488068
  109.5 1.6 %copy-start.1 = (bf16[3,176,2048]{2,1,0:T(8,128)(2,1)S(1)}, bf16[3,176,2048]{2,1,0:T(8,128)(2,1)}, u32[]{:S(2)}) copy-start(bf16[3,176,2048]{2,1,0:T(8,128)(2,1)} %copy-done) | copy-start | bytes 6488068
  114.6 15.4 %all-to-all-start.6 = ((bf16[64,8,128]{2,1,0:T(8,128)(2,1)}), bf16[64,8,128]{2,1,0:T(8,128)(2,1)S(1)}, u32[]{:S(2)}, u32[]{:S(2)}) async-start(bf16[64,8,128]{2,1,0:T(8,128)(2,1)} %shard_map.196), calls=%async_computation.6 | async-start | bytes 262144 | tf_op jit(solution)/shard_map/all_to_all | solution.py:28

commit v5 on v4

--- a/solution.py
+++ b/solution.py
@@ -78,9 +78,13 @@
     return jnp.where(mask, 1.0, 0.0).astype(jnp.bfloat16)
 
 
-def local(body, outs, *args, scratch=(), outside=(), held_out=False, vmem=False, flops=1 << 20):
+def local(body, outs, *args, scratch=(), outside=(), held_out=False, vmem=False, sent=(), flops=1 << 20):
     kind = pltpu.VMEM if vmem else jax.ShapeDtypeStruct
-    shapes = [kind(s, d) for s, d in outs]
+    shapes = [pltpu.HBM(s, d) if k in sent else kind(s, d) for k, (s, d) in enumerate(outs)]
+    placed = [
+        pl.BlockSpec(memory_space=pltpu.HBM) if k in sent else pl.BlockSpec(memory_space=pltpu.VMEM)
+        for k in range(len(outs))
+    ]
     held = pl.BlockSpec(memory_space=pltpu.VMEM)
     specs = [pl.BlockSpec(memory_space=pl.ANY) if k in outside else held for k in range(len(args))]
     args = [
@@ -92,7 +96,7 @@
         body,
         out_shape=shapes,
         in_specs=specs,
-        out_specs=[held] * len(outs),
+        out_specs=placed,
         scratch_shapes=list(scratch),
         compiler_params=pltpu.CompilerParams(vmem_limit_bytes=VMEM_LIMIT),
         cost_estimate=pl.CostEstimate(flops=flops, bytes_accessed=size, transcendentals=0),
@@ -172,12 +176,6 @@
         move.wait()
 
 
-def load_state(state, held, sem):
-    move = pltpu.make_async_copy(state, held, sem)
-    move.start()
-    move.wait()
-
-
 def load_parts(*refs):
     *parts, held, sems = refs
     moves = [
@@ -190,7 +188,7 @@
         move.wait()
 
 
-def pack_early(query, forget, inputs, out_gate, mix, out, *scratch):
+def pack_early(query, forget, inputs, out_gate, mix, packed, out, *scratch):
     *held, sems = scratch
     moves = [
         pltpu.make_async_copy(w, held[k], sems.at[k])
@@ -208,6 +206,9 @@
             at = (k * heads + h) * per
             out[at : at + 4 * per, :] = bf(block)
     moves[4].wait()
+    move = pltpu.make_async_copy(out, packed, sems.at[5])
+    move.start()
+    move.wait()
 
 
 def flipped(x, out):
@@ -301,14 +302,21 @@
         merged[k * heads : (k + 1) * heads, :] = gated
 
 
-def next_state(state, vectors, out):
-    heads = out.shape[1]
-    columns = vectors[0].T
-    for h in range(heads):
-        line = vectors[0, 2 * heads + h : 2 * heads + h + 1, :]
-        out[0, h] = (
-            columns[:, h : h + 1] * state[0, h] + columns[:, heads + h : heads + h + 1] * line
-        )
+def next_state(state, vectors, out, held, sems):
+    seqs, heads = state.shape[:2]
+    moves = []
+    for k in range(seqs):
+        columns = vectors[k].T
+        for h in range(heads):
+            line = vectors[k, 2 * heads + h : 2 * heads + h + 1, :]
+            held[k, h] = (
+                columns[:, h : h + 1] * state[k, h] + columns[:, heads + h : heads + h + 1] * line
+            )
+        move = pltpu.make_async_copy(held.at[k], out.at[k], sems.at[k])
+        move.start()
+        moves.append(move)
+    for move in moves:
+        move.wait()
 
 
 def mix_out(tiles, w_mix, residual, after, rows):
@@ -465,9 +473,14 @@
         [((LANES + own_cols, width), half16)],
         *kinds,
         w_mix_out.T,
-        scratch=(*[pltpu.VMEM(k.shape, half16) for k in kinds], dma((5,))),
+        scratch=(
+            pltpu.VMEM((LANES + own_cols, width), half16),
+            *[pltpu.VMEM(k.shape, half16) for k in kinds],
+            dma((6,)),
+        ),
         outside=(0, 1, 2, 3, 4),
         held_out=True,
+        sent=(0,),
     )
     late_top = jnp.concatenate([w_gate_two.T, w_up_two.T], axis=0)
 
@@ -542,14 +555,7 @@
     )
     zgroups = [[a * Y_COUNT + b for a in range(Z_COUNT)] for b in range(Y_COUNT)]
     arrived = exchange(channels.reshape(Z_COUNT, 16, LANES), "kv", zgroups)
-    (held,) = local(
-        load_state,
-        [(state.shape, half32)],
-        state,
-        scratch=(dma,),
-        outside=(0,),
-        vmem=True,
-    )
+    held = state
     gated, vectors = local(
         read_state,
         [((seqs * heads, LANES), half32), ((seqs, 3 * heads, LANES), half32)],
@@ -560,20 +566,14 @@
         held,
     )
     merged_tiles = slab_exchange(bf(gated))
-    whole = lambda *dims: pl.BlockSpec((1, *dims), lambda k: (k, *(0 for _ in dims)))
-    new_state = pl.pallas_call(
+    (new_state,) = local(
         next_state,
-        grid=(seqs,),
-        out_shape=jax.ShapeDtypeStruct(state.shape, half32),
-        in_specs=[
-            whole(*state.shape[1:]),
-            whole(3 * heads, LANES),
-        ],
-        out_specs=whole(*state.shape[1:]),
-        compiler_params=pltpu.CompilerParams(vmem_limit_bytes=VMEM_LIMIT),
-        cost_estimate=pl.CostEstimate(flops=1 << 20, bytes_accessed=1 << 22, transcendentals=0),
-        name="next_state",
-    )(held, vectors)
+        [(state.shape, half32)],
+        held,
+        vectors,
+        scratch=(pltpu.VMEM(state.shape, half32), dma((seqs,))),
+        sent=(0,),
+    )
     (w_mix,) = local(
         load_mix,
         [((Y_COUNT, own_cols, width), half16)],

time: 132 us -> 132 us (level)
  local copies, waits for them, and re-layouts: 7.64 us -> 4.99 us
    unnamed x26 -> x22, local copies, waits for them, and re-layouts: 4.93 us -> 2.29 us
    all_to_all x6, waiting for transfers between devices: 27 us -> 29.3 us  [exchange(): lax.all_to_all(tiles, axis, split_axis=0, concat_axis=0, axis_index_group...]
    pallas_call x14 -> x13, Pallas kernels: 19.2 us -> 19.3 us  [local(): pl.pallas_call(body, out_shape=shapes, in_specs=specs, out_specs=placed,...]
  transfers between devices with their start and end apart: 17 -> 17, of which waited for: 8 -> 9; matrix products, arithmetic and copies ran while one was open for 2% -> 3% of each run, Pallas kernels for 11% -> 11%
where the time goes in v5:
time: 132 us; the launch traced here: 131 us
  starting transfers between devices  41.7 us (32%)
  waiting for transfers between devices  39.3 us (30%)
  blocking collectives  23.1 us (18%)
  Pallas kernels  19.3 us (15%)
  local copies, waits for them, and re-layouts  4.99 us (4%)
  other arithmetic  1.67 us (1%)
    all_to_all x6, waiting for transfers between devices, exchange(): lax.all_to_all(tiles, axis, split_axis=0, concat_axis=0, axis_index_group...  29.3 us
    all_to_all x6, starting transfers between devices, exchange(): lax.all_to_all(tiles, axis, split_axis=0, concat_axis=0, axis_index_group...  24.7 us
    all_to_all x1, blocking collectives, exchange(): lax.all_to_all(tiles, axis, split_axis=0, concat_axis=0, axis_index_group...  23.1 us
    pallas_call x13, Pallas kernels, local(): pl.pallas_call(body, out_shape=shapes, in_specs=specs, out_specs=placed,...  19.3 us
    ppermute x9, starting transfers between devices, shift_y(): return lax.ppermute(x, 'kv', pairs)  14.3 us
    ppermute x9, waiting for transfers between devices, shift_y(): return lax.ppermute(x, 'kv', pairs)  10 us
    broadcast_in_dim x4, local copies, waits for them, and re-layouts, copies(): return jnp.broadcast_to(x, (count, *x.shape))  2.71 us
    ppermute x2, starting transfers between devices, swap_cores(): return lax.ppermute(x, 'tp', [(0, 1), (1, 0)])  2.65 us
  transfers between devices with their start and end apart: 17, of which 9 were waited for; matrix products, arithmetic and copies ran while one was open for 3% of the time, Pallas kernels for 11%

profile of v5, /device:TPU:1, one launch (start us, length us, event | category | flops | bytes accessed | tf_op | source)
XLA Modules:
  0.0 131.0 jit_solution(18405964909427753682)
XLA Ops:
  0.6 0.7 broadcast_in_dim.12
  1.4 23.1 %all_to_all.35.own = bf16[32,32,96]{2,1,0:T(8,128)(2,1)S(1)} all-to-all(bf16[32,32,96]{2,1,0:T(8,128)(2,1)S(1)} %broadcast_in_dim.12), channel_id=1, replica_groups=mesh['dp'=4,'kv'=32,'tp'=2] {'kv'}, dimensions={0} | all-to-all | bytes 393216 | tf_op jit(solution)/shard_map/all_to_all | solution.py:28
  24.5 2.5 %collective-permute-start = (bf16[32,32,96]{2,1,0:T(8,128)(2,1)S(1)}, bf16[32,32,96]{2,1,0:T(8,128)(2,1)S(1)}, u32[]{:S(2)}, u32[]{:S(2)}) collective-permute-start(bf16[32,32,96]{2,1,0:T(8,128)(2,1)S(1)} %all_to_all.35.own), channel_id=1, source_target_pairs={{0,1},{1,0},{2,3},{3,2},{4,5},{5,4},{6,7},{7,6},{8,9},{9,8},{10,11... | collective-permute-start | bytes 589832 | tf_op jit(solution)/shard_map/ppermute | solution.py:38
  27.0 2.1 %shard_map.187.refs_0_.a0 = bf16[160,2048]{1,0:T(8,128)(2,1)} custom-call(bf16[8,4,2048]{2,1,0:T(4,128)(2,1)} %bitcast.25, bf16[8,4,2048]{2,1,0:T(4,128)(2,1)} %bitcast.26, bf16[8,4,2048]{2,1,0:T(4,128)(2,1)} %bitcast.27, bf16[8,4,2048]{2,1,0:T(4,128)(2,1)} %bitcast.28, bf16[32,2048]{1,0:T(8,128)(2,1)} %bitcast.29), custom_call_target="tpu_custom_call" | custom-call | flops 1048576 | bytes 655360 | tf_op jit(solution)/shard_map/pallas_call | solution.py:95
  29.0 0.0 copy-start.9
  29.1 0.0 copy-start.10
  29.1 0.1 collective-permute-start.2
  29.2 1.3 shard_map.185
  30.5 0.0 collective-permute-done.other
  30.5 0.0 copy-done.3
  30.5 1.5 %shard_map.186 = (f32[8,96,128]{2,1,0:T(8,128)S(1)}, bf16[8,96,128]{2,1,0:T(8,128)(2,1)S(1)}, f32[24,128]{1,0:T(8,128)S(1)}) custom-call(bf16[32,32,96]{2,1,0:T(8,128)(2,1)S(1)} %all_to_all.35.own, bf16[32,32,96]{2,1,0:T(8,128)(2,1)S(1)} %collective-permute-done.other, f32[16,128]{1,0:T(8,128)S(1)} %bitcast.18, ...), custom_call_target="tpu_custom_call" | custom-call | flops 1048576 | bytes 1482752 | tf_op jit(solution)/shard_map/pallas_call | solution.py:95
  31.9 0.2 collective-permute-start.1
  32.1 0.9 pad_maximum_fusion.refs_0_
  33.0 2.8 %collective-permute-start.6 = (bf16[176,2048]{1,0:T(8,128)(2,1)}, bf16[176,2048]{1,0:T(8,128)(2,1)}, u32[]{:S(2)}, u32[]{:S(2)}) collective-permute-start(bf16[176,2048]{1,0:T(8,128)(2,1)} %pad_maximum_fusion.refs_0_), channel_id=1, source_target_pairs={{0,6},{2,0},{4,2},{6,4},{8,14},{10,8},{12,10},{14,12},{16,22},{18,... | collective-permute-start | bytes 2162696 | tf_op jit(solution)/shard_map/ppermute | solution.py:47
  35.8 0.0 collective-permute-done.1
  35.8 0.7 add_convert_fusion
  36.5 3.9 %all-to-all-start.1 = ((bf16[32,24,128]{2,1,0:T(8,128)(2,1)}), bf16[32,24,128]{2,1,0:T(8,128)(2,1)S(1)}, u32[]{:S(2)}, u32[]{:S(2)}) async-start(bf16[32,24,128]{2,1,0:T(8,128)(2,1)} %bitcast.4), calls=%async_computation.1 | async-start | bytes 393216 | tf_op jit(solution)/shard_map/all_to_all | solution.py:28
  40.4 7.0 %collective-permute-done.2.refs_1_.a1 = bf16[160,2048]{1,0:T(8,128)(2,1)S(1)} collective-permute-done((bf16[160,2048]{1,0:T(8,128)(2,1)}, bf16[160,2048]{1,0:T(8,128)(2,1)S(1)}, u32[]{:S(2)}, u32[]{:S(2)}) %collective-permute-start.2) | collective-permute-done | bytes 655392 | tf_op jit(solution)/shard_map/ppermute | solution.py:47
  47.4 0.0 collective-permute-start.3
  47.4 2.7 %collective-permute-start.4 = (bf16[160,2048]{1,0:T(8,128)(2,1)}, bf16[160,2048]{1,0:T(8,128)(2,1)}, u32[]{:S(2)}, u32[]{:S(2)}) collective-permute-start(bf16[160,2048]{1,0:T(8,128)(2,1)} %shard_map.187.refs_0_.a0), channel_id=1, source_target_pairs={{0,6},{2,0},{4,2},{6,4},{8,14},{10,8},{12,10},{14,12},{16,22},{18,... | collective-permute-start | bytes 1966088 | tf_op jit(solution)/shard_map/ppermute | solution.py:47
  50.1 0.0 collective-permute-start.5
  50.1 2.7 %collective-permute-start.9 = (bf16[88,2048]{1,0:T(8,128)(2,1)}, bf16[88,2048]{1,0:T(8,128)(2,1)}, u32[]{:S(2)}, u32[]{:S(2)}) collective-permute-start(bf16[88,2048]{1,0:T(8,128)(2,1)} %d0.1), channel_id=1, source_target_pairs={{0,6},{2,0},{4,2},{6,4},{8,14},{10,8},{12,10},{14,12},{16,22},{18,... | collective-permute-start | bytes 1081352 | tf_op jit(solution)/shard_map/ppermute | solution.py:47
  52.7 0.6 collective-permute-done.6.refs_2_
  53.3 3.5 %collective-permute-start.7 = (bf16[176,2048]{1,0:T(8,128)(2,1)}, bf16[176,2048]{1,0:T(8,128)(2,1)}, u32[]{:S(2)}, u32[]{:S(2)}) collective-permute-start(bf16[176,2048]{1,0:T(8,128)(2,1)} %collective-permute-done.6.refs_2_), channel_id=1, source_target_pairs={{0,6},{2,0},{4,2},{6,4},{8,14},{10,8},{12,10},{14,12},{16,22},{18,... | collective-permute-start | bytes 2162696 | tf_op jit(solution)/shard_map/ppermute | solution.py:47
  56.8 0.0 all-to-all-done.1
  56.8 0.6 broadcast_in_dim.13
  57.5 5.3 %all-to-all-start.2 = ((bf16[16,24,128]{2,1,0:T(8,128)(2,1)}), bf16[16,24,128]{2,1,0:T(8,128)(2,1)S(1)}, u32[]{:S(2)}, u32[]{:S(2)}) async-start(bf16[16,24,128]{2,1,0:T(8,128)(2,1)} %broadcast_in_dim.13), calls=%async_computation.2 | async-start | bytes 196608 | tf_op jit(solution)/shard_map/all_to_all | solution.py:28
  62.8 0.7 collective-permute-done.3.refs_2_.a2
  63.6 0.8 copy-done.8
  64.4 1.4 %shard_map.188.w_held = bf16[3,128,2048]{2,1,0:T(8,128)(2,1)S(1)} custom-call(bf16[160,2048]{1,0:T(8,128)(2,1)} %shard_map.187.refs_0_.a0, bf16[160,2048]{1,0:T(8,128)(2,1)} %copy-done.7, bf16[160,2048]{1,0:T(8,128)(2,1)} %copy-done.8), custom_call_target="tpu_custom_call" | custom-call | flops 1048576 | bytes 1966080 | tf_op jit(solution)/shard_map/pallas_call | solution.py:95
  65.8 0.0 copy-start.2
  65.8 0.0 copy-start
  65.8 0.0 copy-start.6
  65.8 1.7 %collective-permute-done.4.a3 = bf16[160,2048]{1,0:T(8,128)(2,1)} collective-permute-done((bf16[160,2048]{1,0:T(8,128)(2,1)}, bf16[160,2048]{1,0:T(8,128)(2,1)}, u32[]{:S(2)}, u32[]{:S(2)}) %collective-permute-start.4) | collective-permute-done | bytes 655392 | tf_op jit(solution)/shard_map/ppermute | solution.py:47
  67.5 3.8 %all-to-all-done.2.tiles = bf16[16,24,128]{2,1,0:T(8,128)(2,1)S(1)} async-done(((bf16[16,24,128]{2,1,0:T(8,128)(2,1)}), bf16[16,24,128]{2,1,0:T(8,128)(2,1)S(1)}, u32[]{:S(2)}, u32[]{:S(2)}) %all-to-all-start.2) | async-done | bytes 98336 | tf_op jit(solution)/shard_map/all_to_all | solution.py:28
  71.3 2.2 %shard_map.189 = (bf16[128,128]{1,0:T(8,128)(2,1)}, f32[24,128]{1,0:T(8,128)S(1)}) custom-call(bf16[16,24,128]{2,1,0:T(8,128)(2,1)S(1)} %all-to-all-done.2.tiles, f32[1,2048]{1,0:T(1,128)S(1)} %bitcast.19, bf16[3,128,2048]{2,1,0:T(8,128)(2,1)S(1)} %shard_map.188.w_held, bf16[160,2048]{1,0:T(8,128)(2,1)} %collective-permute-done.4.a3), custom_call_target="tpu_custom_call" | custom-call | flops 1048576 | bytes 2334720 | tf_op jit(solution)/shard_map/pallas_call | solution.py:95
  73.5 3.3 %all-to-all-start.3 = ((bf16[8,16,128]{2,1,0:T(8,128)(2,1)}), bf16[8,16,128]{2,1,0:T(8,128)(2,1)S(1)}, u32[]{:S(2)}, u32[]{:S(2)}) async-start(bf16[8,16,128]{2,1,0:T(8,128)(2,1)} %bitcast.11), calls=%async_computation.3 | async-start | bytes 65536 | tf_op jit(solution)/shard_map/all_to_all | solution.py:28
  76.9 0.1 shard_map.190.floor_t
  77.0 6.7 %all-to-all-done.3 = bf16[8,16,128]{2,1,0:T(8,128)(2,1)S(1)} async-done(((bf16[8,16,128]{2,1,0:T(8,128)(2,1)}), bf16[8,16,128]{2,1,0:T(8,128)(2,1)S(1)}, u32[]{:S(2)}, u32[]{:S(2)}) %all-to-all-start.3) | async-done | bytes 32800 | tf_op jit(solution)/shard_map/all_to_all | solution.py:28
  83.7 1.2 shard_map.191
  84.9 0.7 broadcast_in_dim.14
  85.6 4.4 %all-to-all-start.4 = ((bf16[16,24,128]{2,1,0:T(8,128)(2,1)}), bf16[16,24,128]{2,1,0:T(8,128)(2,1)S(1)}, u32[]{:S(2)}, u32[]{:S(2)}) async-start(bf16[16,24,128]{2,1,0:T(8,128)(2,1)} %broadcast_in_dim.14), calls=%async_computation.4 | async-start | bytes 196608 | tf_op jit(solution)/shard_map/all_to_all | solution.py:28
  90.0 0.0 collective-permute-start.8
  90.0 0.0 collective-permute-done.9.d2
  90.0 2.7 %collective-permute-start.10 = (bf16[88,2048]{1,0:T(8,128)(2,1)}, bf16[88,2048]{1,0:T(8,128)(2,1)S(1)}, u32[]{:S(2)}, u32[]{:S(2)}) collective-permute-start(bf16[88,2048]{1,0:T(8,128)(2,1)} %collective-permute-done.9.d2), channel_id=1, source_target_pairs={{0,6},{2,0},{4,2},{6,4},{8,14},{10,8},{12,10},{14,12},{16,22},{18,... | collective-permute-start | bytes 1081352 | tf_op jit(solution)/shard_map/ppermute | solution.py:47
  92.7 1.1 shard_map.192.w_mix
  93.8 4.7 %all-to-all-done.4.tiles = bf16[16,24,128]{2,1,0:T(8,128)(2,1)S(1)} async-done(((bf16[16,24,128]{2,1,0:T(8,128)(2,1)}), bf16[16,24,128]{2,1,0:T(8,128)(2,1)S(1)}, u32[]{:S(2)}, u32[]{:S(2)}) %all-to-all-start.4) | async-done | bytes 98336 | tf_op jit(solution)/shard_map/all_to_all | solution.py:28
  98.5 0.4 shard_map.193.after
  98.9 0.7 broadcast_in_dim.15
  99.5 3.4 %all-to-all-start.5 = ((bf16[16,24,128]{2,1,0:T(8,128)(2,1)}), bf16[16,24,128]{2,1,0:T(8,128)(2,1)S(1)}, u32[]{:S(2)}, u32[]{:S(2)}) async-start(bf16[16,24,128]{2,1,0:T(8,128)(2,1)} %broadcast_in_dim.15), calls=%async_computation.5 | async-start | bytes 196608 | tf_op jit(solution)/shard_map/all_to_all | solution.py:28
  102.9 0.0 copy-start.5
  102.9 0.0 collective-permute-done.5.refs_1_
  103.0 1.6 %shard_map.194.w_held = bf16[3,176,2048]{2,1,0:T(8,128)(2,1)S(1)} custom-call(bf16[176,2048]{1,0:T(8,128)(2,1)} %pad_maximum_fusion.refs_0_, bf16[176,2048]{1,0:T(8,128)(2,1)} %collective-permute-done.5.refs_1_, bf16[176,2048]{1,0:T(8,128)(2,1)} %collective-permute-done.6.refs_2_), custom_call_target="tpu_custom_call" | custom-call | flops 1048576 | bytes 2162688 | tf_op jit(solution)/shard_map/pallas_call | solution.py:95
  104.5 0.0 collective-permute-done.8.d1
  104.6 0.0 collective-permute-done.10.d3
  104.6 0.0 collective-permute-done.7.t3
  104.6 6.7 %all-to-all-done.5.tiles = bf16[16,24,128]{2,1,0:T(8,128)(2,1)S(1)} async-done(((bf16[16,24,128]{2,1,0:T(8,128)(2,1)}), bf16[16,24,128]{2,1,0:T(8,128)(2,1)S(1)}, u32[]{:S(2)}, u32[]{:S(2)}) %all-to-all-start.5) | async-done | bytes 98336 | tf_op jit(solution)/shard_map/all_to_all | solution.py:28
  111.3 3.5 %shard_map.195 = bf16[64,8,128]{2,1,0:T(8,128)(2,1)} custom-call(bf16[16,24,128]{2,1,0:T(8,128)(2,1)S(1)} %all-to-all-done.5.tiles, f32[1,2048]{1,0:T(1,128)S(1)} %bitcast.20, bf16[24,128]{1,0:T(8,128)(2,1)S(1)} %shard_map.193.after, bf16[3,176,2048]{2,1,0:T(8,128)(2,1)S(1)} %shard_map.194.w_held, bf16[176,2048]{1,0:T(8,128)(2,1)} %collective-permute-done.7.t3, ...), custom_call_target="tpu_custom_call" | custom-call | flops 1048576 | bytes 4438016 | tf_op jit(solution)/shard_map/pallas_call | solution.py:95
  114.8 4.3 %all-to-all-start.6 = ((bf16[64,8,128]{2,1,0:T(8,128)(2,1)}), bf16[64,8,128]{2,1,0:T(8,128)(2,1)S(1)}, u32[]{:S(2)}, u32[]{:S(2)}) async-start(bf16[64,8,128]{2,1,0:T(8,128)(2,1)} %shard_map.195), calls=%async_computation.6 | async-start | bytes 262144 | tf_op jit(solution)/shard_map/all_to_all | solution.py:28
  119.1 0.0 copy-start.1
  119.2 1.4 %copy-done.1 = f32[3,8,128,128]{3,2,1,0:T(8,128)S(1)} copy-done((f32[3,8,128,128]{3,2,1,0:T(8,128)S(1)}, f32[3,8,128,128]{3,2,1,0:T(8,128)}, u32[]{:S(2)}) %copy-start.1) | copy-done | bytes 1572888
  120.6 2.2 %shard_map.197 = f32[3,8,128,128]{3,2,1,0:T(8,128)} custom-call(f32[3,8,128,128]{3,2,1,0:T(8,128)S(1)} %copy-done.1, f32[3,24,128]{2,1,0:T(8,128)S(1)} %get-tuple-element.21.vectors), custom_call_target="tpu_custom_call" | custom-call | flops 1048576 | bytes 1609728 | tf_op jit(solution)/shard_map/pallas_call | solution.py:95
  122.7 7.5 %all-to-all-done.6.arrived = bf16[64,8,128]{2,1,0:T(8,128)(2,1)S(1)} async-done(((bf16[64,8,128]{2,1,0:T(8,128)(2,1)}), bf16[64,8,128]{2,1,0:T(8,128)(2,1)S(1)}, u32[]{:S(2)}, u32[]{:S(2)}) %all-to-all-start.6) | async-done | bytes 131104 | tf_op jit(solution)/shard_map/all_to_all | solution.py:28
  130.2 0.8 shard_map.196
  (15 shorter events, 0.1 us)
Async XLA Ops:
  0.6 29.8 %copy-start.3 = (f32[2048]{0:T(1024)S(1)}, f32[2048]{0:T(1024)}, u32[]{:S(2)}) copy-start(f32[2048]{0:T(1024)} %param.21) | copy-start | bytes 24580
  24.5 6.0 %collective-permute-start = (bf16[32,32,96]{2,1,0:T(8,128)(2,1)S(1)}, bf16[32,32,96]{2,1,0:T(8,128)(2,1)S(1)}, u32[]{:S(2)}, u32[]{:S(2)}) collective-permute-start(bf16[32,32,96]{2,1,0:T(8,128)(2,1)S(1)} %all_to_all.35.own), channel_id=1, source_target_pairs={{0,1},{1,0},{2,3},{3,2},{4,5},{5,4},{6,7},{7,6},{8,9},{9,8},{10,11... | collective-permute-start | bytes 589832 | tf_op jit(solution)/shard_map/ppermute | solution.py:38
  29.0 3.1 %copy-start.9 = (bf16[2048,88]{0,1:T(8,128)(2,1)S(1)}, bf16[2048,88]{0,1:T(8,128)(2,1)}, u32[]{:S(2)}) copy-start(bf16[2048,88]{0,1:T(8,128)(2,1)} %param.34) | copy-start | bytes 1081348
  29.1 3.1 %copy-start.10 = (bf16[2048,88]{0,1:T(8,128)(2,1)S(1)}, bf16[2048,88]{0,1:T(8,128)(2,1)}, u32[]{:S(2)}) copy-start(bf16[2048,88]{0,1:T(8,128)(2,1)} %param.33) | copy-start | bytes 1081348
  29.1 18.3 %collective-permute-start.2 = (bf16[160,2048]{1,0:T(8,128)(2,1)}, bf16[160,2048]{1,0:T(8,128)(2,1)S(1)}, u32[]{:S(2)}, u32[]{:S(2)}) collective-permute-start(bf16[160,2048]{1,0:T(8,128)(2,1)} %shard_map.187.refs_0_.a0), channel_id=1, source_target_pairs={{0,2},{2,4},{4,6},{6,0},{8,10},{10,12},{12,14},{14,8},{16,18},{18,... | collective-permute-start | bytes 1966088 | tf_op jit(solution)/shard_map/ppermute | solution.py:47
  31.9 3.9 %collective-permute-start.1 = (bf16[8,96,128]{2,1,0:T(8,128)(2,1)S(1)}, bf16[8,96,128]{2,1,0:T(8,128)(2,1)S(1)}, u32[]{:S(2)}, u32[]{:S(2)}) collective-permute-start(bf16[8,96,128]{2,1,0:T(8,128)(2,1)S(1)} %get-tuple-element.17), channel_id=1, source_target_pairs={{0,1},{1,0},{2,3},{3,2},{4,5},{5,4},{6,7},{7,6},{8,9},{9,8},{10,11... | collective-permute-start | bytes 589832 | tf_op jit(solution)/shard_map/ppermute | solution.py:38
  33.0 20.3 %collective-permute-start.6 = (bf16[176,2048]{1,0:T(8,128)(2,1)}, bf16[176,2048]{1,0:T(8,128)(2,1)}, u32[]{:S(2)}, u32[]{:S(2)}) collective-permute-start(bf16[176,2048]{1,0:T(8,128)(2,1)} %pad_maximum_fusion.refs_0_), channel_id=1, source_target_pairs={{0,6},{2,0},{4,2},{6,4},{8,14},{10,8},{12,10},{14,12},{16,22},{18,... | collective-permute-start | bytes 2162696 | tf_op jit(solution)/shard_map/ppermute | solution.py:47
  36.5 20.3 %all-to-all-start.1 = ((bf16[32,24,128]{2,1,0:T(8,128)(2,1)}), bf16[32,24,128]{2,1,0:T(8,128)(2,1)S(1)}, u32[]{:S(2)}, u32[]{:S(2)}) async-start(bf16[32,24,128]{2,1,0:T(8,128)(2,1)} %bitcast.4), calls=%async_computation.1 | async-start | bytes 393216 | tf_op jit(solution)/shard_map/all_to_all | solution.py:28
  47.4 16.2 %copy-start.7 = (bf16[160,2048]{1,0:T(8,128)(2,1)}, bf16[160,2048]{1,0:T(8,128)(2,1)S(1)}, u32[]{:S(2)}) copy-start(bf16[160,2048]{1,0:T(8,128)(2,1)S(1)} %collective-permute-done.2.refs_1_.a1) | copy-start | bytes 1966084
  47.4 16.2 %collective-permute-start.3 = (bf16[160,2048]{1,0:T(8,128)(2,1)S(1)}, bf16[160,2048]{1,0:T(8,128)(2,1)S(1)}, u32[]{:S(2)}, u32[]{:S(2)}) collective-permute-start(bf16[160,2048]{1,0:T(8,128)(2,1)S(1)} %collective-permute-done.2.refs_1_.a1), channel_id=1, source_target_pairs={{0,2},{2,4},{4,6},{6,0},{8,10},{10,12},{12,14},{14,8},{16,18},{18,... | collective-permute-start | bytes 1966088 | tf_op jit(solution)/shard_map/ppermute | solution.py:47
  47.4 20.2 %collective-permute-start.4 = (bf16[160,2048]{1,0:T(8,128)(2,1)}, bf16[160,2048]{1,0:T(8,128)(2,1)}, u32[]{:S(2)}, u32[]{:S(2)}) collective-permute-start(bf16[160,2048]{1,0:T(8,128)(2,1)} %shard_map.187.refs_0_.a0), channel_id=1, source_target_pairs={{0,6},{2,0},{4,2},{6,4},{8,14},{10,8},{12,10},{14,12},{16,22},{18,... | collective-permute-start | bytes 1966088 | tf_op jit(solution)/shard_map/ppermute | solution.py:47
  50.1 52.9 %collective-permute-start.5 = (bf16[176,2048]{1,0:T(8,128)(2,1)}, bf16[176,2048]{1,0:T(8,128)(2,1)}, u32[]{:S(2)}, u32[]{:S(2)}) collective-permute-start(bf16[176,2048]{1,0:T(8,128)(2,1)} %pad_maximum_fusion.refs_0_), channel_id=1, source_target_pairs={{0,2},{2,4},{4,6},{6,0},{8,10},{10,12},{12,14},{14,8},{16,18},{18,... | collective-permute-start | bytes 2162696 | tf_op jit(solution)/shard_map/ppermute | solution.py:47
  50.1 39.9 %collective-permute-start.9 = (bf16[88,2048]{1,0:T(8,128)(2,1)}, bf16[88,2048]{1,0:T(8,128)(2,1)}, u32[]{:S(2)}, u32[]{:S(2)}) collective-permute-start(bf16[88,2048]{1,0:T(8,128)(2,1)} %d0.1), channel_id=1, source_target_pairs={{0,6},{2,0},{4,2},{6,4},{8,14},{10,8},{12,10},{14,12},{16,22},{18,... | collective-permute-start | bytes 1081352 | tf_op jit(solution)/shard_map/ppermute | solution.py:47
  53.3 51.3 %collective-permute-start.7 = (bf16[176,2048]{1,0:T(8,128)(2,1)}, bf16[176,2048]{1,0:T(8,128)(2,1)}, u32[]{:S(2)}, u32[]{:S(2)}) collective-permute-start(bf16[176,2048]{1,0:T(8,128)(2,1)} %collective-permute-done.6.refs_2_), channel_id=1, source_target_pairs={{0,6},{2,0},{4,2},{6,4},{8,14},{10,8},{12,10},{14,12},{16,22},{18,... | collective-permute-start | bytes 2162696 | tf_op jit(solution)/shard_map/ppermute | solution.py:47
  57.5 13.8 %all-to-all-start.2 = ((bf16[16,24,128]{2,1,0:T(8,128)(2,1)}), bf16[16,24,128]{2,1,0:T(8,128)(2,1)S(1)}, u32[]{:S(2)}, u32[]{:S(2)}) async-start(bf16[16,24,128]{2,1,0:T(8,128)(2,1)} %broadcast_in_dim.13), calls=%async_computation.2 | async-start | bytes 196608 | tf_op jit(solution)/shard_map/all_to_all | solution.py:28
  62.8 8.5 %copy-start.4 = (f32[2048]{0:T(1024)S(1)}, f32[2048]{0:T(1024)}, u32[]{:S(2)}) copy-start(f32[2048]{0:T(1024)} %param.25) | copy-start | bytes 24580
  63.6 0.8 copy-start.8
  65.8 11.1 %copy-start.2 = (f32[8,128]{1,0:T(8,128)S(1)}, f32[8,128]{1,0:T(8,128)}, u32[]{:S(2)}) copy-start(f32[8,128]{1,0:T(8,128)} %floor_rows.1) | copy-start | bytes 12292
  65.8 17.9 %copy-start = (f32[3,8,128,128]{3,2,1,0:T(8,128)S(1)}, f32[3,8,128,128]{3,2,1,0:T(8,128)}, u32[]{:S(2)}) copy-start(f32[3,8,128,128]{3,2,1,0:T(8,128)} %state.3) | copy-start | bytes 4718596
  65.8 17.9 %copy-start.6 = (f32[8,128]{1,0:T(8,128)S(1)}, f32[8,128]{1,0:T(8,128)}, u32[]{:S(2)}) copy-start(f32[8,128]{1,0:T(8,128)} %gain.1) | copy-start | bytes 12292
  73.5 10.1 %all-to-all-start.3 = ((bf16[8,16,128]{2,1,0:T(8,128)(2,1)}), bf16[8,16,128]{2,1,0:T(8,128)(2,1)S(1)}, u32[]{:S(2)}, u32[]{:S(2)}) async-start(bf16[8,16,128]{2,1,0:T(8,128)(2,1)} %bitcast.11), calls=%async_computation.3 | async-start | bytes 65536 | tf_op jit(solution)/shard_map/all_to_all | solution.py:28
  85.6 12.9 %all-to-all-start.4 = ((bf16[16,24,128]{2,1,0:T(8,128)(2,1)}), bf16[16,24,128]{2,1,0:T(8,128)(2,1)S(1)}, u32[]{:S(2)}, u32[]{:S(2)}) async-start(bf16[16,24,128]{2,1,0:T(8,128)(2,1)} %broadcast_in_dim.14), calls=%async_computation.4 | async-start | bytes 196608 | tf_op jit(solution)/shard_map/all_to_all | solution.py:28
  90.0 14.6 %collective-permute-start.8 = (bf16[88,2048]{1,0:T(8,128)(2,1)}, bf16[88,2048]{1,0:T(8,128)(2,1)S(1)}, u32[]{:S(2)}, u32[]{:S(2)}) collective-permute-start(bf16[88,2048]{1,0:T(8,128)(2,1)} %d0.1), channel_id=1, source_target_pairs={{0,2},{2,4},{4,6},{6,0},{8,10},{10,12},{12,14},{14,8},{16,18},{18,... | collective-permute-start | bytes 1081352 | tf_op jit(solution)/shard_map/ppermute | solution.py:47
  90.0 14.6 %collective-permute-start.10 = (bf16[88,2048]{1,0:T(8,128)(2,1)}, bf16[88,2048]{1,0:T(8,128)(2,1)S(1)}, u32[]{:S(2)}, u32[]{:S(2)}) collective-permute-start(bf16[88,2048]{1,0:T(8,128)(2,1)} %collective-permute-done.9.d2), channel_id=1, source_target_pairs={{0,6},{2,0},{4,2},{6,4},{8,14},{10,8},{12,10},{14,12},{16,22},{18,... | collective-permute-start | bytes 1081352 | tf_op jit(solution)/shard_map/ppermute | solution.py:47
  99.5 11.7 %all-to-all-start.5 = ((bf16[16,24,128]{2,1,0:T(8,128)(2,1)}), bf16[16,24,128]{2,1,0:T(8,128)(2,1)S(1)}, u32[]{:S(2)}, u32[]{:S(2)}) async-start(bf16[16,24,128]{2,1,0:T(8,128)(2,1)} %broadcast_in_dim.15), calls=%async_computation.5 | async-start | bytes 196608 | tf_op jit(solution)/shard_map/all_to_all | solution.py:28
  102.9 8.3 %copy-start.5 = (f32[2048]{0:T(1024)S(1)}, f32[2048]{0:T(1024)}, u32[]{:S(2)}) copy-start(f32[2048]{0:T(1024)} %param.32) | copy-start | bytes 24580
  114.8 15.4 %all-to-all-start.6 = ((bf16[64,8,128]{2,1,0:T(8,128)(2,1)}), bf16[64,8,128]{2,1,0:T(8,128)(2,1)S(1)}, u32[]{:S(2)}, u32[]{:S(2)}) async-start(bf16[64,8,128]{2,1,0:T(8,128)(2,1)} %shard_map.195), calls=%async_computation.6 | async-start | bytes 262144 | tf_op jit(solution)/shard_map/all_to_all | solution.py:28
  119.1 1.4 %copy-start.1 = (f32[3,8,128,128]{3,2,1,0:T(8,128)S(1)}, f32[3,8,128,128]{3,2,1,0:T(8,128)}, u32[]{:S(2)}) copy-start(f32[3,8,128,128]{3,2,1,0:T(8,128)} %state.3) | copy-start | bytes 4718596

commit v6 on v5

--- a/solution.py
+++ b/solution.py
@@ -117,7 +117,7 @@
         move.wait()
 
 
-def first_block(own, other, gain, w_gate, w_up, w_down, mine, theirs, slab, xt, low):
+def first_block(own, other, gain, w_gate, w_up, w_down, theirs, slab, mid_out, xt):
     z, y, core = place()
     cols = own.shape[1]
     for kv in range(KV_COUNT):
@@ -148,16 +148,21 @@
         + rem(new, seqs)
     )
     mid = bf(matmul(hot(old == wanted), mid, NT))
-    low[...] = matmul(mid, w_down[...], NN)
+    mid_out[...] = mid
     for k in range(Z_COUNT):
-        at = pl.multiple_of((k * TP_COUNT + core) * LANES, LANES)
         to = pl.multiple_of((k * TP_COUNT + 1 - core) * LANES, LANES)
-        mine[k] = low[:, pl.ds(at, LANES)]
-        theirs[k] = bf(low[:, pl.ds(to, LANES)])
+        theirs[k] = bf(matmul(mid, w_down[:, pl.ds(to, LANES)], NN))
     at = pl.multiple_of((z * TP_COUNT + core) * LANES, LANES)
     new, old = iota((count, rows), 0), iota((count, rows), 1)
     pick = hot(old == div(new, seqs) * (Y_COUNT * seqs) + y * seqs + rem(new, seqs))
     slab[...] = matmul(pick, xt[pl.ds(at, LANES), :], NT)
+
+
+def own_half(mid, w_down, mine):
+    _, _, core = place()
+    for k in range(Z_COUNT):
+        at = pl.multiple_of((k * TP_COUNT + core) * LANES, LANES)
+        mine[k] = matmul(mid[...], w_down[:, pl.ds(at, LANES)], NN)
 
 
 def load_mix(a0, a1, a2, a3, w_mix, sems):
@@ -499,20 +504,22 @@
         vmem=True,
     )
     other = swap_cores(own)
-    mine, theirs, slab = local(
+    theirs, slab, mid = local(
         first_block,
         [
-            ((Z_COUNT, rows, LANES), half32),
             ((Z_COUNT, rows, LANES), half16),
             ((slab_rows, LANES), half32),
+            ((rows, hidden), half16),
         ],
         own,
         other,
         ffn_gain_one.reshape(-1, LANES),
         *first_w,
-        scratch=(pltpu.VMEM((width, rows), half16), pltpu.VMEM((rows, width), half32)),
-    )
-    both = bf(mine + f32(swap_cores(theirs)))
+        scratch=(pltpu.VMEM((width, rows), half16),),
+    )
+    from_other = swap_cores(theirs)
+    (mine,) = local(own_half, [((Z_COUNT, rows, LANES), half32)], mid, first_w[2])
+    both = bf(mine + f32(from_other))
     summed = exchange(both.reshape(KV_COUNT, slab_rows, LANES), "kv")
     below, above = shift_y(early, 1), shift_y(early, -1)
     twice = shift_y(below, 1)

time: 132 us -> 132 us (level)
    pallas_call x13 -> x14, Pallas kernels: 19.3 us -> 19.3 us  [local(): pl.pallas_call(body, out_shape=shapes, in_specs=specs, out_specs=placed,...]
where the time goes in v6:
time: 132 us; the launch traced here: 131 us
  starting transfers between devices  41.7 us (32%)
  waiting for transfers between devices  39.1 us (30%)
  blocking collectives  23.1 us (18%)
  Pallas kernels  19.3 us (15%)
  local copies, waits for them, and re-layouts  4.99 us (4%)
  other arithmetic  1.7 us (1%)
    all_to_all x6, waiting for transfers between devices, exchange(): lax.all_to_all(tiles, axis, split_axis=0, concat_axis=0, axis_index_group...  29.3 us
    all_to_all x6, starting transfers between devices, exchange(): lax.all_to_all(tiles, axis, split_axis=0, concat_axis=0, axis_index_group...  24.7 us
    all_to_all x1, blocking collectives, exchange(): lax.all_to_all(tiles, axis, split_axis=0, concat_axis=0, axis_index_group...  23.1 us
    pallas_call x14, Pallas kernels, local(): pl.pallas_call(body, out_shape=shapes, in_specs=specs, out_specs=placed,...  19.3 us
    ppermute x9, starting transfers between devices, shift_y(): return lax.ppermute(x, 'kv', pairs)  14.3 us
    ppermute x9, waiting for transfers between devices, shift_y(): return lax.ppermute(x, 'kv', pairs)  9.79 us
    broadcast_in_dim x4, local copies, waits for them, and re-layouts, copies(): return jnp.broadcast_to(x, (count, *x.shape))  2.71 us
  transfers between devices with their start and end apart: 17, of which 9 were waited for; matrix products, arithmetic and copies ran while one was open for 3% of the time, Pallas kernels for 11%

profile of v6, /device:TPU:1, one launch (start us, length us, event | category | flops | bytes accessed | tf_op | source)
XLA Modules:
  0.0 130.9 jit_solution(10818371882368029879)
XLA Ops:
  0.6 0.7 broadcast_in_dim.12
  1.4 23.1 %all_to_all.35.own = bf16[32,32,96]{2,1,0:T(8,128)(2,1)S(1)} all-to-all(bf16[32,32,96]{2,1,0:T(8,128)(2,1)S(1)} %broadcast_in_dim.12), channel_id=1, replica_groups=mesh['dp'=4,'kv'=32,'tp'=2] {'kv'}, dimensions={0} | all-to-all | bytes 393216 | tf_op jit(solution)/shard_map/all_to_all | solution.py:28
  24.5 2.5 %collective-permute-start = (bf16[32,32,96]{2,1,0:T(8,128)(2,1)S(1)}, bf16[32,32,96]{2,1,0:T(8,128)(2,1)S(1)}, u32[]{:S(2)}, u32[]{:S(2)}) collective-permute-start(bf16[32,32,96]{2,1,0:T(8,128)(2,1)S(1)} %all_to_all.35.own), channel_id=1, source_target_pairs={{0,1},{1,0},{2,3},{3,2},{4,5},{5,4},{6,7},{7,6},{8,9},{9,8},{10,11... | collective-permute-start | bytes 589832 | tf_op jit(solution)/shard_map/ppermute | solution.py:38
  27.0 2.1 %shard_map.188.refs_0_.a0 = bf16[160,2048]{1,0:T(8,128)(2,1)} custom-call(bf16[8,4,2048]{2,1,0:T(4,128)(2,1)} %bitcast.25, bf16[8,4,2048]{2,1,0:T(4,128)(2,1)} %bitcast.26, bf16[8,4,2048]{2,1,0:T(4,128)(2,1)} %bitcast.27, bf16[8,4,2048]{2,1,0:T(4,128)(2,1)} %bitcast.28, bf16[32,2048]{1,0:T(8,128)(2,1)} %bitcast.29), custom_call_target="tpu_custom_call" | custom-call | flops 1048576 | bytes 655360 | tf_op jit(solution)/shard_map/pallas_call | solution.py:95
  29.0 0.0 copy-start.9
  29.1 0.0 copy-start.10
  29.1 0.1 collective-permute-start.2
  29.2 1.3 shard_map.185
  30.5 0.0 collective-permute-done.other
  30.5 1.3 shard_map.186
  31.8 0.2 collective-permute-start.1
  32.0 0.9 pad_maximum_fusion.refs_0_
  32.9 2.8 %collective-permute-start.6 = (bf16[176,2048]{1,0:T(8,128)(2,1)}, bf16[176,2048]{1,0:T(8,128)(2,1)}, u32[]{:S(2)}, u32[]{:S(2)}) collective-permute-start(bf16[176,2048]{1,0:T(8,128)(2,1)} %pad_maximum_fusion.refs_0_), channel_id=1, source_target_pairs={{0,6},{2,0},{4,2},{6,4},{8,14},{10,8},{12,10},{14,12},{16,22},{18,... | collective-permute-start | bytes 2162696 | tf_op jit(solution)/shard_map/ppermute | solution.py:47
  35.7 0.2 shard_map.187
  35.9 0.0 collective-permute-done.1
  35.9 0.7 add_convert_fusion
  36.6 3.9 %all-to-all-start.1 = ((bf16[32,24,128]{2,1,0:T(8,128)(2,1)}), bf16[32,24,128]{2,1,0:T(8,128)(2,1)S(1)}, u32[]{:S(2)}, u32[]{:S(2)}) async-start(bf16[32,24,128]{2,1,0:T(8,128)(2,1)} %bitcast.4), calls=%async_computation.1 | async-start | bytes 393216 | tf_op jit(solution)/shard_map/all_to_all | solution.py:28
  40.5 6.9 %collective-permute-done.2.refs_1_.a1 = bf16[160,2048]{1,0:T(8,128)(2,1)S(1)} collective-permute-done((bf16[160,2048]{1,0:T(8,128)(2,1)}, bf16[160,2048]{1,0:T(8,128)(2,1)S(1)}, u32[]{:S(2)}, u32[]{:S(2)}) %collective-permute-start.2) | collective-permute-done | bytes 655392 | tf_op jit(solution)/shard_map/ppermute | solution.py:47
  47.4 0.0 collective-permute-start.3
  47.4 2.7 %collective-permute-start.4 = (bf16[160,2048]{1,0:T(8,128)(2,1)}, bf16[160,2048]{1,0:T(8,128)(2,1)}, u32[]{:S(2)}, u32[]{:S(2)}) collective-permute-start(bf16[160,2048]{1,0:T(8,128)(2,1)} %shard_map.188.refs_0_.a0), channel_id=1, source_target_pairs={{0,6},{2,0},{4,2},{6,4},{8,14},{10,8},{12,10},{14,12},{16,22},{18,... | collective-permute-start | bytes 1966088 | tf_op jit(solution)/shard_map/ppermute | solution.py:47
  50.1 0.0 collective-permute-start.5
  50.1 2.7 %collective-permute-start.9 = (bf16[88,2048]{1,0:T(8,128)(2,1)}, bf16[88,2048]{1,0:T(8,128)(2,1)}, u32[]{:S(2)}, u32[]{:S(2)}) collective-permute-start(bf16[88,2048]{1,0:T(8,128)(2,1)} %d0.1), channel_id=1, source_target_pairs={{0,6},{2,0},{4,2},{6,4},{8,14},{10,8},{12,10},{14,12},{16,22},{18,... | collective-permute-start | bytes 1081352 | tf_op jit(solution)/shard_map/ppermute | solution.py:47
  52.7 0.4 collective-permute-done.6.refs_2_
  53.2 3.5 %collective-permute-start.7 = (bf16[176,2048]{1,0:T(8,128)(2,1)}, bf16[176,2048]{1,0:T(8,128)(2,1)}, u32[]{:S(2)}, u32[]{:S(2)}) collective-permute-start(bf16[176,2048]{1,0:T(8,128)(2,1)} %collective-permute-done.6.refs_2_), channel_id=1, source_target_pairs={{0,6},{2,0},{4,2},{6,4},{8,14},{10,8},{12,10},{14,12},{16,22},{18,... | collective-permute-start | bytes 2162696 | tf_op jit(solution)/shard_map/ppermute | solution.py:47
  56.6 0.0 all-to-all-done.1
  56.7 0.6 broadcast_in_dim.13
  57.3 5.3 %all-to-all-start.2 = ((bf16[16,24,128]{2,1,0:T(8,128)(2,1)}), bf16[16,24,128]{2,1,0:T(8,128)(2,1)S(1)}, u32[]{:S(2)}, u32[]{:S(2)}) async-start(bf16[16,24,128]{2,1,0:T(8,128)(2,1)} %broadcast_in_dim.13), calls=%async_computation.2 | async-start | bytes 196608 | tf_op jit(solution)/shard_map/all_to_all | solution.py:28
  62.7 0.9 collective-permute-done.3.refs_2_.a2
  63.6 0.8 copy-done.8
  64.5 1.4 %shard_map.189.w_held = bf16[3,128,2048]{2,1,0:T(8,128)(2,1)S(1)} custom-call(bf16[160,2048]{1,0:T(8,128)(2,1)} %shard_map.188.refs_0_.a0, bf16[160,2048]{1,0:T(8,128)(2,1)} %copy-done.7, bf16[160,2048]{1,0:T(8,128)(2,1)} %copy-done.8), custom_call_target="tpu_custom_call" | custom-call | flops 1048576 | bytes 1966080 | tf_op jit(solution)/shard_map/pallas_call | solution.py:95
  65.8 0.0 copy-start.2
  65.9 0.0 copy-start
  65.9 0.0 copy-start.6
  65.9 1.5 %collective-permute-done.4.a3 = bf16[160,2048]{1,0:T(8,128)(2,1)} collective-permute-done((bf16[160,2048]{1,0:T(8,128)(2,1)}, bf16[160,2048]{1,0:T(8,128)(2,1)}, u32[]{:S(2)}, u32[]{:S(2)}) %collective-permute-start.4) | collective-permute-done | bytes 655392 | tf_op jit(solution)/shard_map/ppermute | solution.py:47
  67.4 3.8 %all-to-all-done.2.tiles = bf16[16,24,128]{2,1,0:T(8,128)(2,1)S(1)} async-done(((bf16[16,24,128]{2,1,0:T(8,128)(2,1)}), bf16[16,24,128]{2,1,0:T(8,128)(2,1)S(1)}, u32[]{:S(2)}, u32[]{:S(2)}) %all-to-all-start.2) | async-done | bytes 98336 | tf_op jit(solution)/shard_map/all_to_all | solution.py:28
  71.2 2.2 %shard_map.190 = (bf16[128,128]{1,0:T(8,128)(2,1)}, f32[24,128]{1,0:T(8,128)S(1)}) custom-call(bf16[16,24,128]{2,1,0:T(8,128)(2,1)S(1)} %all-to-all-done.2.tiles, f32[1,2048]{1,0:T(1,128)S(1)} %bitcast.19, bf16[3,128,2048]{2,1,0:T(8,128)(2,1)S(1)} %shard_map.189.w_held, bf16[160,2048]{1,0:T(8,128)(2,1)} %collective-permute-done.4.a3), custom_call_target="tpu_custom_call" | custom-call | flops 1048576 | bytes 2334720 | tf_op jit(solution)/shard_map/pallas_call | solution.py:95
  73.4 3.3 %all-to-all-start.3 = ((bf16[8,16,128]{2,1,0:T(8,128)(2,1)}), bf16[8,16,128]{2,1,0:T(8,128)(2,1)S(1)}, u32[]{:S(2)}, u32[]{:S(2)}) async-start(bf16[8,16,128]{2,1,0:T(8,128)(2,1)} %bitcast.11), calls=%async_computation.3 | async-start | bytes 65536 | tf_op jit(solution)/shard_map/all_to_all | solution.py:28
  76.7 0.1 shard_map.191.floor_t
  76.8 6.7 %all-to-all-done.3 = bf16[8,16,128]{2,1,0:T(8,128)(2,1)S(1)} async-done(((bf16[8,16,128]{2,1,0:T(8,128)(2,1)}), bf16[8,16,128]{2,1,0:T(8,128)(2,1)S(1)}, u32[]{:S(2)}, u32[]{:S(2)}) %all-to-all-start.3) | async-done | bytes 32800 | tf_op jit(solution)/shard_map/all_to_all | solution.py:28
  83.5 1.2 shard_map.192
  84.7 0.7 broadcast_in_dim.14
  85.4 4.4 %all-to-all-start.4 = ((bf16[16,24,128]{2,1,0:T(8,128)(2,1)}), bf16[16,24,128]{2,1,0:T(8,128)(2,1)S(1)}, u32[]{:S(2)}, u32[]{:S(2)}) async-start(bf16[16,24,128]{2,1,0:T(8,128)(2,1)} %broadcast_in_dim.14), calls=%async_computation.4 | async-start | bytes 196608 | tf_op jit(solution)/shard_map/all_to_all | solution.py:28
  89.8 0.0 collective-permute-start.8
  89.8 0.0 collective-permute-done.9.d2
  89.8 2.7 %collective-permute-start.10 = (bf16[88,2048]{1,0:T(8,128)(2,1)}, bf16[88,2048]{1,0:T(8,128)(2,1)S(1)}, u32[]{:S(2)}, u32[]{:S(2)}) collective-permute-start(bf16[88,2048]{1,0:T(8,128)(2,1)} %collective-permute-done.9.d2), channel_id=1, source_target_pairs={{0,6},{2,0},{4,2},{6,4},{8,14},{10,8},{12,10},{14,12},{16,22},{18,... | collective-permute-start | bytes 1081352 | tf_op jit(solution)/shard_map/ppermute | solution.py:47
  92.5 1.1 shard_map.193.w_mix
  93.6 4.7 %all-to-all-done.4.tiles = bf16[16,24,128]{2,1,0:T(8,128)(2,1)S(1)} async-done(((bf16[16,24,128]{2,1,0:T(8,128)(2,1)}), bf16[16,24,128]{2,1,0:T(8,128)(2,1)S(1)}, u32[]{:S(2)}, u32[]{:S(2)}) %all-to-all-start.4) | async-done | bytes 98336 | tf_op jit(solution)/shard_map/all_to_all | solution.py:28
  98.3 0.4 shard_map.194.after
  98.7 0.7 broadcast_in_dim.15
  99.4 3.4 %all-to-all-start.5 = ((bf16[16,24,128]{2,1,0:T(8,128)(2,1)}), bf16[16,24,128]{2,1,0:T(8,128)(2,1)S(1)}, u32[]{:S(2)}, u32[]{:S(2)}) async-start(bf16[16,24,128]{2,1,0:T(8,128)(2,1)} %broadcast_in_dim.15), calls=%async_computation.5 | async-start | bytes 196608 | tf_op jit(solution)/shard_map/all_to_all | solution.py:28
  102.8 0.0 copy-start.5
  102.8 0.0 collective-permute-done.5.refs_1_
  102.8 1.6 %shard_map.195.w_held = bf16[3,176,2048]{2,1,0:T(8,128)(2,1)S(1)} custom-call(bf16[176,2048]{1,0:T(8,128)(2,1)} %pad_maximum_fusion.refs_0_, bf16[176,2048]{1,0:T(8,128)(2,1)} %collective-permute-done.5.refs_1_, bf16[176,2048]{1,0:T(8,128)(2,1)} %collective-permute-done.6.refs_2_), custom_call_target="tpu_custom_call" | custom-call | flops 1048576 | bytes 2162688 | tf_op jit(solution)/shard_map/pallas_call | solution.py:95
  104.4 0.0 collective-permute-done.8.d1
  104.4 0.0 collective-permute-done.10.d3
  104.4 0.0 collective-permute-done.7.t3
  104.4 6.7 %all-to-all-done.5.tiles = bf16[16,24,128]{2,1,0:T(8,128)(2,1)S(1)} async-done(((bf16[16,24,128]{2,1,0:T(8,128)(2,1)}), bf16[16,24,128]{2,1,0:T(8,128)(2,1)S(1)}, u32[]{:S(2)}, u32[]{:S(2)}) %all-to-all-start.5) | async-done | bytes 98336 | tf_op jit(solution)/shard_map/all_to_all | solution.py:28
  111.1 3.5 %shard_map.196 = bf16[64,8,128]{2,1,0:T(8,128)(2,1)} custom-call(bf16[16,24,128]{2,1,0:T(8,128)(2,1)S(1)} %all-to-all-done.5.tiles, f32[1,2048]{1,0:T(1,128)S(1)} %bitcast.20, bf16[24,128]{1,0:T(8,128)(2,1)S(1)} %shard_map.194.after, bf16[3,176,2048]{2,1,0:T(8,128)(2,1)S(1)} %shard_map.195.w_held, bf16[176,2048]{1,0:T(8,128)(2,1)} %collective-permute-done.7.t3, ...), custom_call_target="tpu_custom_call" | custom-call | flops 1048576 | bytes 4438016 | tf_op jit(solution)/shard_map/pallas_call | solution.py:95
  114.6 4.3 %all-to-all-start.6 = ((bf16[64,8,128]{2,1,0:T(8,128)(2,1)}), bf16[64,8,128]{2,1,0:T(8,128)(2,1)S(1)}, u32[]{:S(2)}, u32[]{:S(2)}) async-start(bf16[64,8,128]{2,1,0:T(8,128)(2,1)} %shard_map.196), calls=%async_computation.6 | async-start | bytes 262144 | tf_op jit(solution)/shard_map/all_to_all | solution.py:28
  119.0 0.0 copy-start.1
  119.0 1.4 %copy-done.1 = f32[3,8,128,128]{3,2,1,0:T(8,128)S(1)} copy-done((f32[3,8,128,128]{3,2,1,0:T(8,128)S(1)}, f32[3,8,128,128]{3,2,1,0:T(8,128)}, u32[]{:S(2)}) %copy-start.1) | copy-done | bytes 1572888
  120.4 2.2 %shard_map.198 = f32[3,8,128,128]{3,2,1,0:T(8,128)} custom-call(f32[3,8,128,128]{3,2,1,0:T(8,128)S(1)} %copy-done.1, f32[3,24,128]{2,1,0:T(8,128)S(1)} %get-tuple-element.21.vectors), custom_call_target="tpu_custom_call" | custom-call | flops 1048576 | bytes 1609728 | tf_op jit(solution)/shard_map/pallas_call | solution.py:95
  122.6 7.5 %all-to-all-done.6.arrived = bf16[64,8,128]{2,1,0:T(8,128)(2,1)S(1)} async-done(((bf16[64,8,128]{2,1,0:T(8,128)(2,1)}), bf16[64,8,128]{2,1,0:T(8,128)(2,1)S(1)}, u32[]{:S(2)}, u32[]{:S(2)}) %all-to-all-start.6) | async-done | bytes 131104 | tf_op jit(solution)/shard_map/all_to_all | solution.py:28
  130.1 0.8 shard_map.197
  (16 shorter events, 0.1 us)
Async XLA Ops:
  0.6 29.8 %copy-start.3 = (f32[2048]{0:T(1024)S(1)}, f32[2048]{0:T(1024)}, u32[]{:S(2)}) copy-start(f32[2048]{0:T(1024)} %param.21) | copy-start | bytes 24580
  24.5 6.0 %collective-permute-start = (bf16[32,32,96]{2,1,0:T(8,128)(2,1)S(1)}, bf16[32,32,96]{2,1,0:T(8,128)(2,1)S(1)}, u32[]{:S(2)}, u32[]{:S(2)}) collective-permute-start(bf16[32,32,96]{2,1,0:T(8,128)(2,1)S(1)} %all_to_all.35.own), channel_id=1, source_target_pairs={{0,1},{1,0},{2,3},{3,2},{4,5},{5,4},{6,7},{7,6},{8,9},{9,8},{10,11... | collective-permute-start | bytes 589832 | tf_op jit(solution)/shard_map/ppermute | solution.py:38
  29.0 2.9 %copy-start.9 = (bf16[2048,88]{0,1:T(8,128)(2,1)S(1)}, bf16[2048,88]{0,1:T(8,128)(2,1)}, u32[]{:S(2)}) copy-start(bf16[2048,88]{0,1:T(8,128)(2,1)} %param.34) | copy-start | bytes 1081348
  29.1 2.9 %copy-start.10 = (bf16[2048,88]{0,1:T(8,128)(2,1)S(1)}, bf16[2048,88]{0,1:T(8,128)(2,1)}, u32[]{:S(2)}) copy-start(bf16[2048,88]{0,1:T(8,128)(2,1)} %param.33) | copy-start | bytes 1081348
  29.1 18.3 %collective-permute-start.2 = (bf16[160,2048]{1,0:T(8,128)(2,1)}, bf16[160,2048]{1,0:T(8,128)(2,1)S(1)}, u32[]{:S(2)}, u32[]{:S(2)}) collective-permute-start(bf16[160,2048]{1,0:T(8,128)(2,1)} %shard_map.188.refs_0_.a0), channel_id=1, source_target_pairs={{0,2},{2,4},{4,6},{6,0},{8,10},{10,12},{12,14},{14,8},{16,18},{18,... | collective-permute-start | bytes 1966088 | tf_op jit(solution)/shard_map/ppermute | solution.py:47
  31.8 4.1 %collective-permute-start.1 = (bf16[8,96,128]{2,1,0:T(8,128)(2,1)S(1)}, bf16[8,96,128]{2,1,0:T(8,128)(2,1)S(1)}, u32[]{:S(2)}, u32[]{:S(2)}) collective-permute-start(bf16[8,96,128]{2,1,0:T(8,128)(2,1)S(1)} %get-tuple-element.17), channel_id=1, source_target_pairs={{0,1},{1,0},{2,3},{3,2},{4,5},{5,4},{6,7},{7,6},{8,9},{9,8},{10,11... | collective-permute-start | bytes 589832 | tf_op jit(solution)/shard_map/ppermute | solution.py:38
  32.9 20.3 %collective-permute-start.6 = (bf16[176,2048]{1,0:T(8,128)(2,1)}, bf16[176,2048]{1,0:T(8,128)(2,1)}, u32[]{:S(2)}, u32[]{:S(2)}) collective-permute-start(bf16[176,2048]{1,0:T(8,128)(2,1)} %pad_maximum_fusion.refs_0_), channel_id=1, source_target_pairs={{0,6},{2,0},{4,2},{6,4},{8,14},{10,8},{12,10},{14,12},{16,22},{18,... | collective-permute-start | bytes 2162696 | tf_op jit(solution)/shard_map/ppermute | solution.py:47
  36.6 20.0 %all-to-all-start.1 = ((bf16[32,24,128]{2,1,0:T(8,128)(2,1)}), bf16[32,24,128]{2,1,0:T(8,128)(2,1)S(1)}, u32[]{:S(2)}, u32[]{:S(2)}) async-start(bf16[32,24,128]{2,1,0:T(8,128)(2,1)} %bitcast.4), calls=%async_computation.1 | async-start | bytes 393216 | tf_op jit(solution)/shard_map/all_to_all | solution.py:28
  47.4 16.2 %copy-start.7 = (bf16[160,2048]{1,0:T(8,128)(2,1)}, bf16[160,2048]{1,0:T(8,128)(2,1)S(1)}, u32[]{:S(2)}) copy-start(bf16[160,2048]{1,0:T(8,128)(2,1)S(1)} %collective-permute-done.2.refs_1_.a1) | copy-start | bytes 1966084
  47.4 16.2 %collective-permute-start.3 = (bf16[160,2048]{1,0:T(8,128)(2,1)S(1)}, bf16[160,2048]{1,0:T(8,128)(2,1)S(1)}, u32[]{:S(2)}, u32[]{:S(2)}) collective-permute-start(bf16[160,2048]{1,0:T(8,128)(2,1)S(1)} %collective-permute-done.2.refs_1_.a1), channel_id=1, source_target_pairs={{0,2},{2,4},{4,6},{6,0},{8,10},{10,12},{12,14},{14,8},{16,18},{18,... | collective-permute-start | bytes 1966088 | tf_op jit(solution)/shard_map/ppermute | solution.py:47
  47.4 20.0 %collective-permute-start.4 = (bf16[160,2048]{1,0:T(8,128)(2,1)}, bf16[160,2048]{1,0:T(8,128)(2,1)}, u32[]{:S(2)}, u32[]{:S(2)}) collective-permute-start(bf16[160,2048]{1,0:T(8,128)(2,1)} %shard_map.188.refs_0_.a0), channel_id=1, source_target_pairs={{0,6},{2,0},{4,2},{6,4},{8,14},{10,8},{12,10},{14,12},{16,22},{18,... | collective-permute-start | bytes 1966088 | tf_op jit(solution)/shard_map/ppermute | solution.py:47
  50.1 52.7 %collective-permute-start.5 = (bf16[176,2048]{1,0:T(8,128)(2,1)}, bf16[176,2048]{1,0:T(8,128)(2,1)}, u32[]{:S(2)}, u32[]{:S(2)}) collective-permute-start(bf16[176,2048]{1,0:T(8,128)(2,1)} %pad_maximum_fusion.refs_0_), channel_id=1, source_target_pairs={{0,2},{2,4},{4,6},{6,0},{8,10},{10,12},{12,14},{14,8},{16,18},{18,... | collective-permute-start | bytes 2162696 | tf_op jit(solution)/shard_map/ppermute | solution.py:47
  50.1 39.7 %collective-permute-start.9 = (bf16[88,2048]{1,0:T(8,128)(2,1)}, bf16[88,2048]{1,0:T(8,128)(2,1)}, u32[]{:S(2)}, u32[]{:S(2)}) collective-permute-start(bf16[88,2048]{1,0:T(8,128)(2,1)} %d0.1), channel_id=1, source_target_pairs={{0,6},{2,0},{4,2},{6,4},{8,14},{10,8},{12,10},{14,12},{16,22},{18,... | collective-permute-start | bytes 1081352 | tf_op jit(solution)/shard_map/ppermute | solution.py:47
  53.2 51.2 %collective-permute-start.7 = (bf16[176,2048]{1,0:T(8,128)(2,1)}, bf16[176,2048]{1,0:T(8,128)(2,1)}, u32[]{:S(2)}, u32[]{:S(2)}) collective-permute-start(bf16[176,2048]{1,0:T(8,128)(2,1)} %collective-permute-done.6.refs_2_), channel_id=1, source_target_pairs={{0,6},{2,0},{4,2},{6,4},{8,14},{10,8},{12,10},{14,12},{16,22},{18,... | collective-permute-start | bytes 2162696 | tf_op jit(solution)/shard_map/ppermute | solution.py:47
  57.3 13.8 %all-to-all-start.2 = ((bf16[16,24,128]{2,1,0:T(8,128)(2,1)}), bf16[16,24,128]{2,1,0:T(8,128)(2,1)S(1)}, u32[]{:S(2)}, u32[]{:S(2)}) async-start(bf16[16,24,128]{2,1,0:T(8,128)(2,1)} %broadcast_in_dim.13), calls=%async_computation.2 | async-start | bytes 196608 | tf_op jit(solution)/shard_map/all_to_all | solution.py:28
  62.7 8.5 %copy-start.4 = (f32[2048]{0:T(1024)S(1)}, f32[2048]{0:T(1024)}, u32[]{:S(2)}) copy-start(f32[2048]{0:T(1024)} %param.25) | copy-start | bytes 24580
  63.6 0.8 copy-start.8
  65.8 10.9 %copy-start.2 = (f32[8,128]{1,0:T(8,128)S(1)}, f32[8,128]{1,0:T(8,128)}, u32[]{:S(2)}) copy-start(f32[8,128]{1,0:T(8,128)} %floor_rows.1) | copy-start | bytes 12292
  65.9 17.7 %copy-start = (f32[3,8,128,128]{3,2,1,0:T(8,128)S(1)}, f32[3,8,128,128]{3,2,1,0:T(8,128)}, u32[]{:S(2)}) copy-start(f32[3,8,128,128]{3,2,1,0:T(8,128)} %state.3) | copy-start | bytes 4718596
  65.9 17.6 %copy-start.6 = (f32[8,128]{1,0:T(8,128)S(1)}, f32[8,128]{1,0:T(8,128)}, u32[]{:S(2)}) copy-start(f32[8,128]{1,0:T(8,128)} %gain.1) | copy-start | bytes 12292
  73.4 10.1 %all-to-all-start.3 = ((bf16[8,16,128]{2,1,0:T(8,128)(2,1)}), bf16[8,16,128]{2,1,0:T(8,128)(2,1)S(1)}, u32[]{:S(2)}, u32[]{:S(2)}) async-start(bf16[8,16,128]{2,1,0:T(8,128)(2,1)} %bitcast.11), calls=%async_computation.3 | async-start | bytes 65536 | tf_op jit(solution)/shard_map/all_to_all | solution.py:28
  85.4 12.9 %all-to-all-start.4 = ((bf16[16,24,128]{2,1,0:T(8,128)(2,1)}), bf16[16,24,128]{2,1,0:T(8,128)(2,1)S(1)}, u32[]{:S(2)}, u32[]{:S(2)}) async-start(bf16[16,24,128]{2,1,0:T(8,128)(2,1)} %broadcast_in_dim.14), calls=%async_computation.4 | async-start | bytes 196608 | tf_op jit(solution)/shard_map/all_to_all | solution.py:28
  89.8 14.6 %collective-permute-start.8 = (bf16[88,2048]{1,0:T(8,128)(2,1)}, bf16[88,2048]{1,0:T(8,128)(2,1)S(1)}, u32[]{:S(2)}, u32[]{:S(2)}) collective-permute-start(bf16[88,2048]{1,0:T(8,128)(2,1)} %d0.1), channel_id=1, source_target_pairs={{0,2},{2,4},{4,6},{6,0},{8,10},{10,12},{12,14},{14,8},{16,18},{18,... | collective-permute-start | bytes 1081352 | tf_op jit(solution)/shard_map/ppermute | solution.py:47
  89.8 14.6 %collective-permute-start.10 = (bf16[88,2048]{1,0:T(8,128)(2,1)}, bf16[88,2048]{1,0:T(8,128)(2,1)S(1)}, u32[]{:S(2)}, u32[]{:S(2)}) collective-permute-start(bf16[88,2048]{1,0:T(8,128)(2,1)} %collective-permute-done.9.d2), channel_id=1, source_target_pairs={{0,6},{2,0},{4,2},{6,4},{8,14},{10,8},{12,10},{14,12},{16,22},{18,... | collective-permute-start | bytes 1081352 | tf_op jit(solution)/shard_map/ppermute | solution.py:47
  99.4 11.7 %all-to-all-start.5 = ((bf16[16,24,128]{2,1,0:T(8,128)(2,1)}), bf16[16,24,128]{2,1,0:T(8,128)(2,1)S(1)}, u32[]{:S(2)}, u32[]{:S(2)}) async-start(bf16[16,24,128]{2,1,0:T(8,128)(2,1)} %broadcast_in_dim.15), calls=%async_computation.5 | async-start | bytes 196608 | tf_op jit(solution)/shard_map/all_to_all | solution.py:28
  102.8 8.3 %copy-start.5 = (f32[2048]{0:T(1024)S(1)}, f32[2048]{0:T(1024)}, u32[]{:S(2)}) copy-start(f32[2048]{0:T(1024)} %param.32) | copy-start | bytes 24580
  114.6 15.4 %all-to-all-start.6 = ((bf16[64,8,128]{2,1,0:T(8,128)(2,1)}), bf16[64,8,128]{2,1,0:T(8,128)(2,1)S(1)}, u32[]{:S(2)}, u32[]{:S(2)}) async-start(bf16[64,8,128]{2,1,0:T(8,128)(2,1)} %shard_map.196), calls=%async_computation.6 | async-start | bytes 262144 | tf_op jit(solution)/shard_map/all_to_all | solution.py:28
  119.0 1.4 %copy-start.1 = (f32[3,8,128,128]{3,2,1,0:T(8,128)S(1)}, f32[3,8,128,128]{3,2,1,0:T(8,128)}, u32[]{:S(2)}) copy-start(f32[3,8,128,128]{3,2,1,0:T(8,128)} %state.3) | copy-start | bytes 4718596
